TPU v7x, 512 devices: a whole 4x8x8 slice. The times are simulated.
512 devices in a mesh: sp: 32 (over z, x), dp: 16 (over y, core).
Axes of the slice: x: 4, y: 8, z: 8, core: 2. Of those that a mesh axis runs over, the one named last changes fastest.
Arguments:
- layer_activity: bfloat16 [16, 4096, 2048], P('dp', 'sp'), may hold values from -6 to 6
- writer_matrix: bfloat16 [2048, 256], P('dp'), may hold values from -0.125 to 0.125
- reader_matrix: bfloat16 [2048, 256], P('dp'), may hold values from -0.125 to 0.125
- source_unfiltered: bfloat16 [16, 4096, 2048], P('dp', 'sp'), may hold values from -6 to 6
- switch_raw_signal: bfloat16 [16, 4096, 2048], P('dp', 'sp'), may hold values from -6 to 6
- saved_result: bfloat16 [16, 4096, 2048], P('dp', 'sp'), may hold values from -6 to 6
- final_adjoint: bfloat16 [16, 4096, 2048], P('dp', 'sp'), may hold values from -6 to 6
- delta_raw: bfloat16 [16, 4096, 32], P('dp', 'sp'), may hold values from -4 to 4
- extra_logdrop: float32 [16, 4096, 32], P('dp', None, 'sp'), may hold values from 0 to 2.1
- source_filter_coefs: float32 [5, 2048], P(None, 'sp'), may hold values from -2.5 to 2.5
- writer_filter_coefs: float32 [5, 256], replicated, may hold values from -2.5 to 2.5
- reader_filter_coefs: float32 [5, 256], replicated, may hold values from -2.5 to 2.5
- delta_offset: float32 [32], P('sp'), may hold values from -7.5 to -6
- fading_exponents: float32 [32], P('sp'), may hold values from -6 to 3.4
- direct_factor: float32 [32], P('sp'), may hold values from 0.1 to 1.9
- rescale_factor: float32 [2048], replicated, may hold values from 0.1 to 1.9
Outputs:
- d_hidden: bfloat16 [16, 4096, 2048], P('dp', 'sp')
- d_x_raw: bfloat16 [16, 4096, 2048], P('dp', 'sp')
- d_gate: bfloat16 [16, 4096, 2048], P('dp', 'sp')
- d_dt_raw: bfloat16 [16, 4096, 32], P('dp', 'sp')
- d_w_b: float32 [2048, 256], P('dp')
- d_w_c: float32 [2048, 256], P('dp')
All inputs are finite; a program needn't handle non-finite values.
Results may differ from a plain program's by a relative error of at most 0.012.
Values may be sent and summed in bfloat16 or wider, within the bound.
A program may use at most 128 MiB of HBM per device.

v0:
```python
import functools

import jax
import jax.numpy as jnp
from jax import lax
from jax.sharding import Mesh
from jax.sharding import PartitionSpec as P

HEADS = 32
HEAD_DIM = 64
STATE = 128
GROUPS = 2
NORM_GROUPS = 8
CONV_K = 5
BLOCK = 128
INNER = 2048
SP = ("sp_0", "sp_1")


EPSILON = 1e-06
highest = lax.Precision.HIGHEST


def laid_out(blocks, dim):
    dims = list(blocks.shape[1:])
    dims[dim] *= blocks.shape[0]
    return jnp.moveaxis(blocks, 0, dim).reshape(dims)


def sent_to_all(value, axis):
    copies = jnp.broadcast_to(value, (lax.axis_size(axis), *value.shape))
    return lax.all_to_all(copies, axis, split_axis=0, concat_axis=0, tiled=True)


def gathered_copies(value, axis, dim):
    return laid_out(sent_to_all(value, axis), dim)


def in_one_piece(arrays, axis, split_dim, concat_dim, along):
    widths = [a.shape[along] for a in arrays]
    both = jnp.concatenate(arrays, axis=along)
    out = lax.all_to_all(both, axis, split_axis=split_dim, concat_axis=concat_dim, tiled=True)
    return tuple(jnp.split(out, [sum(widths[:k]) for k in range(1, len(widths))], axis=along))


def over_axes(value, axes):
    return functools.reduce(lax.psum, axes, value)


def centred_conv(values, tap_weights):
    sample_window = values.shape[0]
    reach_side = (tap_weights.shape[0] - 1) // 2
    padded = jnp.pad(values, ((reach_side, reach_side), (0, 0)))
    summed = jnp.zeros_like(values)
    for offset in range(tap_weights.shape[0]):
        summed = summed + tap_weights[offset][None, :] * padded[offset : offset + sample_window]
    return summed


def one_channel_scan(
    source_unfiltered,
    writer_unfiltered,
    reader_unfiltered,
    delta_raw,
    extra_logdrop,
    source_filter_coefs,
    writer_filter_coefs,
    reader_filter_coefs,
    delta_offset,
    fading_exponents,
    direct_factor,
):
    inputs = jax.nn.silu(centred_conv(source_unfiltered, source_filter_coefs))
    keys_b = jax.nn.silu(centred_conv(writer_unfiltered, writer_filter_coefs))
    reads_c = jax.nn.silu(centred_conv(reader_unfiltered, reader_filter_coefs))
    smooth_delta = jax.nn.softplus(delta_raw + delta_offset)
    channel_fading = smooth_delta * jnp.exp(fading_exponents) + extra_logdrop
    cumulative = jnp.cumsum(channel_fading)
    sample_window = source_unfiltered.shape[0]
    blocks = sample_window // BLOCK
    driven = (inputs * smooth_delta[:, None]).reshape(blocks, BLOCK, -1)
    keyed = keys_b.reshape(blocks, BLOCK, -1)
    reading = reads_c.reshape(blocks, BLOCK, -1)
    levels = cumulative.reshape(blocks, BLOCK)
    within = jnp.exp(-jnp.abs(levels[:, :, None] - levels[:, None, :]))
    scores = jnp.einsum("ktn,ksn->kts", reading, keyed, precision=highest) * within
    output = jnp.einsum("kts,ksp->ktp", scores, driven, precision=highest)
    block_ends = levels[:, -1]
    block_starts = levels[:, 0]
    block_order = jnp.arange(blocks, dtype=jnp.int32)
    prev_end = jnp.concatenate([cumulative[:1], block_ends[:-1]])
    next_start = jnp.concatenate([block_starts[1:], cumulative[-1:]])
    weight_fwd = jnp.exp(levels - block_ends[:, None])
    state_fwd = jnp.einsum(
        "ksn,ksp->knp", keyed * weight_fwd[:, :, None], driven, precision=highest
    )
    mask_fwd = (block_order[None, :] < block_order[:, None]).astype(cumulative.dtype)
    link_fwd = jnp.exp(-jnp.abs(prev_end[:, None] - block_ends[None, :])) * mask_fwd
    carry_fwd = jnp.einsum("kj,jnp->knp", link_fwd, state_fwd, precision=highest)
    read_fwd = reading * jnp.exp(prev_end[:, None] - levels)[:, :, None]
    weight_bwd = jnp.exp(block_starts[:, None] - levels)
    state_bwd = jnp.einsum(
        "ksn,ksp->knp", keyed * weight_bwd[:, :, None], driven, precision=highest
    )
    mask_bwd = (block_order[None, :] > block_order[:, None]).astype(cumulative.dtype)
    link_bwd = jnp.exp(-jnp.abs(next_start[:, None] - block_starts[None, :])) * mask_bwd
    carry_bwd = jnp.einsum("kj,jnp->knp", link_bwd, state_bwd, precision=highest)
    read_bwd = reading * jnp.exp(levels - next_start[:, None])[:, :, None]
    output = output + jnp.einsum("ktn,knp->ktp", read_fwd, carry_fwd, precision=highest)
    output = output + jnp.einsum("ktn,knp->ktp", read_bwd, carry_bwd, precision=highest)
    return output.reshape(sample_window, -1) + direct_factor * inputs


def channelwise_derivs(
    source_unfiltered,
    writer_unfiltered,
    reader_unfiltered,
    delta_raw,
    extra_logdrop,
    source_filter_coefs,
    writer_filter_coefs,
    reader_filter_coefs,
    delta_offset,
    fading_exponents,
    direct_factor,
    result_adjoint,
):

    def forward(source_filtered, writer_filtered, reader_filtered, delta_argument):
        return one_channel_scan(
            source_filtered,
            writer_filtered,
            reader_filtered,
            delta_argument,
            extra_logdrop,
            source_filter_coefs,
            writer_filter_coefs,
            reader_filter_coefs,
            delta_offset,
            fading_exponents,
            direct_factor,
        )

    primal, pullback = jax.vjp(
        forward,
        source_unfiltered.astype(jnp.float32),
        writer_unfiltered.astype(jnp.float32),
        reader_unfiltered.astype(jnp.float32),
        delta_raw.astype(jnp.float32),
    )
    source_derivative, writer_derivative, reader_derivative, delta_derivative = pullback(
        result_adjoint.astype(jnp.float32)
    )
    return (
        source_derivative.astype(jnp.bfloat16),
        writer_derivative.astype(jnp.bfloat16),
        reader_derivative.astype(jnp.bfloat16),
        delta_derivative.astype(jnp.bfloat16),
    )


def gated_norm(values, gating, rescale_factor):
    mixed = values * jax.nn.silu(gating)
    grouped = mixed.reshape(mixed.shape[0], NORM_GROUPS, -1)
    scaled = grouped * lax.rsqrt(jnp.mean(grouped * grouped, axis=-1, keepdims=True) + EPSILON)
    return scaled.reshape(mixed.shape) * rescale_factor


def norm_backward(saved_result, switch_raw_signal, final_adjoint, rescale_factor):
    primal, pullback = jax.vjp(
        lambda values, gating: gated_norm(values, gating, rescale_factor),
        saved_result.astype(jnp.float32),
        switch_raw_signal.astype(jnp.float32),
    )
    d_values, d_gates = pullback(final_adjoint.astype(jnp.float32))
    return (d_values.astype(jnp.bfloat16), d_gates.astype(jnp.bfloat16))


def spread_heads(columns, tokens):
    grouped = columns.reshape(tokens, GROUPS, 1, STATE)
    copied = jnp.broadcast_to(grouped, (tokens, GROUPS, HEADS // GROUPS, STATE))
    return copied.reshape(1, tokens, HEADS * STATE)


def heads_first(values, window, local_channels, width):
    return jnp.transpose(values.reshape(window, local_channels, width), (1, 0, 2))


def local(
    layer_activity,
    writer_matrix,
    reader_matrix,
    source_unfiltered,
    switch_raw_signal,
    saved_result,
    final_adjoint,
    delta_raw,
    extra_logdrop,
    source_filter_coefs,
    writer_filter_coefs,
    reader_filter_coefs,
    delta_offset,
    fading_exponents,
    direct_factor,
    rescale_factor,
):
    tokens = layer_activity.shape[1]
    width_in = layer_activity.shape[2]
    latent_dimension = GROUPS * STATE
    local_channels = delta_offset.shape[0]
    per_group = HEADS // GROUPS
    weights = gathered_copies(jnp.concatenate([writer_matrix, reader_matrix], axis=1), "dp", 0)
    token_rows = layer_activity.reshape(tokens, width_in)
    projected = jnp.dot(token_rows, weights, preferred_element_type=jnp.float32).astype(
        jnp.bfloat16
    )
    result_adjoint, d_gate = norm_backward(
        saved_result.reshape(tokens, INNER),
        switch_raw_signal.reshape(tokens, INNER),
        final_adjoint.reshape(tokens, INNER),
        rescale_factor,
    )
    copies_b = spread_heads(projected[:, :latent_dimension], tokens)
    copies_c = spread_heads(projected[:, latent_dimension:], tokens)
    heads_x, heads_b, heads_c, heads_dt, heads_dy = (
        lax.all_to_all(source_unfiltered, SP, split_axis=2, concat_axis=1, tiled=True),
        *in_one_piece((copies_b, copies_c), SP, 2, 1, 0),
        lax.all_to_all(delta_raw, SP, split_axis=2, concat_axis=1, tiled=True),
        lax.all_to_all(
            result_adjoint.reshape(1, tokens, INNER), SP, split_axis=2, concat_axis=1, tiled=True
        ),
    )
    window = heads_x.shape[1]
    first_head = lax.axis_index(SP) * local_channels
    head_ids = first_head + jnp.arange(local_channels, dtype=jnp.int32)
    chooser = (
        head_ids[:, None] // per_group == jnp.arange(GROUPS, dtype=jnp.int32)[None, :]
    ).astype(jnp.float32)
    writer_filter_fn = jnp.einsum(
        "kgn,hg->hkn",
        writer_filter_coefs.reshape(CONV_K, GROUPS, STATE),
        chooser,
        precision=highest,
    )
    reader_filter_fn = jnp.einsum(
        "kgn,hg->hkn",
        reader_filter_coefs.reshape(CONV_K, GROUPS, STATE),
        chooser,
        precision=highest,
    )
    source_filter_fn = jnp.transpose(
        source_filter_coefs.reshape(CONV_K, local_channels, HEAD_DIM), (1, 0, 2)
    )
    per_head = jax.vmap(channelwise_derivs)
    source_derivative, writer_derivative, reader_derivative, delta_derivative = per_head(
        heads_first(heads_x, window, local_channels, HEAD_DIM),
        heads_first(heads_b, window, local_channels, STATE),
        heads_first(heads_c, window, local_channels, STATE),
        heads_dt.reshape(window, local_channels).T,
        extra_logdrop.reshape(window, local_channels).T,
        source_filter_fn,
        writer_filter_fn,
        reader_filter_fn,
        delta_offset,
        fading_exponents,
        direct_factor,
        heads_first(heads_dy, window, local_channels, HEAD_DIM),
    )
    back_x, back_b, back_c, back_dt = (
        lax.all_to_all(
            jnp.transpose(source_derivative, (1, 0, 2)).reshape(
                1, window, local_channels * HEAD_DIM
            ),
            SP,
            split_axis=1,
            concat_axis=2,
            tiled=True,
        ),
        *in_one_piece(
            (
                jnp.transpose(writer_derivative, (1, 0, 2)).reshape(
                    1, window, local_channels * STATE
                ),
                jnp.transpose(reader_derivative, (1, 0, 2)).reshape(
                    1, window, local_channels * STATE
                ),
            ),
            SP,
            1,
            2,
            0,
        ),
        lax.all_to_all(
            delta_derivative.T.reshape(1, window, local_channels),
            SP,
            split_axis=1,
            concat_axis=2,
            tiled=True,
        ),
    )
    summed_b = jnp.sum(back_b.reshape(tokens, GROUPS, per_group, STATE).astype(jnp.float32), axis=2)
    summed_c = jnp.sum(back_c.reshape(tokens, GROUPS, per_group, STATE).astype(jnp.float32), axis=2)
    gradients = jnp.concatenate(
        [
            summed_b.reshape(tokens, latent_dimension).astype(jnp.bfloat16),
            summed_c.reshape(tokens, latent_dimension).astype(jnp.bfloat16),
        ],
        axis=1,
    )
    d_hidden = jnp.einsum(
        "tc,dc->td", gradients, weights, preferred_element_type=jnp.float32
    ).astype(jnp.bfloat16)
    shard_sum = lax.psum_scatter(
        jnp.einsum("td,tc->dc", token_rows, gradients, preferred_element_type=jnp.float32).astype(
            jnp.bfloat16
        ),
        "dp",
        scatter_dimension=0,
        tiled=True,
    ).astype(jnp.float32)
    total_grad = over_axes(shard_sum, SP)
    return (
        d_hidden.reshape(1, tokens, width_in),
        back_x,
        d_gate.reshape(1, tokens, INNER),
        back_dt,
        total_grad[:, :latent_dimension],
        total_grad[:, latent_dimension:],
    )


def solution(mesh):
    split = Mesh(mesh.devices.reshape(8, 4, mesh.shape["dp"]), ("sp_0", "sp_1", "dp"))
    in_specs = (
        P("dp", SP, None),
        P("dp", None),
        P("dp", None),
        P("dp", SP, None),
        P("dp", SP, None),
        P("dp", SP, None),
        P("dp", SP, None),
        P("dp", SP, None),
        P("dp", None, SP),
        P(None, SP),
        P(),
        P(),
        P(SP),
        P(SP),
        P(SP),
        P(),
    )
    out_specs = (
        P("dp", SP, None),
        P("dp", SP, None),
        P("dp", SP, None),
        P("dp", SP, None),
        P("dp", None),
        P("dp", None),
    )
    return jax.shard_map(local, mesh=split, in_specs=in_specs, out_specs=out_specs, check_vma=False)
```

profile of v0, /device:TPU:8, one launch (start us, length us, event | category | flops | bytes accessed | tf_op | source)
XLA Modules:
  0.0 532.8 jit_solution(6923392075280680294)
XLA Ops:
  8.6 13.2 %all-to-all-start.3 = ((bf16[1,128,32]{1,0,2:T(2,128)(2,1)}), bf16[1,128,32]{1,0,2:T(2,128)(2,1)S(1)}, u32[]{:S(2)}, u32[]{:S(2)}) async-start(bf16[1,128,32]{1,0,2:T(2,128)(2,1)} %copy.304), calls=%async_computation.3 | async-start | bytes 32768 | tf_op jit(solution)/shard_map/all_to_all | solution.py:228
  21.7 2.4 copy.306
  24.6 11.5 %reduce.45 = bf16[2048,128]{1,0:T(8,128)(2,1)S(1)} reduce(bf16[2048,1,128]{2,1,0:T(2,128)(2,1)S(1)} %bitcast.411, bf16[]{:T(256)} %broadcast.893), dimensions={1}, to_apply=%bitcast.351.reduce_sub_computation | reduce | bytes 1048578
  37.1 9.8 %all-to-all-start.4 = ((bf16[32,2,4096]{2,1,0:T(2,128)(2,1)}), bf16[32,2,4096]{2,1,0:T(2,128)(2,1)S(1)}, u32[]{:S(2)}, u32[]{:S(2)}) async-start(bf16[32,2,4096]{2,1,0:T(2,128)(2,1)} %reshape.1930), calls=%async_computation.4 | async-start | bytes 1048576 | tf_op jit(solution)/shard_map/all_to_all | solution.py:226
  46.9 17.2 %all-to-all-done.4 = bf16[32,2,4096]{2,1,0:T(2,128)(2,1)S(1)} async-done(((bf16[32,2,4096]{2,1,0:T(2,128)(2,1)}), bf16[32,2,4096]{2,1,0:T(2,128)(2,1)S(1)}, u32[]{:S(2)}, u32[]{:S(2)}) %all-to-all-start.4) | async-done | bytes 524320 | tf_op jit(solution)/shard_map/all_to_all | solution.py:226
  64.1 1.6 broadcast_in_dim.20
  65.6 8.1 %all-to-all-start.1 = ((bf16[16,128,512]{2,1,0:T(8,128)(2,1)}), bf16[16,128,512]{2,1,0:T(8,128)(2,1)S(1)}, u32[]{:S(2)}, u32[]{:S(2)}) async-start(bf16[16,128,512]{2,1,0:T(8,128)(2,1)} %broadcast_in_dim.20), calls=%async_computation.1 | async-start | bytes 4194304 | tf_op jit(solution)/shard_map/all_to_all | solution.py:32
  78.3 2.4 mul.773
  81.8 2.4 broadcast_in_dim.19
  84.2 3.6 fusion.68
  87.8 3.6 copy.300
  91.4 12.6 %reduce.44 = bf16[2048,128]{1,0:T(8,128)(2,1)S(1)} reduce(bf16[2048,1,128]{2,1,0:T(2,128)(2,1)} %bitcast.412, bf16[]{:T(256)} %broadcast.893), dimensions={1}, to_apply=%bitcast.349.reduce_sub_computation | reduce | bytes 1048578
  104.9 15.9 %all-to-all-done.1 = bf16[16,128,512]{2,1,0:T(8,128)(2,1)S(1)} async-done(((bf16[16,128,512]{2,1,0:T(8,128)(2,1)}), bf16[16,128,512]{2,1,0:T(8,128)(2,1)S(1)}, u32[]{:S(2)}, u32[]{:S(2)}) %all-to-all-start.1) | async-done | bytes 2097184 | tf_op jit(solution)/shard_map/all_to_all | solution.py:32
  120.8 5.2 all-to-all-start
  127.4 18.1 %copy.301 = bf16[2,128,4096]{1,0,2:T(2,128)(2,1)} copy(bf16[2,128,4096]{1,2,0:T(8,128)(2,1)S(1)} %pad_maximum_fusion) | data formatting | bytes 4194304 | tf_op jit(solution)/shard_map/concatenate | solution.py:41
  146.4 10.0 %all-to-all-start.2 = ((bf16[2,128,4096]{1,0,2:T(2,128)(2,1)}), bf16[2,128,4096]{1,0,2:T(2,128)(2,1)}, u32[]{:S(2)}, u32[]{:S(2)}) async-start(bf16[2,128,4096]{1,0,2:T(2,128)(2,1)} %copy.301), calls=%async_computation.2 | async-start | bytes 4194304 | tf_op jit(solution)/shard_map/all_to_all | solution.py:42
  164.1 2.2 multiply_bitcast_fusion
  166.5 3.0 fusion.111
  169.5 37.1 %all-to-all-done.2 = bf16[2,128,4096]{1,0,2:T(2,128)(2,1)} async-done(((bf16[2,128,4096]{1,0,2:T(2,128)(2,1)}), bf16[2,128,4096]{1,0,2:T(2,128)(2,1)}, u32[]{:S(2)}, u32[]{:S(2)}) %all-to-all-start.2) | async-done | bytes 2097184 | tf_op jit(solution)/shard_map/all_to_all | solution.py:42
  206.6 1.9 copy.302
  208.4 2.7 slice_convert_fusion
  211.1 2.9 copy.318
  214.0 3.1 copy.303
  217.1 6.3 %fusion.30 = (f32[1,4096,128]{2,1,0:T(8,128)S(1)}, f32[1,4096,128]{2,1,0:T(8,128)S(1)}) fusion(f32[128]{0:T(128)S(1)} %get-tuple-element.126, f32[128]{0:T(128)S(1)} %get-tuple-element.127, f32[1,4096,128]{2,1,0:T(8,128)} %bitcast.407, f32[128]{0:T(128)S(1)} %get-tuple-element.128, f32[128]{0:T(128)S(1)} %get-tuple-element.129, f32[128]{0:T(128)S(1)} %get-tuple-element.125), kind=kLoop, calls=%fused_computation.60 | loop fusion | flops 6815744 | bytes 6294016 | tf_op jit(solution)/shard_map/vmap(jvp(jit(silu)))/mul | solution.py:75
  224.8 1.7 convolution_bitcast_fusion
  228.0 1.7 convolution_bitcast_fusion.1
  229.7 4.4 fusion.100
  234.1 1.7 fusion.24
  235.8 5.4 %fusion.23 = (f32[32,128]{1,0:T(8,128)S(1)}, f32[32,128]{1,0:T(8,128)S(1)}, f32[32,128,128]{1,2,0:T(8,128)S(1)}) fusion(f32[1,32,128,128]{3,2,1,0:T(8,128)S(1)} %bitcast.376, f32[32,128,128]{1,2,0:T(8,128)S(1)} %fusion.100, f32[32,128,64]{1,0,2:T(8,128)S(1)} %bitcast.390, f32[32,128,64]{1,0,2:T(8,128)S(1)} %convolution_bitcast_fusion.1), kind=kOutput, calls=%fused_computation.42 | convolution fusion | flops 404742144 | bytes 8421376 | tf_op jit(solution)/shard_map/vmap(transpose(jvp(ksn,ksp->knp)))/dot_general | solution.py:102
  241.4 2.6 fusion.38
  244.0 2.6 fusion.34
  246.6 2.0 fusion.94
  248.6 1.6 fusion.97
  250.2 1.7 fusion.74
  251.9 5.9 %fusion.21 = f32[1,32,128,128]{3,2,1,0:T(8,128)S(1)} fusion(f32[32,128,128]{1,2,0:T(8,128)S(1)} %fusion.100, f32[32,128,128]{1,2,0:T(8,128)S(1)} %get-tuple-element.130, f32[32,128,128]{2,1,0:T(8,128)S(1)} %bitcast.385, f32[32,128,128]{2,1,0:T(8,128)S(1)} %copy-done.4, f32[32,128]{1,0:T(8,128)S(1)} %get-tuple-element.81, ...), kind=kOutput, calls=%fused_computation.38 | convolution fusion | flops 809500672 | bytes 10534912 | tf_op jit(solution)/shard_map/vmap(transpose(jvp(ktn,ksn->kts)))/dot_general | solution.py:86
  257.8 2.7 multiply_reduce_fusion.1
  260.5 4.4 add_add_fusion
  269.8 18.1 %copy.325 = bf16[2,4096,128]{2,0,1:T(2,128)(2,1)} copy(bf16[2,4096,128]{2,1,0:T(8,128)(2,1)S(1)} %pad_maximum_fusion.1) | data formatting | bytes 4194304 | tf_op jit(solution)/shard_map/concatenate | solution.py:41
  287.9 6.1 %all-to-all-start.5 = ((bf16[2,4096,128]{2,0,1:T(2,128)(2,1)}), bf16[2,4096,128]{2,0,1:T(2,128)(2,1)}, u32[]{:S(2)}, u32[]{:S(2)}) async-start(bf16[2,4096,128]{2,0,1:T(2,128)(2,1)} %copy.325), calls=%async_computation.5 | async-start | bytes 4194304 | tf_op jit(solution)/shard_map/all_to_all | solution.py:42
  295.2 1.7 copy.333
  297.0 2.2 fusion.200
  300.0 2.2 fusion.201
  302.6 7.3 %fusion.199 = (f32[32,128]{1,0:T(8,128)S(1)}, f32[32,128]{1,0:T(8,128)S(1)}, f32[32,128,128]{2,1,0:T(8,128)S(1)}) fusion(f32[32,128,128]{2,1,0:T(8,128)} %fusion.111, f32[32,128,128]{2,1,0:T(8,128)} %bitcast.387, f32[32,128,128]{2,1,0:T(8,128)S(1)} %bitcast.380, f32[32,128]{1,0:T(8,128)S(1)} %get-tuple-element.81), kind=kOutput, calls=%fused_computation.320 | convolution fusion | flops 812113920 | bytes 8437760 | tf_op jit(solution)/shard_map/vmap(jvp(ktn,ksn->kts))/dot_general | solution.py:86
  310.1 2.8 fusion.11
  312.9 5.4 %fusion.32 = f32[32,64,128]{2,1,0:T(8,128)} fusion(f32[32,128,128]{2,1,0:T(8,128)S(1)} %bitcast.381, f32[32,128]{1,0:T(8,128)S(1)} %get-tuple-element.112, f32[32,128,64]{1,0,2:T(8,128)S(1)} %copy-done.16), kind=kOutput, calls=%fused_computation.64 | convolution fusion | flops 403177472 | bytes 4210688 | tf_op jit(solution)/shard_map/vmap(transpose(jvp(ksn,ksp->knp)))/dot_general | solution.py:94
  319.0 24.1 %all-to-all-done.5 = bf16[2,4096,128]{2,0,1:T(2,128)(2,1)} async-done(((bf16[2,4096,128]{2,0,1:T(2,128)(2,1)}), bf16[2,4096,128]{2,0,1:T(2,128)(2,1)}, u32[]{:S(2)}, u32[]{:S(2)}) %all-to-all-start.5) | async-done | bytes 2097184 | tf_op jit(solution)/shard_map/all_to_all | solution.py:42
  343.1 1.9 copy.326
  349.4 2.0 fusion
  351.5 4.4 copy.356
  355.9 6.2 %fusion.48 = f32[1,32,128,64]{2,3,1,0:T(8,128)S(1)} fusion(f32[32,64,128]{2,1,0:T(8,128)} %fusion.11, f32[32,64,128]{2,1,0:T(8,128)} %fusion.32, f32[32,128,128]{2,1,0:T(8,128)S(1)} %bitcast.382, f32[32,128]{1,0:T(8,128)S(1)} %get-tuple-element.69, f32[32,128,64]{1,0,2:T(8,128)} %copy-done.17), kind=kOutput, calls=%fused_computation.77 | convolution fusion | flops 403701760 | bytes 6307840 | tf_op jit(solution)/shard_map/vmap(transpose(jvp(ksn,ksp->knp)))/dot_general | solution.py:102
  362.1 1.6 copy.336
  365.4 4.6 broadcast_multiply_fusion.10
  370.2 3.9 copy.349
  374.1 6.2 %all-to-all-start.7 = ((bf16[1,4096,1]{2,0,1:T(2,128)(2,1)}), bf16[1,4096,1]{2,0,1:T(2,128)(2,1)}, u32[]{:S(2)}, u32[]{:S(2)}) async-start(bf16[1,4096,1]{2,0,1:T(2,128)(2,1)} %copy.349), calls=%async_computation.7 | async-start | bytes 4194304 | tf_op jit(solution)/shard_map/all_to_all | solution.py:293
  382.8 2.8 copy.339
  385.6 23.5 %reduce.46 = bf16[4096,64]{1,0:T(8,128)(2,1)} reduce(bf16[4096,1,64]{2,1,0:T(2,128)(2,1)S(1)} %bitcast.404, bf16[]{:T(256)} %broadcast.893), dimensions={1}, to_apply=%bitcast.353.reduce_sub_computation | reduce | bytes 1048578
  409.0 3.0 reshape.1932
  412.1 16.9 %all-to-all-done.7 = bf16[1,4096,1]{2,0,1:T(2,128)(2,1)} async-done(((bf16[1,4096,1]{2,0,1:T(2,128)(2,1)}), bf16[1,4096,1]{2,0,1:T(2,128)(2,1)}, u32[]{:S(2)}, u32[]{:S(2)}) %all-to-all-start.7) | async-done | bytes 8224 | tf_op jit(solution)/shard_map/all_to_all | solution.py:293
  429.0 5.9 %all-to-all-start.6 = ((bf16[32,2,4096]{2,1,0:T(2,128)(2,1)}), bf16[32,2,4096]{2,1,0:T(2,128)(2,1)S(1)}, u32[]{:S(2)}, u32[]{:S(2)}) async-start(bf16[32,2,4096]{2,1,0:T(2,128)(2,1)} %reshape.1932), calls=%async_computation.6 | async-start | bytes 1048576 | tf_op jit(solution)/shard_map/all_to_all | solution.py:270
  436.0 36.7 %all-reduce.28 = f32[128,512]{0,1:T(8,128)} all-reduce(bf16[128,512]{0,1:T(8,128)(2,1)S(1)} %copy.357), channel_id=1, replica_groups=mesh['sp_0'=8,'sp_1'=4,'dp'=16] {'sp_0'}, use_global_device_ids=true, to_apply=%region_24.25 | all-reduce | flops 65536 | bytes 393216 | tf_op jit(solution)/shard_map/psum | solution.py:47
  472.8 32.1 %reduce.37 = bf16[4096]{0:T(1024)(128)(2,1)} reduce(bf16[1,4096,1]{2,0,1:T(2,128)(2,1)} %all-to-all-done.7, bf16[]{:T(256)} %constant.148), dimensions={0,2}, to_apply=%all_to_all.92.reduce_sub_computation | reduce | bytes 16386 | tf_op jit(solution)/shard_map/all_to_all | solution.py:293
  506.2 2.3 copy.340
  510.2 1.6 fusion.1
  511.8 11.4 %all-reduce.27.cloned.1.call-done = f32[128,512]{0,1:T(8,128)} async-done(((f32[128,512]{0,1:T(8,128)}), f32[128,512]{0,1:T(8,128)}) %all-reduce.27.cloned.1.call-update) | async-done | bytes 262160 | tf_op jit(solution)/shard_map/psum | solution.py:47
  (168 shorter events, 43.6 us)
Async XLA Ops:
  7.2 118.8 %copy-start = (bf16[1,128,2048]{2,1,0:T(8,128)(2,1)S(1)}, bf16[1,128,2048]{2,1,0:T(8,128)(2,1)}, u32[]{:S(2)}) copy-start(bf16[1,128,2048]{2,1,0:T(8,128)(2,1)} %param.16) | copy-start | bytes 1572868
  8.6 28.5 %all-to-all-start.3 = ((bf16[1,128,32]{1,0,2:T(2,128)(2,1)}), bf16[1,128,32]{1,0,2:T(2,128)(2,1)S(1)}, u32[]{:S(2)}, u32[]{:S(2)}) async-start(bf16[1,128,32]{1,0,2:T(2,128)(2,1)} %copy.304), calls=%async_computation.3 | async-start | bytes 32768 | tf_op jit(solution)/shard_map/all_to_all | solution.py:228
  24.1 22.8 %copy-start.26 = (bf16[128,256]{1,0:T(8,128)(2,1)S(1)}, bf16[128,256]{1,0:T(8,128)(2,1)}, u32[]{:S(2)}) copy-start(bf16[128,256]{1,0:T(8,128)(2,1)} %param.18) | copy-start | bytes 196612
  24.1 22.8 %copy-start.27 = (bf16[128,256]{1,0:T(8,128)(2,1)S(1)}, bf16[128,256]{1,0:T(8,128)(2,1)}, u32[]{:S(2)}) copy-start(bf16[128,256]{1,0:T(8,128)(2,1)} %param.17) | copy-start | bytes 196612
  37.1 27.0 %all-to-all-start.4 = ((bf16[32,2,4096]{2,1,0:T(2,128)(2,1)}), bf16[32,2,4096]{2,1,0:T(2,128)(2,1)S(1)}, u32[]{:S(2)}, u32[]{:S(2)}) async-start(bf16[32,2,4096]{2,1,0:T(2,128)(2,1)} %reshape.1930), calls=%async_computation.4 | async-start | bytes 1048576 | tf_op jit(solution)/shard_map/all_to_all | solution.py:226
  64.1 1.6 copy-start.22
  65.6 8.1 %copy-start.28 = (f32[2048]{0:T(1024)S(1)}, f32[2048]{0:T(1024)}, u32[]{:S(2)}) copy-start(f32[2048]{0:T(1024)} %param.31) | copy-start | bytes 24580
  65.6 55.2 %all-to-all-start.1 = ((bf16[16,128,512]{2,1,0:T(8,128)(2,1)}), bf16[16,128,512]{2,1,0:T(8,128)(2,1)S(1)}, u32[]{:S(2)}, u32[]{:S(2)}) async-start(bf16[16,128,512]{2,1,0:T(8,128)(2,1)} %broadcast_in_dim.20), calls=%async_computation.1 | async-start | bytes 4194304 | tf_op jit(solution)/shard_map/all_to_all | solution.py:32
  73.7 2.4 copy-start.21
  120.8 6.2 %copy-start.5 = (bf16[16,128,512]{2,1,0:T(8,128)(2,1)}, bf16[16,128,512]{2,1,0:T(8,128)(2,1)S(1)}, u32[]{:S(2)}) copy-start(bf16[16,128,512]{2,1,0:T(8,128)(2,1)S(1)} %all-to-all-done.1) | copy-start | bytes 6291460
  120.8 24.8 %all-to-all-start = ((bf16[32,2,4096]{2,1,0:T(2,128)(2,1)}), bf16[32,2,4096]{2,1,0:T(2,128)(2,1)S(1)}, u32[]{:S(2)}, u32[]{:S(2)}) async-start(bf16[32,2,4096]{2,1,0:T(2,128)(2,1)} %reshape.1928), calls=%async_computation | async-start | bytes 1048576 | tf_op jit(solution)/shard_map/all_to_all | solution.py:229
  145.6 12.2 %copy-start.30 = (f32[5,256]{1,0:T(8,128)S(1)}, f32[5,256]{1,0:T(8,128)}, u32[]{:S(2)}) copy-start(f32[5,256]{1,0:T(8,128)} %param.26) | copy-start | bytes 15364
  145.6 12.2 %copy-start.31 = (f32[5,256]{1,0:T(8,128)S(1)}, f32[5,256]{1,0:T(8,128)}, u32[]{:S(2)}) copy-start(f32[5,256]{1,0:T(8,128)} %param.27) | copy-start | bytes 15364
  145.6 12.6 %copy-start.32 = (f32[5,64]{1,0:T(8,128)S(1)}, f32[5,64]{1,0:T(8,128)}, u32[]{:S(2)}) copy-start(f32[5,64]{1,0:T(8,128)} %param.25) | copy-start | bytes 3844
  145.6 12.6 %copy-start.29 = (f32[1,4096,1]{1,2,0:T(1,128)S(1)}, f32[1,4096,1]{1,2,0:T(1,128)}, u32[]{:S(2)}) copy-start(f32[1,4096,1]{1,2,0:T(1,128)} %param.24) | copy-start | bytes 49156
  145.6 15.9 %copy-start.23 = (bf16[32,2,4096]{2,1,0:T(2,128)(2,1)S(1)}, bf16[32,2,4096]{2,1,0:T(2,128)(2,1)}, u32[]{:S(2)}) copy-start(bf16[32,2,4096]{2,1,0:T(2,128)(2,1)} %copy-done.22) | copy-start | bytes 1572868
  145.6 0.8 copy-start.24
  146.4 60.2 %all-to-all-start.2 = ((bf16[2,128,4096]{1,0,2:T(2,128)(2,1)}), bf16[2,128,4096]{1,0,2:T(2,128)(2,1)}, u32[]{:S(2)}, u32[]{:S(2)}) async-start(bf16[2,128,4096]{1,0,2:T(2,128)(2,1)} %copy.301), calls=%async_computation.2 | async-start | bytes 4194304 | tf_op jit(solution)/shard_map/all_to_all | solution.py:42
  162.2 1.2 copy-start.25
  166.5 63.2 %copy-start.2 = (f32[8,8,32,128]{3,2,1,0:T(8,128)}, f32[8,8,32,128]{3,2,1,0:T(8,128)S(1)}, u32[]{:S(2)}) copy-start(f32[8,8,32,128]{3,2,1,0:T(8,128)S(1)} %copy.362) | copy-start | bytes 3145732
  223.4 34.4 %copy-start.1 = (f32[1,4096,128]{2,1,0:T(8,128)}, f32[1,4096,128]{2,1,0:T(8,128)S(1)}, u32[]{:S(2)}) copy-start(f32[1,4096,128]{2,1,0:T(8,128)S(1)} %get-tuple-element.76) | copy-start | bytes 6291460
  224.8 3.1 copy-start.7
  226.5 3.2 copy-start.15
  227.9 6.1 %copy-start.9 = (f32[32,128,64]{1,2,0:T(8,128)}, f32[32,128,64]{1,2,0:T(8,128)S(1)}, u32[]{:S(2)}) copy-start(f32[32,128,64]{1,2,0:T(8,128)S(1)} %fusion.51) | copy-start | bytes 3145732
  229.7 6.1 %copy-start.17 = (f32[32,128,64]{1,0,2:T(8,128)}, f32[32,128,64]{1,0,2:T(8,128)S(1)}, u32[]{:S(2)}) copy-start(f32[32,128,64]{1,0,2:T(8,128)S(1)} %convolution_bitcast_fusion.1) | copy-start | bytes 3145732
  229.7 4.4 copy-start.18
  234.1 1.7 copy-start.3
  244.0 4.6 copy-start.13
  246.6 3.6 copy-start.11
  250.1 1.7 copy-start.4
  287.9 55.3 %all-to-all-start.5 = ((bf16[2,4096,128]{2,0,1:T(2,128)(2,1)}), bf16[2,4096,128]{2,0,1:T(2,128)(2,1)}, u32[]{:S(2)}, u32[]{:S(2)}) async-start(bf16[2,4096,128]{2,0,1:T(2,128)(2,1)} %copy.325), calls=%async_computation.5 | async-start | bytes 4194304 | tf_op jit(solution)/shard_map/all_to_all | solution.py:42
  294.0 141.0 %reduce-scatter.4.cloned.1.call-start = ((), (), s32[]{:S(2)}) async-start(), calls=%async_computation.10 | async-start | bytes 2228224
  294.2 2.7 copy-start.10
  294.2 2.7 copy-start.14
  295.2 4.8 copy-start.8
  295.2 4.8 copy-start.12
  309.9 2.9 copy-start.16
  362.1 3.3 copy-start.19
  374.1 54.9 %all-to-all-start.7 = ((bf16[1,4096,1]{2,0,1:T(2,128)(2,1)}), bf16[1,4096,1]{2,0,1:T(2,128)(2,1)}, u32[]{:S(2)}, u32[]{:S(2)}) async-start(bf16[1,4096,1]{2,0,1:T(2,128)(2,1)} %copy.349), calls=%async_computation.7 | async-start | bytes 4194304 | tf_op jit(solution)/shard_map/all_to_all | solution.py:293
  380.3 1.2 copy-start.20
  429.0 75.9 %all-to-all-start.6 = ((bf16[32,2,4096]{2,1,0:T(2,128)(2,1)}), bf16[32,2,4096]{2,1,0:T(2,128)(2,1)S(1)}, u32[]{:S(2)}, u32[]{:S(2)}) async-start(bf16[32,2,4096]{2,1,0:T(2,128)(2,1)} %reshape.1932), calls=%async_computation.6 | async-start | bytes 1048576 | tf_op jit(solution)/shard_map/all_to_all | solution.py:270
  434.9 88.3 %all-reduce.27.cloned.1.call-start = ((), (), s32[]{:S(2)}) async-start(), calls=%async_computation.9 | async-start | bytes 524288 | tf_op jit(solution)/shard_map/psum | solution.py:47
  508.4 1.8 copy-start.6
Sparse Core Ops, SparseCore 0:
  356.0 56.0 reduce-scatter.3
  472.9 50.2 all-reduce.26
where the time goes:
time: 539 us; the launch traced here: 533 us
  waiting for transfers between devices  123 us (23%)
  other arithmetic  116 us (22%)
  local copies, waits for them, and re-layouts  101 us (19%)
  matrix products  73.2 us (14%)
  starting transfers between devices  64.7 us (12%)
  blocking collectives  36.7 us (7%)
  between operations  17.5 us (3%)
    all_to_all x2, waiting for transfers between devices, in_one_piece(): lax.all_to_all(both, axis, split_axis=split_dim, concat_axis=concat_dim,...  61.2 us
    unnamed x4, other arithmetic  49.7 us
    psum x1, blocking collectives, over_axes(): return functools.reduce(lax.psum, axes, value)  36.7 us
    concatenate x2, local copies, waits for them, and re-layouts, in_one_piece(): both = jnp.concatenate(arrays, axis=along)  36.2 us
    all_to_all x1, other arithmetic, local(): lax.all_to_all(delta_derivative.T.reshape(1, window, local_channels), SP,...  32.1 us
    unnamed x86, local copies, waits for them, and re-layouts  24.2 us
    dot_general x3, matrix products, one_channel_scan(): jnp.einsum('ktn,ksn->kts', reading, keyed, precision=highest) * within  17.6 us
    all_to_all x1, waiting for transfers between devices, local(): lax.all_to_all(source_unfiltered, SP, split_axis=2, concat_axis=1, tiled=...  17.2 us
  transfers between devices with their start and end apart: 10, of which 6 were waited for; matrix products, arithmetic and copies ran while one was open for 36% of the time, Pallas kernels for 0%

commit v1 on v0

v1 whole, which is shorter than its diff:
```python
import functools

import jax
import jax.numpy as jnp
from jax import lax
from jax.experimental import pallas as pl
from jax.experimental.pallas import tpu as pltpu
from jax.sharding import Mesh
from jax.sharding import PartitionSpec as P

HEADS = 32
HEAD_DIM = 64
STATE = 128
GROUPS = 2
NORM_GROUPS = 8
CONV_K = 5
BLOCK = 128
INNER = 2048
NZ, NX, NY, NC = 8, 4, 8, 2
LH = HEADS // NX
LW = LH * HEAD_DIM
CHUNK = NX * BLOCK
EDGE = 16
EPSILON = 1e-06
VMEM_LIMIT = 60 * 1024 * 1024

f32 = jnp.float32
bf16 = jnp.bfloat16
highest = lax.Precision.HIGHEST
MESH = pl.DeviceIdType.MESH
DMA = pltpu.SemaphoreType.DMA


def vmem():
    return pl.BlockSpec(memory_space=pltpu.VMEM)


def remote(src, dst, send, recv, device):
    return pltpu.make_async_remote_copy(
        src_ref=src, dst_ref=dst, send_sem=send, recv_sem=recv, device_id=device, device_id_type=MESH
    )


def greet(barrier, device):
    pl.semaphore_signal(barrier, inc=1, device_id=device, device_id_type=MESH)


def columns(start, size):
    return pl.ds(pl.multiple_of(start * size, size), size)


def norm_kernel(saved_ref, switch_ref, final_ref, gain_ref, dy_ref, dgate_ref):
    width = INNER // NORM_GROUPS
    for group in range(NORM_GROUPS):
        cols = slice(group * width, (group + 1) * width)
        saved = saved_ref[:, cols].astype(f32)
        switch = switch_ref[:, cols].astype(f32)
        final = final_ref[:, cols].astype(f32)
        gate = 1.0 / (1.0 + jnp.exp(-switch))
        act = switch * gate
        mixed = saved * act
        scale = lax.rsqrt(jnp.mean(mixed * mixed, axis=-1, keepdims=True) + EPSILON)
        d_normed = final * gain_ref[:, cols]
        inner = jnp.mean(d_normed * mixed, axis=-1, keepdims=True)
        d_mixed = d_normed * scale - mixed * (scale * scale * scale * inner)
        dy_ref[:, cols] = (d_mixed * act).astype(bf16)
        slope = gate * (1.0 + switch * (1.0 - gate))
        dgate_ref[:, cols] = (d_mixed * saved * slope).astype(bf16)


def norm_backward(saved, switch, final, gain):
    out = jax.ShapeDtypeStruct(saved.shape, bf16)
    return pl.pallas_call(
        norm_kernel,
        out_shape=(out, out),
        in_specs=[vmem()] * 4,
        out_specs=(vmem(), vmem()),
        compiler_params=pltpu.CompilerParams(vmem_limit_bytes=VMEM_LIMIT),
        name="norm_backward",
    )(saved, switch, final, gain)


def exchange_in_kernel(
    w_ref, x_ref, dy_ref, dt_ref, msg_ref,
    wf_ref, xh_ref, dyh_ref, dth_ref, prm_ref, xp_ref, xn_ref,
    own_sem, xs, xr, ys, yr, ts, tr, ms, mr, hs, hr, rs, rr, ls, lr, ps, pr,
):
    z, x, y, c = (lax.axis_index(name) for name in ("z", "x", "y", "c"))
    half = BLOCK // 2
    up, down = lax.rem(z + 1, NZ), lax.rem(z + NZ - 1, NZ)
    right, left = lax.rem(y + 1, NY), lax.rem(y + NY - 1, NY)
    other = 1 - c
    head = z * NX + x
    dest = z // 2
    slot = lax.rem(head, LH)
    mine = dest == x

    barrier = pltpu.get_barrier_semaphore()
    for d in range(1, NX):
        greet(barrier, {"x": lax.rem(x + d, NX)})
    greet(barrier, {"z": up})
    greet(barrier, {"z": down})
    greet(barrier, {"y": right})
    greet(barrier, {"y": left})
    greet(barrier, {"c": other})
    for i in range(LH):
        sz, sx = 2 * x + i // NX, i % NX

        @pl.when(jnp.logical_not(jnp.logical_and(sz == z, sx == x)))
        def _():
            greet(barrier, {"z": sz, "x": sx})

    pl.semaphore_wait(barrier, NX - 1 + 5 + NZ - mine.astype(jnp.int32))

    def rows(h):
        return pl.ds(h * half, half)

    def ring_right(s, h):
        block = lax.rem(y - s + NY, NY) * NC + c
        src = w_ref.at[rows(h)] if s == 0 else wf_ref.at[block, rows(h)]
        return remote(src, wf_ref.at[block, rows(h)], rs.at[s, h], rr.at[s, h], {"y": right})

    def ring_left(s, h):
        block = lax.rem(y + s, NY) * NC + c
        src = w_ref.at[rows(h)] if s == 0 else wf_ref.at[block, rows(h)]
        return remote(src, wf_ref.at[block, rows(h)], ls.at[s, h], lr.at[s, h], {"y": left})

    def across(n, h):
        offset = 0 if n == 0 else (-n if n < 5 else n - 4)
        block = lax.rem(y + offset + NY, NY) * NC + c
        src = w_ref.at[rows(h)] if n == 0 else wf_ref.at[block, rows(h)]
        return remote(src, wf_ref.at[block, rows(h)], ps.at[n, h], pr.at[n, h], {"c": other})

    for h in range(2):
        ring_right(0, h).start()
        ring_left(0, h).start()

    own = [
        pltpu.make_async_copy(w_ref, wf_ref.at[y * NC + c], own_sem.at[0]),
        pltpu.make_async_copy(x_ref.at[:, columns(x, LW)], xh_ref.at[x], own_sem.at[1]),
        pltpu.make_async_copy(dy_ref.at[:, columns(x, LW)], dyh_ref.at[x], own_sem.at[2]),
        pltpu.make_async_copy(dt_ref.at[columns(x, LH)], dth_ref.at[x], own_sem.at[3]),
    ]
    for copy in own:
        copy.start()

    def to_x(d):
        peer = lax.rem(x + d, NX)
        device = {"x": peer}
        return (
            remote(x_ref.at[:, columns(peer, LW)], xh_ref.at[x], xs.at[d - 1], xr.at[d - 1], device),
            remote(dt_ref.at[columns(peer, LH)], dth_ref.at[x], ts.at[d - 1], tr.at[d - 1], device),
            remote(dy_ref.at[:, columns(peer, LW)], dyh_ref.at[x], ys.at[d - 1], yr.at[d - 1], device),
        )

    for d in range(1, NX):
        for copy in to_x(d):
            copy.start()

    def message(i):
        return remote(
            msg_ref.at[i], prm_ref.at[slot], ms.at[i], mr.at[slot], {"z": jnp.int32(i), "x": dest}
        )

    keep = pltpu.make_async_copy(msg_ref.at[z], prm_ref.at[slot], own_sem.at[4])
    for i in range(NZ):

        @pl.when(jnp.logical_not(jnp.logical_and(mine, z == i)))
        def _():
            message(i).start()

    @pl.when(mine)
    def _():
        keep.start()

    for h in range(2):
        across(0, h).start()

    for d in range(1, NX):
        to_x(d)[0].wait_recv()
    own[1].wait()
    edge_up = remote(xh_ref.at[NX - 1, pl.ds(BLOCK - EDGE, EDGE)], xp_ref, hs.at[0], hr.at[0], {"z": up})
    edge_down = remote(xh_ref.at[0, pl.ds(0, EDGE)], xn_ref, hs.at[1], hr.at[1], {"z": down})
    edge_up.start()
    edge_down.start()

    for s in range(4):
        for h in range(2):
            ring_right(s, h).wait_recv()
            if s < 3:
                ring_right(s + 1, h).start()
            across(1 + s, h).start()
            if s < 3:
                ring_left(s, h).wait_recv()
                if s < 2:
                    ring_left(s + 1, h).start()
                across(5 + s, h).start()

    for d in range(1, NX):
        copies = to_x(d)
        copies[0].wait_send()
        copies[1].wait()
        copies[2].wait()
    edge_up.wait()
    edge_down.wait()
    for i in range(LH):
        sz, sx = 2 * x + i // NX, i % NX

        @pl.when(jnp.logical_not(jnp.logical_and(sz == z, sx == x)))
        def _():
            remote(msg_ref.at[i], prm_ref.at[i], ms.at[i], mr.at[i], {"z": sz, "x": sx}).wait_recv()

    for i in range(NZ):

        @pl.when(jnp.logical_not(jnp.logical_and(mine, z == i)))
        def _():
            message(i).wait_send()

    @pl.when(mine)
    def _():
        keep.wait()

    for n in (0, 2, 3):
        own[n].wait()
    for h in range(2):
        for s in range(4):
            ring_right(s, h).wait_send()
        for s in range(3):
            ring_left(s, h).wait_send()
        for n in range(8):
            across(n, h).wait()


def exchange_in(w, x, dy, dt, msg):
    shapes = (
        jax.ShapeDtypeStruct((NY * NC, BLOCK, 2 * GROUPS * STATE), bf16),
        jax.ShapeDtypeStruct((NX, BLOCK, LW), bf16),
        jax.ShapeDtypeStruct((NX, BLOCK, LW), bf16),
        jax.ShapeDtypeStruct((NX, LH, BLOCK), f32),
        jax.ShapeDtypeStruct((LH, 16, BLOCK), f32),
        jax.ShapeDtypeStruct((EDGE, LW), bf16),
        jax.ShapeDtypeStruct((EDGE, LW), bf16),
    )
    return pl.pallas_call(
        exchange_in_kernel,
        out_shape=shapes,
        in_specs=[vmem()] * 5,
        out_specs=tuple(vmem() for _ in shapes),
        scratch_shapes=[
            DMA((5,)), DMA((3,)), DMA((3,)), DMA((3,)), DMA((3,)), DMA((3,)), DMA((3,)),
            DMA((8,)), DMA((8,)), DMA((2,)), DMA((2,)),
            DMA((4, 2)), DMA((4, 2)), DMA((3, 2)), DMA((3, 2)), DMA((8, 2)), DMA((8, 2)),
        ],
        compiler_params=pltpu.CompilerParams(
            collective_id=0, has_side_effects=True, vmem_limit_bytes=VMEM_LIMIT
        ),
        name="exchange_in",
    )(w, x, dy, dt, msg)


def maps_in_kernel(bc_ref, out_ref, prev_ref, next_ref, own_sem, send, recv, hs, hr):
    z, x = lax.axis_index("z"), lax.axis_index("x")
    up, down = lax.rem(z + 1, NZ), lax.rem(z + NZ - 1, NZ)
    barrier = pltpu.get_barrier_semaphore()
    for d in range(1, NX):
        greet(barrier, {"x": lax.rem(x + d, NX)})
    greet(barrier, {"z": up})
    greet(barrier, {"z": down})
    pl.semaphore_wait(barrier, NX + 1)

    def to_x(d):
        peer = lax.rem(x + d, NX)
        return remote(
            bc_ref.at[:, columns(peer // 2, 2 * STATE)], out_ref.at[x], send.at[d - 1], recv.at[d - 1], {"x": peer}
        )

    for d in range(1, NX):
        to_x(d).start()
    own = pltpu.make_async_copy(bc_ref.at[:, columns(x // 2, 2 * STATE)], out_ref.at[x], own_sem.at[0])
    own.start()
    own.wait()
    for d in range(1, NX):
        to_x(d).wait_recv()
    edge_up = remote(out_ref.at[NX - 1, pl.ds(BLOCK - EDGE, EDGE)], prev_ref, hs.at[0], hr.at[0], {"z": up})
    edge_down = remote(out_ref.at[0, pl.ds(0, EDGE)], next_ref, hs.at[1], hr.at[1], {"z": down})
    edge_up.start()
    edge_down.start()
    for d in range(1, NX):
        to_x(d).wait_send()
    edge_up.wait()
    edge_down.wait()


def maps_in(bc):
    shapes = (
        jax.ShapeDtypeStruct((NX, BLOCK, 2 * STATE), bf16),
        jax.ShapeDtypeStruct((EDGE, 2 * STATE), bf16),
        jax.ShapeDtypeStruct((EDGE, 2 * STATE), bf16),
    )
    return pl.pallas_call(
        maps_in_kernel,
        out_shape=shapes,
        in_specs=[vmem()],
        out_specs=tuple(vmem() for _ in shapes),
        scratch_shapes=[DMA((1,)), DMA((3,)), DMA((3,)), DMA((2,)), DMA((2,))],
        compiler_params=pltpu.CompilerParams(
            collective_id=1, has_side_effects=True, vmem_limit_bytes=VMEM_LIMIT
        ),
        name="maps_in",
    )(bc)


def scan_kernel(sr_ref, sl_ref, decay_ref, cr_ref, cl_ref, outr, outl, rs, rr, ls, lr):
    z = lax.axis_index("z")
    up, down = lax.rem(z + 1, NZ), lax.rem(z + NZ - 1, NZ)
    first, last = z == 0, z == NZ - 1
    barrier = pltpu.get_barrier_semaphore()

    @pl.when(jnp.logical_not(first))
    def _():
        greet(barrier, {"z": down})

    @pl.when(jnp.logical_not(last))
    def _():
        greet(barrier, {"z": up})

    @pl.when(first)
    def _():
        cr_ref[...] = jnp.zeros_like(cr_ref)

    @pl.when(last)
    def _():
        cl_ref[...] = jnp.zeros_like(cl_ref)

    pl.semaphore_wait(barrier, 2 - first.astype(jnp.int32) - last.astype(jnp.int32))
    count = 2 * LW // 128

    def piece(n):
        return n // (LW // 128), slice(None), columns(lax.rem(n, LW // 128), 128)

    def going_up(n):
        return remote(outr.at[piece(n)], cr_ref.at[piece(n)], rs.at[n], rr.at[n], {"z": up})

    def going_down(n):
        return remote(outl.at[piece(n)], cl_ref.at[piece(n)], ls.at[n], lr.at[n], {"z": down})

    def step(t, carry):
        n = t - z

        @pl.when(jnp.logical_and(n >= 0, n < count))
        def _():
            @pl.when(jnp.logical_not(first))
            def _():
                going_up(n).wait_recv()

            @pl.when(jnp.logical_not(last))
            def _():
                at = piece(n)
                outr[at] = (cr_ref[at].astype(f32) * decay_ref[0:1, at[2]] + sr_ref[at]).astype(bf16)
                going_up(n).start()

        m = t - (NZ - 1 - z)

        @pl.when(jnp.logical_and(m >= 0, m < count))
        def _():
            @pl.when(jnp.logical_not(last))
            def _():
                going_down(m).wait_recv()

            @pl.when(jnp.logical_not(first))
            def _():
                at = piece(m)
                outl[at] = (cl_ref[at].astype(f32) * decay_ref[0:1, at[2]] + sl_ref[at]).astype(bf16)
                going_down(m).start()

        return carry

    lax.fori_loop(0, NZ - 1 + count, step, 0)
    for n in range(count):

        @pl.when(jnp.logical_not(last))
        def _():
            going_up(jnp.int32(n)).wait_send()

        @pl.when(jnp.logical_not(first))
        def _():
            going_down(jnp.int32(n)).wait_send()


def scan_states(sr, sl, decay):
    out = jax.ShapeDtypeStruct((2, STATE, LW), bf16)
    return pl.pallas_call(
        scan_kernel,
        out_shape=(out, out),
        in_specs=[vmem()] * 3,
        out_specs=(vmem(), vmem()),
        scratch_shapes=[
            pltpu.VMEM((2, STATE, LW), bf16),
            pltpu.VMEM((2, STATE, LW), bf16),
            DMA((8,)), DMA((8,)), DMA((8,)), DMA((8,)),
        ],
        compiler_params=pltpu.CompilerParams(
            collective_id=2, has_side_effects=True, vmem_limit_bytes=VMEM_LIMIT
        ),
        name="scan_states",
    )(sr, sl, decay)


def dot(a, b):
    return jnp.dot(a, b, preferred_element_type=f32)


def dot_nt(a, b):
    return lax.dot_general(a, b, (((1,), (1,)), ((), ())), preferred_element_type=f32)


def dot_tn(a, b):
    return lax.dot_general(a, b, (((0,), (0,)), ((), ())), preferred_element_type=f32)


def iota2(shape, dim):
    return lax.broadcasted_iota(jnp.int32, shape, dim)


def parts_of(value, count):
    out = []
    for _ in range(count):
        top = value.astype(bf16).astype(f32)
        out.append(top)
        value = value - top
    return out


def spreaders():
    r, cc = iota2((48, 3 * LW), 0), iota2((48, 3 * LW), 1)
    three = jnp.logical_and(r // 16 == cc // LW, lax.rem(r, 8) == lax.rem(cc, LW) // HEAD_DIM)
    r, cc = iota2((24, LH * BLOCK), 0), iota2((24, LH * BLOCK), 1)
    wide = lax.rem(r, 8) == cc // BLOCK
    r, cc = iota2((LH, 2 * LW), 0), iota2((LH, 2 * LW), 1)
    gather = lax.rem(cc, LW) // HEAD_DIM == r
    return three.astype(bf16), wide.astype(bf16), gather.astype(bf16)


def per_head_sum(gather_ref, value):
    return dot_nt(gather_ref[...], jnp.concatenate(parts_of(value, 2), axis=1).astype(bf16))


def silu_parts(pre):
    gate = 1.0 / (1.0 + jnp.exp(-pre))
    return pre * gate, gate * (1.0 + pre * (1.0 - gate))


def pair_row(prm_ref, row, j):
    lane = iota2((1, 128), 1)
    return jnp.where(lane < HEAD_DIM, prm_ref[row, 2 * j : 2 * j + 1, :], prm_ref[row, 2 * j + 1 : 2 * j + 2, :])


def fill_padded(pad_ref, body_ref, prev_ref, next_ref, z):
    pad_ref[pl.ds(0, EDGE)] = jnp.where(z == 0, 0.0, prev_ref[...].astype(f32))
    for k in range(NX):
        pad_ref[pl.ds(EDGE + k * BLOCK, BLOCK)] = body_ref[k].astype(f32)
    pad_ref[pl.ds(EDGE + CHUNK, EDGE)] = jnp.where(z == NZ - 1, 0.0, next_ref[...].astype(f32))


def maps_of(bcp_ref, taps_ref, rows, which):
    lanes = slice(which * STATE, (which + 1) * STATE)
    pre = jnp.zeros((rows.size, STATE), f32)
    for tap in range(CONV_K):
        pre = pre + taps_ref[tap : tap + 1, lanes] * bcp_ref[pl.ds(rows.start + EDGE - 2 + tap, rows.size), lanes]
    return silu_parts(pre)


def block_scalars(prm_ref, dth_ref, k, upper):
    raw = dth_ref[k] + prm_ref[9]
    dt = jax.nn.softplus(raw)
    rate = dt * jnp.exp(prm_ref[10]) + prm_ref[k]
    level = jnp.dot(rate, upper, precision=highest, preferred_element_type=f32)
    total = level[:, BLOCK - 1 : BLOCK]
    return raw, dt, level, jnp.exp(-level), jnp.exp(level - total)


def prepare(
    k, prm_ref, dth_ref, dyh_ref, bcp_ref, taps_ref, xpad_ref, three_ref,
    v16, pv16, qv16, pdy16, qdy16, b16, c16, gamma, u_ref, slope_ref, spread_ref, bs_ref, cs_ref, level_ref,
):
    row, col = iota2((BLOCK, BLOCK), 0), iota2((BLOCK, BLOCK), 1)
    upper = (row <= col).astype(f32)
    raw, dt, level, p, q = block_scalars(prm_ref, dth_ref, k, upper)
    stack = jnp.concatenate(parts_of(dt, 2) + parts_of(p, 2) + parts_of(q, 2), axis=0)
    spread = dot_tn(stack.astype(bf16), three_ref[...])
    rows = pl.ds(k * BLOCK, BLOCK)
    keys, key_slope = maps_of(bcp_ref, taps_ref, rows, 0)
    reads, read_slope = maps_of(bcp_ref, taps_ref, rows, 1)
    b16[rows], c16[rows] = keys.astype(bf16), reads.astype(bf16)
    if level_ref is not None:
        level_ref[k] = level
        spread_ref[rows] = spread
        bs_ref[rows], cs_ref[rows] = key_slope, read_slope
    gamma[k] = jnp.broadcast_to(spread[BLOCK - 1 : BLOCK, LW : 2 * LW], (8, LW))
    for j in range(LH // 2):
        lanes = slice(128 * j, 128 * (j + 1))
        pre = jnp.zeros((BLOCK, 128), f32)
        for tap in range(CONV_K):
            pre = pre + pair_row(prm_ref, 4 + tap, j) * xpad_ref[pl.ds(k * BLOCK + EDGE - 2 + tap, BLOCK), lanes]
        u, slope = silu_parts(pre)
        if u_ref is not None:
            u_ref[rows, lanes], slope_ref[rows, lanes] = u, slope
        pe = spread[:, LW + 128 * j : LW + 128 * (j + 1)]
        qe = spread[:, 2 * LW + 128 * j : 2 * LW + 128 * (j + 1)]
        v = u * spread[:, lanes]
        dy = dyh_ref[k, :, lanes].astype(f32)
        if v16 is not None:
            v16[rows, lanes] = v.astype(bf16)
        pv16[rows, lanes], qv16[rows, lanes] = (pe * v).astype(bf16), (qe * v).astype(bf16)
        pdy16[rows, lanes], qdy16[rows, lanes] = (pe * dy).astype(bf16), (qe * dy).astype(bf16)


def block_states(k, b16, c16, pv16, qv16, pdy16, qdy16):
    rows = pl.ds(k * BLOCK, BLOCK)
    b, c = b16[rows], c16[rows]
    return (
        dot_tn(b, qv16[rows]), dot_tn(c, qdy16[rows]),
        dot_tn(b, pv16[rows]), dot_tn(c, pdy16[rows]),
    )


def states_kernel(
    xh_ref, xp_ref, xn_ref, dyh_ref, bch_ref, bp_ref, bn_ref, dth_ref, prm_ref, taps_ref, three_ref,
    sr_ref, sl_ref, decay_ref,
    xpad, bcpad, pv16, qv16, pdy16, qdy16, b16, c16, gamma,
):
    z = lax.axis_index("z")
    fill_padded(xpad, xh_ref, xp_ref, xn_ref, z)
    fill_padded(bcpad, bch_ref, bp_ref, bn_ref, z)
    decay_ref[...] = jnp.ones_like(decay_ref)
    for k in range(NX):
        prepare(
            k, prm_ref, dth_ref, dyh_ref, bcpad, taps_ref, xpad, three_ref,
            None, pv16, qv16, pdy16, qdy16, b16, c16, gamma, None, None, None, None, None, None,
        )
        kvr, cdr, kvl, cdl = block_states(k, b16, c16, pv16, qv16, pdy16, qdy16)
        g = gamma[k, 0:1]
        if k == 0:
            sr_ref[0], sr_ref[1], sl_ref[0], sl_ref[1] = kvr, cdr, kvl, cdl
        else:
            before = decay_ref[0:1]
            sr_ref[0] = sr_ref[0] * g + kvr
            sr_ref[1] = sr_ref[1] * g + cdr
            sl_ref[0] = sl_ref[0] + before * kvl
            sl_ref[1] = sl_ref[1] + before * cdl
        decay_ref[...] = decay_ref[...] * gamma[k]


def chunk_states(xh, xp, xn, dyh, bch, bp, bn, dth, prm, taps, three):
    state = jax.ShapeDtypeStruct((2, STATE, LW), f32)
    wide16 = pltpu.VMEM((CHUNK, LW), bf16)
    return pl.pallas_call(
        states_kernel,
        out_shape=(state, state, jax.ShapeDtypeStruct((8, LW), f32)),
        in_specs=[vmem()] * 11,
        out_specs=(vmem(),) * 3,
        scratch_shapes=[
            pltpu.VMEM((CHUNK + 2 * EDGE, LW), f32),
            pltpu.VMEM((CHUNK + 2 * EDGE, 2 * STATE), f32),
            wide16, wide16, wide16, wide16,
            pltpu.VMEM((CHUNK, STATE), bf16),
            pltpu.VMEM((CHUNK, STATE), bf16),
            pltpu.VMEM((NX, 8, LW), f32),
        ],
        compiler_params=pltpu.CompilerParams(vmem_limit_bytes=VMEM_LIMIT),
        name="chunk_states",
    )(xh, xp, xn, dyh, bch, bp, bn, dth, prm, taps, three)


def unconvolved(pad_ref, start, size, lanes, tap_of):
    total = jnp.zeros((size, 128), f32)
    for tap in range(CONV_K):
        total = total + tap_of(tap) * pad_ref[pl.ds(start + 2 * EDGE + 2 - tap, size), lanes]
    return total


def gradients_kernel(
    xh_ref, xp_ref, xn_ref, dyh_ref, bch_ref, bp_ref, bn_ref, dth_ref, prm_ref, taps_ref,
    three_ref, wide_ref, gather_ref, cr_ref, cl_ref,
    dx_ref, dxp_ref, dxn_ref, dbc_ref, dbp_ref, dbn_ref, ddt_ref,
    xpad, bcpad, v16, pv16, qv16, pdy16, qdy16, b16, c16, gamma, u_scr, slope_scr, spread_scr,
    bs_scr, cs_scr, level_scr, right, left, dxpad, dbcpad, dl_scr, dvu_scr,
):
    z = lax.axis_index("z")
    fill_padded(xpad, xh_ref, xp_ref, xn_ref, z)
    fill_padded(bcpad, bch_ref, bp_ref, bn_ref, z)
    for pad in (dxpad, dbcpad):
        pad[pl.ds(0, 2 * EDGE)] = jnp.zeros((2 * EDGE, pad.shape[1]), f32)
        pad[pl.ds(2 * EDGE + CHUNK, 2 * EDGE)] = jnp.zeros((2 * EDGE, pad.shape[1]), f32)
    row, col = iota2((BLOCK, BLOCK), 0), iota2((BLOCK, BLOCK), 1)
    sign = (row > col).astype(f32) - (row < col).astype(f32)
    lower = (row >= col).astype(f32)
    lane = iota2((BLOCK, 128), 1)
    low_half = lane < HEAD_DIM
    head_row = iota2((8, BLOCK), 0)

    right[0, 0], right[0, 1] = cr_ref[0].astype(f32), cr_ref[1].astype(f32)
    left[NX - 1, 0], left[NX - 1, 1] = cl_ref[0].astype(f32), cl_ref[1].astype(f32)
    for k in range(NX):
        prepare(
            k, prm_ref, dth_ref, dyh_ref, bcpad, taps_ref, xpad, three_ref,
            v16, pv16, qv16, pdy16, qdy16, b16, c16, gamma, u_scr, slope_scr, spread_scr, bs_scr, cs_scr, level_scr,
        )
        kvr, cdr, kvl, cdl = block_states(k, b16, c16, pv16, qv16, pdy16, qdy16)
        g = gamma[k, 0:1]
        right[k + 1, 0] = right[k, 0] * g + kvr
        right[k + 1, 1] = right[k, 1] * g + cdr
        if k > 0:
            left[k - 1, 0], left[k - 1, 1] = kvl, cdl
    for k in range(NX - 2, -1, -1):
        g = gamma[k + 1, 0:1]
        left[k, 0] = left[k, 0] + g * left[k + 1, 0]
        left[k, 1] = left[k, 1] + g * left[k + 1, 1]

    def block(k, carry):
        rows = pl.ds(pl.multiple_of(k * BLOCK, BLOCK), BLOCK)
        b, c = b16[rows], c16[rows]
        grid = dot_nt(c, b)
        grid_t = dot_nt(b, c)
        signed = grid * sign
        level = level_scr[k]
        level_cols = dot_tn(jnp.concatenate(parts_of(level, 3), axis=0).astype(bf16), wide_ref[...])
        weights = jnp.zeros((BLOCK, BLOCK), f32)
        dl = jnp.zeros((8, BLOCK), f32)
        dc = jnp.zeros((BLOCK, STATE), f32)
        db = jnp.zeros((BLOCK, STATE), f32)
        dvu = jnp.zeros((8, BLOCK), f32)
        for j in range(LH // 2):
            lanes = slice(128 * j, 128 * (j + 1))
            vj = v16[rows, lanes]
            dyj = dyh_ref[k, :, lanes]
            halves = []
            for i in range(2):
                h = 2 * j + i
                near = jnp.exp(-jnp.abs(level_cols[:, 128 * h : 128 * (h + 1)] - level[h : h + 1, :]))
                keep = low_half if i == 0 else jnp.logical_not(low_half)
                shared = dot_nt(jnp.where(keep, dyj, jnp.zeros_like(dyj)), vj) * near
                weights = weights + shared
                crossing = (shared * signed).astype(bf16)
                pick = (head_row == h).astype(bf16)
                dl = dl + dot(pick, crossing) - dot_nt(pick, crossing)
                halves.append(dot((grid_t * near).astype(bf16), dyj))
            kvr, cdr = right[k, 0, :, lanes].astype(bf16), right[k, 1, :, lanes].astype(bf16)
            kvl, cdl = left[k, 0, :, lanes].astype(bf16), left[k, 1, :, lanes].astype(bf16)
            pe = spread_scr[rows, LW + 128 * j : LW + 128 * (j + 1)]
            qe = spread_scr[rows, 2 * LW + 128 * j : 2 * LW + 128 * (j + 1)]
            from_later, from_earlier = dot(b, cdl), dot(b, cdr)
            pv, qv, pdy, qdy = pv16[rows, lanes], qv16[rows, lanes], pdy16[rows, lanes], qdy16[rows, lanes]
            dv = jnp.where(low_half, halves[0], halves[1]) + qe * from_later + pe * from_earlier
            cross = (
                qv.astype(f32) * from_later - pv.astype(f32) * from_earlier
                + qdy.astype(f32) * dot(c, kvl) - pdy.astype(f32) * dot(c, kvr)
            )
            dc = dc + dot_nt(pdy, kvr) + dot_nt(qdy, kvl)
            db = db + dot_nt(qv, cdl) + dot_nt(pv, cdr)
            picks = jnp.concatenate([gather_ref[:, lanes]] * 2, axis=1)
            dl = dl + dot_nt(picks, jnp.concatenate(parts_of(cross, 2), axis=1).astype(bf16))
            u = u_scr[rows, lanes]
            dvu = dvu + dot_nt(picks, jnp.concatenate(parts_of(dv * u, 2), axis=1).astype(bf16))
            skip = pair_row(prm_ref, 11, j)
            du = dv * spread_scr[rows, lanes] + skip * dyj.astype(f32)
            dxpad[pl.ds(pl.multiple_of(2 * EDGE + k * BLOCK, EDGE), BLOCK), lanes] = du * slope_scr[rows, lanes]
        weights = weights.astype(bf16)
        dc = dc + dot(weights, b)
        db = db + dot_tn(weights, c)
        out_rows = pl.ds(pl.multiple_of(2 * EDGE + k * BLOCK, EDGE), BLOCK)
        dbcpad[out_rows, 0:STATE] = db * bs_scr[rows]
        dbcpad[out_rows, STATE : 2 * STATE] = dc * cs_scr[rows]
        dl_scr[k], dvu_scr[k] = dl, dvu
        return carry

    lax.fori_loop(0, NX, block, 0)

    met = right[NX, 0] * left[NX - 1, 1] + right[NX, 1] * left[NX - 1, 0]
    after = -jnp.sum(per_head_sum(gather_ref, met), axis=1, keepdims=True)
    for k in range(NX - 1, -1, -1):
        d_rate = jnp.dot(dl_scr[k], lower, precision=highest, preferred_element_type=f32) + after
        after = d_rate[:, 0:1]
        raw = dth_ref[k] + prm_ref[9]
        d_dt = d_rate * jnp.exp(prm_ref[10]) + dvu_scr[k]
        ddt_ref[k] = d_dt / (1.0 + jnp.exp(-raw))

    pieces = [(k * BLOCK, BLOCK) for k in range(NX)]
    for j in range(LH // 2):
        lanes = slice(128 * j, 128 * (j + 1))
        tap_of = lambda tap, j=j: pair_row(prm_ref, 4 + tap, j)
        for k, (start, size) in enumerate(pieces):
            dx_ref[k, :, lanes] = unconvolved(dxpad, start, size, lanes, tap_of).astype(bf16)
        before = unconvolved(dxpad, -EDGE, EDGE, lanes, tap_of)
        behind = unconvolved(dxpad, CHUNK, EDGE, lanes, tap_of)
        dxp_ref[:, lanes] = jnp.where(z == 0, 0.0, before).astype(bf16)
        dxn_ref[:, lanes] = jnp.where(z == NZ - 1, 0.0, behind).astype(bf16)
    for w in range(2):
        lanes = slice(STATE * w, STATE * (w + 1))
        tap_of = lambda tap, lanes=lanes: taps_ref[tap : tap + 1, lanes]
        for k, (start, size) in enumerate(pieces):
            dbc_ref[k, :, lanes] = unconvolved(dbcpad, start, size, lanes, tap_of).astype(bf16)
        before = unconvolved(dbcpad, -EDGE, EDGE, lanes, tap_of)
        behind = unconvolved(dbcpad, CHUNK, EDGE, lanes, tap_of)
        dbp_ref[:, lanes] = jnp.where(z == 0, 0.0, before).astype(bf16)
        dbn_ref[:, lanes] = jnp.where(z == NZ - 1, 0.0, behind).astype(bf16)


def chunk_gradients(xh, xp, xn, dyh, bch, bp, bn, dth, prm, taps, three, wide, gather, cr, cl):
    shapes = (
        jax.ShapeDtypeStruct((NX, BLOCK, LW), bf16),
        jax.ShapeDtypeStruct((EDGE, LW), bf16),
        jax.ShapeDtypeStruct((EDGE, LW), bf16),
        jax.ShapeDtypeStruct((NX, BLOCK, 2 * STATE), bf16),
        jax.ShapeDtypeStruct((EDGE, 2 * STATE), bf16),
        jax.ShapeDtypeStruct((EDGE, 2 * STATE), bf16),
        jax.ShapeDtypeStruct((NX, LH, BLOCK), f32),
    )
    wide16 = pltpu.VMEM((CHUNK, LW), bf16)
    return pl.pallas_call(
        gradients_kernel,
        out_shape=shapes,
        in_specs=[vmem()] * 15,
        out_specs=tuple(vmem() for _ in shapes),
        scratch_shapes=[
            pltpu.VMEM((CHUNK + 2 * EDGE, LW), f32),
            pltpu.VMEM((CHUNK + 2 * EDGE, 2 * STATE), f32),
            wide16, wide16, wide16, wide16, wide16,
            pltpu.VMEM((CHUNK, STATE), bf16),
            pltpu.VMEM((CHUNK, STATE), bf16),
            pltpu.VMEM((NX, 8, LW), f32),
            pltpu.VMEM((CHUNK, LW), f32),
            pltpu.VMEM((CHUNK, LW), f32),
            pltpu.VMEM((CHUNK, 3 * LW), f32),
            pltpu.VMEM((CHUNK, STATE), f32),
            pltpu.VMEM((CHUNK, STATE), f32),
            pltpu.VMEM((NX, 8, BLOCK), f32),
            pltpu.VMEM((NX + 1, 2, STATE, LW), f32),
            pltpu.VMEM((NX, 2, STATE, LW), f32),
            pltpu.VMEM((CHUNK + 4 * EDGE, LW), f32),
            pltpu.VMEM((CHUNK + 4 * EDGE, 2 * STATE), f32),
            pltpu.VMEM((NX, 8, BLOCK), f32),
            pltpu.VMEM((NX, 8, BLOCK), f32),
        ],
        compiler_params=pltpu.CompilerParams(vmem_limit_bytes=VMEM_LIMIT),
        name="chunk_gradients",
    )(xh, xp, xn, dyh, bch, bp, bn, dth, prm, taps, three, wide, gather, cr, cl)


def exchange_out_kernel(
    dx_ref, dxp_ref, dxn_ref, dbc_ref, dbp_ref, dbn_ref, ddt_ref,
    dxo_ref, exp_ref, exn_ref, bco_ref, ebp_ref, ebn_ref, dto_ref,
    own_sem, xs, xr, bs, br, ts, tr, es, er,
):
    z, x = lax.axis_index("z"), lax.axis_index("x")
    up, down = lax.rem(z + 1, NZ), lax.rem(z + NZ - 1, NZ)
    first, last = x == 0, x == NX - 1

    @pl.when(jnp.logical_not(first))
    def _():
        exp_ref[...] = jnp.zeros_like(exp_ref)
        ebp_ref[...] = jnp.zeros_like(ebp_ref)

    @pl.when(jnp.logical_not(last))
    def _():
        exn_ref[...] = jnp.zeros_like(exn_ref)
        ebn_ref[...] = jnp.zeros_like(ebn_ref)

    barrier = pltpu.get_barrier_semaphore()
    for d in range(1, NX):
        greet(barrier, {"x": lax.rem(x + d, NX)})

    @pl.when(first)
    def _():
        for n in range(NX):
            greet(barrier, {"z": down, "x": jnp.int32(n)})

    @pl.when(last)
    def _():
        for n in range(NX):
            greet(barrier, {"z": up, "x": jnp.int32(n)})

    pl.semaphore_wait(barrier, NX - 1 + 2)

    def to_x(d):
        peer = lax.rem(x + d, NX)
        device = {"x": peer}
        return (
            remote(dbc_ref.at[peer], bco_ref.at[x], bs.at[d - 1], br.at[d - 1], device),
            remote(ddt_ref.at[peer], dto_ref.at[x], ts.at[d - 1], tr.at[d - 1], device),
            remote(dx_ref.at[peer], dxo_ref.at[:, columns(x, LW)], xs.at[d - 1], xr.at[d - 1], device),
        )

    def edges(n):
        before, behind = {"z": down, "x": jnp.int32(NX - 1)}, {"z": up, "x": jnp.int32(0)}
        return (
            remote(dbp_ref, ebn_ref.at[n], es.at[0], er.at[0, n], before),
            remote(dxp_ref, exn_ref.at[:, columns(n, LW)], es.at[1], er.at[1, n], before),
            remote(dbn_ref, ebp_ref.at[n], es.at[2], er.at[2, n], behind),
            remote(dxn_ref, exp_ref.at[:, columns(n, LW)], es.at[3], er.at[3, n], behind),
        )

    for copy in edges(x):
        copy.start()
    for d in range(1, NX):
        for copy in to_x(d):
            copy.start()
    own = [
        pltpu.make_async_copy(dx_ref.at[x], dxo_ref.at[:, columns(x, LW)], own_sem.at[0]),
        pltpu.make_async_copy(dbc_ref.at[x], bco_ref.at[x], own_sem.at[1]),
        pltpu.make_async_copy(ddt_ref.at[x], dto_ref.at[x], own_sem.at[2]),
    ]
    for copy in own:
        copy.start()
    for copy in own:
        copy.wait()
    for d in range(1, NX):
        for copy in to_x(d):
            copy.wait()
    for copy in edges(x):
        copy.wait_send()

    @pl.when(last)
    def _():
        for n in range(NX):
            for copy in edges(n)[:2]:
                copy.wait_recv()

    @pl.when(first)
    def _():
        for n in range(NX):
            for copy in edges(n)[2:]:
                copy.wait_recv()


def exchange_out(dx, dxp, dxn, dbc, dbp, dbn, ddt):
    shapes = (
        jax.ShapeDtypeStruct((BLOCK, INNER), bf16),
        jax.ShapeDtypeStruct((EDGE, INNER), bf16),
        jax.ShapeDtypeStruct((EDGE, INNER), bf16),
        jax.ShapeDtypeStruct((NX, BLOCK, 2 * STATE), bf16),
        jax.ShapeDtypeStruct((NX, EDGE, 2 * STATE), bf16),
        jax.ShapeDtypeStruct((NX, EDGE, 2 * STATE), bf16),
        jax.ShapeDtypeStruct((NX, LH, BLOCK), f32),
    )
    return pl.pallas_call(
        exchange_out_kernel,
        out_shape=shapes,
        in_specs=[vmem()] * 7,
        out_specs=tuple(vmem() for _ in shapes),
        scratch_shapes=[DMA((3,))] + [DMA((3,))] * 6 + [DMA((4,)), DMA((4, NX))],
        compiler_params=pltpu.CompilerParams(
            collective_id=3, has_side_effects=True, vmem_limit_bytes=VMEM_LIMIT
        ),
        name="exchange_out",
    )(dx, dxp, dxn, dbc, dbp, dbn, ddt)


def weight_sum_kernel(
    part_ref, out_ref,
    pair, inr, inl, outr, outl, quarter, piece, xin, zin, held,
    cs, cr, rs, rr, ls, lr, xs, xr, zs, zr, gs, gr, fs, fr,
):
    z, x, y, c = (lax.axis_index(name) for name in ("z", "x", "y", "c"))
    right, left = lax.rem(y + 1, NY), lax.rem(y + NY - 1, NY)
    other = 1 - c
    half = BLOCK // 2
    barrier = pltpu.get_barrier_semaphore()
    for d in range(1, NX):
        greet(barrier, {"x": lax.rem(x + d, NX)})
    for d in range(1, NZ):
        greet(barrier, {"z": lax.rem(z + d, NZ)})
    greet(barrier, {"y": right})
    greet(barrier, {"y": left})
    greet(barrier, {"c": other})
    pl.semaphore_wait(barrier, NX + NZ + 1)

    order = [4, 5, 3, 6, 2, 7, 1, 0]

    def swap(n):
        block = lax.rem(y + order[n], NY)
        return remote(part_ref.at[block, other], pair.at[block], cs.at[n], cr.at[n], {"c": other})

    for n in range(NY):
        swap(n).start()

    def both(block, rows):
        return part_ref[block, c, rows].astype(f32) + pair[block, rows].astype(f32)

    def going_right(s, h):
        rows = pl.ds(h * half, half)
        return remote(outr.at[s, rows], inr.at[s, rows], rs.at[s, h], rr.at[s, h], {"y": right})

    def going_left(s, h):
        rows = pl.ds(h * half, half)
        return remote(outl.at[s, rows], inl.at[s, rows], ls.at[s, h], lr.at[s, h], {"y": left})

    arrived = 0
    for s in range(4):
        need = 2 * s + 2 if s < 3 else 7
        while arrived < need:
            swap(arrived).wait_recv()
            arrived += 1
        for h in range(2):
            rows = pl.ds(h * half, half)
            value = both(lax.rem(y + 4 - s, NY), rows)
            if s > 0:
                going_right(s - 1, h).wait_recv()
                value = value + inr[s - 1, rows].astype(f32)
            outr[s, rows] = value.astype(bf16)
            going_right(s, h).start()
            if s < 3:
                value = both(lax.rem(y + NY - 3 + s, NY), rows)
                if s > 0:
                    going_left(s - 1, h).wait_recv()
                    value = value + inl[s - 1, rows].astype(f32)
                outl[s, rows] = value.astype(bf16)
                going_left(s, h).start()
    swap(7).wait_recv()
    for h in range(2):
        rows = pl.ds(h * half, half)
        value = both(y, rows)
        going_left(2, h).wait_recv()
        value = value + inl[2, rows].astype(f32)
        going_right(3, h).wait_recv()
        quarter[rows] = value + inr[3, rows].astype(f32)

    strip = BLOCK // NX

    def to_x(d):
        peer = lax.rem(x + d, NX)
        return remote(
            quarter.at[columns(peer, strip)], xin.at[d - 1], xs.at[d - 1], xr.at[d - 1], {"x": peer}
        )

    for d in range(1, NX):
        to_x(d).start()
    total = quarter[columns(x, strip)]
    for d in range(1, NX):
        to_x(d).wait_recv()
        total = total + xin[d - 1]
    for i in range(NZ):
        piece[i] = total[8 * (i // 2) : 8 * (i // 2) + 8, 256 * (i % 2) : 256 * (i % 2) + 256]

    def to_z(d):
        peer = lax.rem(z + d, NZ)
        return remote(piece.at[peer], zin.at[d - 1], zs.at[d - 1], zr.at[d - 1], {"z": peer})

    for d in range(1, NZ):
        to_z(d).start()
    value = piece[z]
    for d in range(1, NZ):
        to_z(d).wait_recv()
        value = value + zin[d - 1]
    held[z] = value

    def back_z(d):
        peer = lax.rem(z + d, NZ)
        return remote(held.at[z], held.at[z], gs.at[d - 1], gr.at[d - 1], {"z": peer})

    for d in range(1, NZ):
        back_z(d).start()
    for d in range(1, NZ):
        source = lax.rem(z - d + NZ, NZ)
        remote(held.at[z], held.at[source], gs.at[d - 1], gr.at[d - 1], {"z": source}).wait_recv()
    mine = columns(x, strip)
    rows_out = [
        jnp.concatenate([held[2 * i], held[2 * i + 1]], axis=1) for i in range(NZ // 2)
    ]
    out_ref[mine] = jnp.concatenate(rows_out, axis=0)

    def back_x(d):
        peer = lax.rem(x + d, NX)
        return remote(out_ref.at[mine], out_ref.at[mine], fs.at[d - 1], fr.at[d - 1], {"x": peer})

    for d in range(1, NX):
        back_x(d).start()
    for d in range(1, NX):
        source = lax.rem(x - d + NX, NX)
        theirs = out_ref.at[columns(source, strip)]
        remote(theirs, theirs, fs.at[d - 1], fr.at[d - 1], {"x": source}).wait_recv()
    for d in range(1, NX):
        to_x(d).wait_send()
        back_x(d).wait_send()
    for d in range(1, NZ):
        to_z(d).wait_send()
        back_z(d).wait_send()
    for n in range(NY):
        swap(n).wait_send()
    for h in range(2):
        for s in range(4):
            going_right(s, h).wait_send()
        for s in range(3):
            going_left(s, h).wait_send()


def weight_sum(part):
    width = part.shape[-1]
    strip = BLOCK // NX
    block16 = lambda n: pltpu.VMEM((n, BLOCK, width), bf16)
    return pl.pallas_call(
        weight_sum_kernel,
        out_shape=jax.ShapeDtypeStruct((BLOCK, width), f32),
        in_specs=[vmem()],
        out_specs=vmem(),
        scratch_shapes=[
            block16(NY), block16(4), block16(3), block16(4), block16(3),
            pltpu.VMEM((BLOCK, width), f32),
            pltpu.VMEM((NZ, 8, 256), f32),
            pltpu.VMEM((NX - 1, strip, width), f32),
            pltpu.VMEM((NZ - 1, 8, 256), f32),
            pltpu.VMEM((NZ, 8, 256), f32),
            DMA((8,)), DMA((8,)), DMA((4, 2)), DMA((4, 2)), DMA((3, 2)), DMA((3, 2)),
            DMA((3,)), DMA((3,)), DMA((7,)), DMA((7,)), DMA((7,)), DMA((7,)), DMA((3,)), DMA((3,)),
        ],
        compiler_params=pltpu.CompilerParams(
            collective_id=4, has_side_effects=True, vmem_limit_bytes=VMEM_LIMIT
        ),
        name="weight_sum",
    )(part)


def interleaved(first, second):
    return jnp.concatenate(
        [first[..., :STATE], second[..., :STATE], first[..., STATE:], second[..., STATE:]], axis=-1
    )


def local(
    layer_activity, writer_matrix, reader_matrix, source_unfiltered, switch_raw_signal, saved_result,
    final_adjoint, delta_raw, extra_logdrop, source_filter_coefs, writer_filter_coefs, reader_filter_coefs,
    delta_offset, fading_exponents, direct_factor, rescale_factor,
):
    tokens = layer_activity.shape[1]
    rows = layer_activity.reshape(tokens, -1)
    dy, d_gate = norm_backward(
        saved_result.reshape(tokens, INNER),
        switch_raw_signal.reshape(tokens, INNER),
        final_adjoint.reshape(tokens, INNER),
        rescale_factor.reshape(1, INNER),
    )
    shard = interleaved(writer_matrix, reader_matrix)
    taps = jnp.concatenate([source_filter_coefs, source_filter_coefs], axis=1)
    scalars = jnp.broadcast_to(
        jnp.concatenate([delta_offset, fading_exponents, direct_factor])[:, None], (3, BLOCK)
    )
    params = jnp.concatenate([taps, scalars, jnp.zeros((4, BLOCK), f32)], axis=0)
    drops = extra_logdrop.reshape(NZ, NX, BLOCK)
    message = jnp.concatenate([drops, jnp.broadcast_to(params[None], (NZ, 12, BLOCK))], axis=1)
    delta = delta_raw.reshape(tokens, HEADS).T.astype(f32)
    weights, xh, dyh, dth, prm, xp, xn = exchange_in(
        shard, source_unfiltered.reshape(tokens, INNER), dy, delta, message
    )
    weights = weights.reshape(-1, shard.shape[1])
    projected = jnp.dot(rows, weights, preferred_element_type=f32).astype(bf16)
    bch, bp, bn = maps_in(projected)
    prm = jnp.transpose(prm, (1, 0, 2))
    group = lax.axis_index("x") // 2
    all_taps = interleaved(writer_filter_coefs, reader_filter_coefs)
    map_taps = jnp.where(group == 0, all_taps[:, : 2 * STATE], all_taps[:, 2 * STATE :])
    three, wide, gather = spreaders()
    base = (xh, xp, xn, dyh, bch, bp, bn, dth, prm, map_taps, three)
    sr, sl, decay = chunk_states(*base)
    cr, cl = scan_states(sr, sl, decay)
    grads = chunk_gradients(*base, wide, gather, cr, cl)
    dx, exp, exn, bco, ebp, ebn, ddt = exchange_out(*grads)

    gap = tokens - 2 * EDGE
    edge = jnp.concatenate([exp, jnp.zeros((gap, INNER), bf16), exn], axis=0)
    d_x = (dx.astype(f32) + edge.astype(f32)).astype(bf16)
    maps = bco.astype(f32) + jnp.concatenate(
        [ebp.astype(f32), jnp.zeros((NX, gap, 2 * STATE), f32), ebn.astype(f32)], axis=1
    )
    d_maps = jnp.concatenate([maps[0] + maps[1], maps[2] + maps[3]], axis=1).astype(bf16)
    d_hidden = lax.dot_general(
        d_maps, weights, (((1,), (1,)), ((), ())), preferred_element_type=f32
    ).astype(bf16)
    part = lax.dot_general(
        rows, d_maps, (((0,), (0,)), ((), ())), preferred_element_type=f32
    ).astype(bf16)
    total = weight_sum(part.reshape(NY, NC, BLOCK, -1))
    d_dt = ddt.reshape(HEADS, tokens).T.astype(bf16)
    return (
        d_hidden.reshape(1, tokens, -1),
        d_x.reshape(1, tokens, INNER),
        d_gate.reshape(1, tokens, INNER),
        d_dt.reshape(1, tokens, HEADS),
        jnp.concatenate([total[:, :STATE], total[:, 2 * STATE : 3 * STATE]], axis=1),
        jnp.concatenate([total[:, STATE : 2 * STATE], total[:, 3 * STATE :]], axis=1),
    )


def solution(mesh):
    split = Mesh(mesh.devices.reshape(NZ, NX, NY, NC), ("z", "x", "y", "c"))
    sp, dp = ("z", "x"), ("y", "c")
    in_specs = (
        P(dp, sp, None),
        P(dp, None),
        P(dp, None),
        P(dp, sp, None),
        P(dp, sp, None),
        P(dp, sp, None),
        P(dp, sp, None),
        P(dp, sp, None),
        P(dp, None, sp),
        P(None, sp),
        P(),
        P(),
        P(sp),
        P(sp),
        P(sp),
        P(),
    )
    out_specs = (
        P(dp, sp, None),
        P(dp, sp, None),
        P(dp, sp, None),
        P(dp, sp, None),
        P(dp, None),
        P(dp, None),
    )
    return jax.shard_map(local, mesh=split, in_specs=in_specs, out_specs=out_specs, check_vma=False)
```

time: 539 us -> 213 us (0.40)
  Pallas kernels: 0 us -> 188 us
  waiting for transfers between devices: 123 us -> 0 us
  other arithmetic: 116 us -> 10.4 us
  local copies, waits for them, and re-layouts: 101 us -> 5.3 us
  matrix products: 73.2 us -> 5.05 us
  starting transfers between devices: 64.7 us -> 0 us
  blocking collectives: 36.7 us -> 0 us
  between operations: 17.5 us -> 2.78 us
    pallas_call x0 -> x8, Pallas kernels: none -> 188 us  [the longest x1 47.5 us: scan_states(): pl.pallas_call(scan_kernel, out_shape=(out, out), in_specs=[vmem()] * 3,...]
    all_to_all x8 -> x0, waiting for transfers between devices: 111 us -> none  [the longest x2 61.2 us: in_one_piece(): lax.all_to_all(both, axis, split_axis=split_dim, concat_axis=concat_dim,...]
    dot_general x24 -> x3, matrix products: 72.9 us -> 5.05 us  [the longest x1 2.73 us: local(): projected = jnp.dot(rows, weights, preferred_element_type=f32).astype(bf16)]
    all_to_all x8 -> x0, starting transfers between devices: 64.4 us -> none  [the longest x2 16.1 us: in_one_piece(): lax.all_to_all(both, axis, split_axis=split_dim, concat_axis=concat_dim,...]
    unnamed x4 -> x0, other arithmetic: 49.7 us -> none
    psum x1 -> x0, blocking collectives: 36.7 us -> none  [over_axes(): return functools.reduce(lax.psum, axes, value)]
    concatenate x2 -> x3, local copies, waits for them, and re-layouts: 36.2 us -> 0.23 us  [the longest x1 0.08 us: local(): edge = jnp.concatenate([exp, jnp.zeros((gap, INNER), bf16), exn], axis=0)]
    all_to_all x1 -> x0, other arithmetic: 32.1 us -> none  [local(): lax.all_to_all(delta_derivative.T.reshape(1, window, local_channels), SP,...]
  transfers between devices with their start and end apart: 10 -> 0, of which waited for: 6 -> 0; matrix products, arithmetic and copies ran while one was open for 36% -> 0% of each run, Pallas kernels for 0% -> 0%
where the time goes in v1:
time: 213 us; the launch traced here: 212 us
  Pallas kernels  188 us (88%)
  other arithmetic  10.4 us (5%)
  local copies, waits for them, and re-layouts  5.3 us (2%)
  matrix products  5.05 us (2%)
  between operations  2.78 us (1%)
    pallas_call x1, Pallas kernels, scan_states(): pl.pallas_call(scan_kernel, out_shape=(out, out), in_specs=[vmem()] * 3,...  47.5 us
    pallas_call x1, Pallas kernels, exchange_in(): pl.pallas_call(exchange_in_kernel, out_shape=shapes, in_specs=[vmem()] *...  42.5 us
    pallas_call x1, Pallas kernels, weight_sum(): pl.pallas_call(weight_sum_kernel, out_shape=jax.ShapeDtypeStruct((BLOCK,...  42 us
    pallas_call x1, Pallas kernels, chunk_gradients(): pl.pallas_call(gradients_kernel, out_shape=shapes, in_specs=[vmem()] * 15...  20.1 us
    pallas_call x1, Pallas kernels, maps_in(): pl.pallas_call(maps_in_kernel, out_shape=shapes, in_specs=[vmem()], out_s...  13 us
    pallas_call x1, Pallas kernels, exchange_out(): pl.pallas_call(exchange_out_kernel, out_shape=shapes, in_specs=[vmem()] *...  12.9 us
    pallas_call x1, Pallas kernels, chunk_states(): pl.pallas_call(states_kernel, out_shape=(state, state, jax.ShapeDtypeStru...  6.96 us

profile of v1, /device:TPU:8, one launch (start us, length us, event | category | flops | bytes accessed | tf_op | source)
XLA Modules:
  0.0 211.8 jit_solution(8981832594566725633)
XLA Ops:
  0.6 0.0 copy-start
  0.6 0.0 copy-start.8
  0.7 0.0 copy-start.11
  0.7 0.0 copy-start.6
  0.7 0.9 fusion.35
  1.6 0.7 pad_maximum_fusion.w_ref
  2.2 3.3 %norm_backward.1 = (bf16[128,2048]{1,0:T(8,128)(2,1)}, bf16[128,2048]{1,0:T(8,128)(2,1)}) custom-call(bf16[128,2048]{1,0:T(8,128)(2,1)} %bitcast.47, bf16[128,2048]{1,0:T(8,128)(2,1)} %bitcast.48, bf16[128,2048]{1,0:T(8,128)(2,1)} %bitcast.49, f32[1,2048]{1,0:T(1,128)} %bitcast.52), custom_call_target="tpu_custom_call" | custom-call | tf_op jit(solution)/shard_map/norm_backward/pallas_call | solution.py:73
  5.6 0.0 copy-done.8
  5.6 0.6 convert_bitcast_fusion.dt_ref
  6.2 0.1 pad.21.clone
  8.2 0.1 pad_maximum_fusion.7
  8.3 0.0 copy-done.11
  8.3 0.1 maximum_maximum_fusion
  8.4 0.0 copy-done.6
  8.4 0.6 pad_maximum_fusion.6.msg_ref
  9.0 0.0 copy-start.9
  9.0 0.0 copy-start.10
  9.0 42.5 %exchange_in.1 = (bf16[16,128,512]{2,1,0:T(8,128)(2,1)}, bf16[4,128,512]{2,1,0:T(8,128)(2,1)}, bf16[4,128,512]{2,1,0:T(8,128)(2,1)}, f32[4,8,128]{2,1,0:T(8,128)...) custom-call(bf16[128,512]{1,0:T(8,128)(2,1)} %pad_maximum_fusion.w_ref, ...), custom_call_target="tpu_custom_call" | custom-call | tf_op jit(solution)/shard_map/exchange_in/pallas_call | solution.py:244
  51.6 0.0 copy-start.5
  51.6 0.0 copy-done
  51.6 2.7 %fusion.2.bc_ref = bf16[128,512]{1,0:T(8,128)(2,1)} fusion(bf16[2048,512]{1,0:T(8,128)(2,1)} %bitcast.42, bf16[1,128,2048]{2,1,0:T(8,128)(2,1)S(1)} %copy-done), kind=kOutput, calls=%fused_computation.5 | convolution fusion | flops 268500992 | bytes 2752512 | tf_op jit(solution)/shard_map/dot_general | solution.py:1055
  54.3 13.0 %maps_in.1 = (bf16[4,128,256]{2,1,0:T(8,128)(2,1)}, bf16[16,256]{1,0:T(8,128)(2,1)}, bf16[16,256]{1,0:T(8,128)(2,1)}) custom-call(bf16[128,512]{1,0:T(8,128)(2,1)} %fusion.2.bc_ref), custom_call_target="tpu_custom_call" | custom-call | tf_op jit(solution)/shard_map/maps_in/pallas_call | solution.py:300
  67.3 0.0 copy-done.5
  67.3 0.7 copy.27
  67.9 0.0 copy-done.9
  68.0 0.0 copy-done.10
  68.0 0.6 maximum_select_fusion.taps_ref
  68.6 0.8 fusion.7.three_ref
  69.4 0.7 fusion.10.wide_ref
  70.1 0.6 fusion.13.gather_ref
  70.7 7.0 %chunk_states.1 = (f32[2,128,512]{2,1,0:T(8,128)}, f32[2,128,512]{2,1,0:T(8,128)}, f32[8,512]{1,0:T(8,128)}) custom-call(bf16[4,128,512]{2,1,0:T(8,128)(2,1)} %get-tuple-element.38.xh_ref, bf16[16,512]{1,0:T(8,128)(2,1)} %get-tuple-element.39.xp_ref, bf16[16,512]{1,0:T(8,128)(2,1)} %get-tuple-element.40.xn_ref, ...), custom_call_target="tpu_custom_call" | custom-call | tf_op jit(solution)/shard_map/chunk_states/pallas_call | solution.py:557
  77.7 47.5 %scan_states.1 = (bf16[2,128,512]{2,1,0:T(8,128)(2,1)}, bf16[2,128,512]{2,1,0:T(8,128)(2,1)}) custom-call(f32[2,128,512]{2,1,0:T(8,128)} %get-tuple-element.48.sr_ref, f32[2,128,512]{2,1,0:T(8,128)} %get-tuple-element.49.sl_ref, f32[8,512]{1,0:T(8,128)} %get-tuple-element.50.decay_ref), custom_call_target="tpu_custom_call" | custom-call | tf_op jit(solution)/shard_map/scan_states/pallas_call | solution.py:392
  125.2 0.0 copy-start.1
  125.2 20.1 %chunk_gradients.1 = (bf16[4,128,512]{2,1,0:T(8,128)(2,1)}, bf16[16,512]{1,0:T(8,128)(2,1)}, bf16[16,512]{1,0:T(8,128)(2,1)}, bf16[4,128,256]{2,1,0:T(8,128)(2,1...) custom-call(bf16[4,128,512]{2,1,0:T(8,128)(2,1)} %get-tuple-element.38.xh_ref, ...), custom_call_target="tpu_custom_call" | custom-call | tf_op jit(solution)/shard_map/chunk_gradients/pallas_call | solution.py:720
  145.4 12.9 %exchange_out.1 = (bf16[128,2048]{1,0:T(8,128)(2,1)}, bf16[16,2048]{1,0:T(8,128)(2,1)}, bf16[16,2048]{1,0:T(8,128)(2,1)}, bf16[4,128,256]{2,1,0:T(8,128)(2,1)}, ...) custom-call(bf16[4,128,512]{2,1,0:T(8,128)(2,1)} %get-tuple-element.53.dx_ref, ...), custom_call_target="tpu_custom_call" | custom-call | tf_op jit(solution)/shard_map/exchange_out/pallas_call | solution.py:846
  158.3 0.8 convert_element_type.70
  159.0 0.8 convert_element_type.69
  159.8 0.1 pad.10.clone
  159.9 0.0 copy-start.2
  159.9 0.0 copy-start.3
  159.9 0.0 copy-start.4
  159.9 1.1 maximum_add_fusion
  161.0 0.0 copy-start.7
  161.0 0.0 copy-done.1
  161.1 1.6 fusion.1
  162.6 0.1 pad.5.clone
  162.7 0.0 copy-done.2
  162.7 0.0 copy-done.3
  162.7 0.0 copy-done.4
  162.7 1.0 fusion.3
  163.7 0.0 copy-done.7
  163.7 0.6 convert_bitcast_fusion.1
  164.3 0.7 fusion
  165.0 2.5 %copy.24 = bf16[2048,512]{1,0:T(8,128)(2,1)} copy(bf16[2048,512]{0,1:T(8,128)(2,1)S(1)} %fusion) | data formatting | bytes 4194304 | tf_op jit(solution)/shard_map/convert_element_type | solution.py:1080
  167.6 42.0 %weight_sum.1 = f32[128,512]{1,0:T(8,128)} custom-call(bf16[8,2,128,512]{3,2,1,0:T(8,128)(2,1)} %bitcast.44), custom_call_target="tpu_custom_call" | custom-call | tf_op jit(solution)/shard_map/weight_sum/pallas_call | solution.py:1001
  209.5 1.0 fusion.34
  210.5 0.7 pad_maximum_fusion.2
  211.2 0.7 pad_maximum_fusion.3
  (17 shorter events, 0.1 us)
Async XLA Ops:
  0.6 50.9 %copy-start = (bf16[1,128,2048]{2,1,0:T(8,128)(2,1)S(1)}, bf16[1,128,2048]{2,1,0:T(8,128)(2,1)}, u32[]{:S(2)}) copy-start(bf16[1,128,2048]{2,1,0:T(8,128)(2,1)} %param.16) | copy-start | bytes 1572868
  0.6 4.9 %copy-start.8 = (bf16[1,128,32]{1,2,0:T(8,128)(2,1)S(1)}, bf16[1,128,32]{1,2,0:T(8,128)(2,1)}, u32[]{:S(2)}) copy-start(bf16[1,128,32]{1,2,0:T(8,128)(2,1)} %param.23) | copy-start | bytes 24580
  0.7 7.6 %copy-start.11 = (f32[5,64]{1,0:T(8,128)S(1)}, f32[5,64]{1,0:T(8,128)}, u32[]{:S(2)}) copy-start(f32[5,64]{1,0:T(8,128)} %param.25) | copy-start | bytes 3844
  0.7 7.7 %copy-start.6 = (f32[1,4096,1]{1,2,0:T(1,128)S(1)}, f32[1,4096,1]{1,2,0:T(1,128)}, u32[]{:S(2)}) copy-start(f32[1,4096,1]{1,2,0:T(1,128)} %param.24) | copy-start | bytes 49156
  9.0 58.9 %copy-start.9 = (f32[5,256]{1,0:T(8,128)S(1)}, f32[5,256]{1,0:T(8,128)}, u32[]{:S(2)}) copy-start(f32[5,256]{1,0:T(8,128)} %param.26) | copy-start | bytes 15364
  9.0 58.9 %copy-start.10 = (f32[5,256]{1,0:T(8,128)S(1)}, f32[5,256]{1,0:T(8,128)}, u32[]{:S(2)}) copy-start(f32[5,256]{1,0:T(8,128)} %param.27) | copy-start | bytes 15364
  51.6 15.7 %copy-start.5 = (f32[8,16,128]{2,1,0:T(8,128)S(1)}, f32[8,16,128]{2,1,0:T(8,128)}, u32[]{:S(2)}) copy-start(f32[8,16,128]{2,1,0:T(8,128)} %get-tuple-element.47) | copy-start | bytes 196612
  125.2 35.8 %copy-start.1 = (bf16[16,128,512]{2,1,0:T(8,128)(2,1)S(1)}, bf16[16,128,512]{2,1,0:T(8,128)(2,1)}, u32[]{:S(2)}) copy-start(bf16[16,128,512]{2,1,0:T(8,128)(2,1)} %get-tuple-element.42) | copy-start | bytes 6291460
  159.9 2.9 %copy-start.2 = (bf16[128,2048]{1,0:T(8,128)(2,1)S(1)}, bf16[128,2048]{1,0:T(8,128)(2,1)}, u32[]{:S(2)}) copy-start(bf16[128,2048]{1,0:T(8,128)(2,1)} %get-tuple-element.63) | copy-start | bytes 1572868
  159.9 2.9 %copy-start.3 = (bf16[16,2048]{1,0:T(8,128)(2,1)S(1)}, bf16[16,2048]{1,0:T(8,128)(2,1)}, u32[]{:S(2)}) copy-start(bf16[16,2048]{1,0:T(8,128)(2,1)} %get-tuple-element.64) | copy-start | bytes 196612
  159.9 2.9 %copy-start.4 = (bf16[16,2048]{1,0:T(8,128)(2,1)S(1)}, bf16[16,2048]{1,0:T(8,128)(2,1)}, u32[]{:S(2)}) copy-start(bf16[16,2048]{1,0:T(8,128)(2,1)} %get-tuple-element.65) | copy-start | bytes 196612
  161.0 2.7 %copy-start.7 = (f32[4,8,128]{2,1,0:T(8,128)S(1)}, f32[4,8,128]{2,1,0:T(8,128)}, u32[]{:S(2)}) copy-start(f32[4,8,128]{2,1,0:T(8,128)} %get-tuple-element.67) | copy-start | bytes 49156

commit v2 on v0

v2 whole, which is shorter than its diff:
```python
import functools

import jax
import jax.numpy as jnp
from jax import lax
from jax.experimental import pallas as pl
from jax.experimental.pallas import tpu as pltpu
from jax.sharding import Mesh
from jax.sharding import PartitionSpec as P

HEADS = 32
HEAD_DIM = 64
STATE = 128
GROUPS = 2
NORM_GROUPS = 8
CONV_K = 5
BLOCK = 128
INNER = 2048
NZ, NX, NY, NC = 8, 4, 8, 2
LH = HEADS // NX
LW = LH * HEAD_DIM
CHUNK = NX * BLOCK
EDGE = 16
EPSILON = 1e-06
VMEM_LIMIT = 60 * 1024 * 1024

f32 = jnp.float32
bf16 = jnp.bfloat16
highest = lax.Precision.HIGHEST
MESH = pl.DeviceIdType.MESH
DMA = pltpu.SemaphoreType.DMA


def vmem():
    return pl.BlockSpec(memory_space=pltpu.VMEM)


def remote(src, dst, send, recv, device):
    return pltpu.make_async_remote_copy(
        src_ref=src, dst_ref=dst, send_sem=send, recv_sem=recv, device_id=device, device_id_type=MESH
    )


def greet(barrier, device):
    pl.semaphore_signal(barrier, inc=1, device_id=device, device_id_type=MESH)


def columns(start, size):
    return pl.ds(pl.multiple_of(start * size, size), size)


def dot(a, b):
    return jnp.dot(a, b, preferred_element_type=f32)


def dot_nt(a, b):
    return lax.dot_general(a, b, (((1,), (1,)), ((), ())), preferred_element_type=f32)


def dot_tn(a, b):
    return lax.dot_general(a, b, (((0,), (0,)), ((), ())), preferred_element_type=f32)


def iota2(shape, dim):
    return lax.broadcasted_iota(jnp.int32, shape, dim)


def parts_of(value, count):
    out = []
    for _ in range(count):
        top = value.astype(bf16).astype(f32)
        out.append(top)
        value = value - top
    return out


def silu_parts(pre):
    gate = 1.0 / (1.0 + jnp.exp(-pre))
    return pre * gate, gate * (1.0 + pre * (1.0 - gate))


def norm_group(group, saved_ref, switch_ref, final_ref, gain_ref, dy_ref, dgate_ref):
    width = INNER // NORM_GROUPS
    cols = slice(group * width, (group + 1) * width)
    saved = saved_ref[:, cols].astype(f32)
    switch = switch_ref[:, cols].astype(f32)
    final = final_ref[:, cols].astype(f32)
    gate = 1.0 / (1.0 + jnp.exp(-switch))
    act = switch * gate
    mixed = saved * act
    scale = lax.rsqrt(jnp.mean(mixed * mixed, axis=-1, keepdims=True) + EPSILON)
    d_normed = final * gain_ref[:, cols]
    inner = jnp.mean(d_normed * mixed, axis=-1, keepdims=True)
    d_mixed = d_normed * scale - mixed * (scale * scale * scale * inner)
    dy_ref[:, cols] = (d_mixed * act).astype(bf16)
    slope = gate * (1.0 + switch * (1.0 - gate))
    dgate_ref[:, cols] = (d_mixed * saved * slope).astype(bf16)


def pair_row(prm_ref, row, j):
    lane = iota2((1, 128), 1)
    return jnp.where(lane < HEAD_DIM, prm_ref[2 * j, row : row + 1, :], prm_ref[2 * j + 1, row : row + 1, :])


def fill_padded(pad_ref, body_ref, prev_ref, next_ref, z):
    pad_ref[pl.ds(0, EDGE)] = jnp.where(z == 0, 0.0, prev_ref[...].astype(f32))
    for k in range(NX):
        pad_ref[pl.ds(EDGE + k * BLOCK, BLOCK)] = body_ref[k].astype(f32)
    pad_ref[pl.ds(EDGE + CHUNK, EDGE)] = jnp.where(z == NZ - 1, 0.0, next_ref[...].astype(f32))


def unconvolved(pad_ref, start, size, lanes, tap_of):
    total = jnp.zeros((size, 128), f32)
    for tap in range(CONV_K):
        total = total + tap_of(tap) * pad_ref[pl.ds(start + 2 * EDGE + 2 - tap, size), lanes]
    return total


BUFFERS = dict(
    dy=((BLOCK, INNER), bf16),
    xh=((NX, BLOCK, LW), bf16),
    dyh=((NX, BLOCK, LW), bf16),
    dth=((NX, LH, BLOCK), f32),
    prm=((LH, 16, BLOCK), f32),
    xp=((EDGE, LW), bf16),
    xn=((EDGE, LW), bf16),
    wf=((NY * NC, BLOCK, 2 * GROUPS * STATE), bf16),
    bc=((BLOCK, 2 * GROUPS * STATE), bf16),
    bch=((NX, BLOCK, 2 * STATE), bf16),
    bp=((EDGE, 2 * STATE), bf16),
    bn=((EDGE, 2 * STATE), bf16),
    three=((48, 3 * LW), bf16),
    wide=((24, LH * BLOCK), bf16),
    gather=((LH, LW), bf16),
    xpad=((CHUNK + 2 * EDGE, LW), f32),
    bcpad=((CHUNK + 2 * EDGE, 2 * STATE), f32),
    v16=((CHUNK, LW), bf16),
    pv16=((CHUNK, LW), bf16),
    qv16=((CHUNK, LW), bf16),
    pdy16=((CHUNK, LW), bf16),
    qdy16=((CHUNK, LW), bf16),
    b16=((CHUNK, STATE), bf16),
    c16=((CHUNK, STATE), bf16),
    u=((CHUNK, LW), f32),
    slope=((CHUNK, LW), f32),
    spread=((CHUNK, 3 * LW), f32),
    bs=((CHUNK, STATE), f32),
    cs=((CHUNK, STATE), f32),
    level=((NX, LH, BLOCK), f32),
    gamma=((NX, 8, LW), f32),
    signed=((NX, BLOCK, BLOCK), f32),
    grid_t=((NX, BLOCK, BLOCK), f32),
    weights=((NX, BLOCK, BLOCK), f32),
    right=((NX + 1, 2, STATE, LW), f32),
    left=((NX, 2, STATE, LW), f32),
    sr=((2, STATE, LW), f32),
    sl=((2, STATE, LW), f32),
    decay=((8, LW), f32),
    outr=((2, STATE, LW), bf16),
    outl=((2, STATE, LW), bf16),
    cr=((2, STATE, LW), bf16),
    cl=((2, STATE, LW), bf16),
    dv=((CHUNK, LW), f32),
    dl=((NX, LH, BLOCK), f32),
    dvu=((NX, LH, BLOCK), f32),
    dxpad=((CHUNK + 4 * EDGE, LW), f32),
    dbcpad=((CHUNK + 4 * EDGE, 2 * STATE), f32),
    dx=((NX, BLOCK, LW), bf16),
    dxp=((EDGE, LW), bf16),
    dxn=((EDGE, LW), bf16),
    dbc=((NX, BLOCK, 2 * STATE), bf16),
    dbp=((EDGE, 2 * STATE), bf16),
    dbn=((EDGE, 2 * STATE), bf16),
    ddt=((NX, LH, BLOCK), f32),
    dto=((NX, LH, BLOCK), f32),
    exp=((EDGE, INNER), bf16),
    exn=((EDGE, INNER), bf16),
    bco=((NX, BLOCK, 2 * STATE), bf16),
    ebp=((NX, EDGE, 2 * STATE), bf16),
    ebn=((NX, EDGE, 2 * STATE), bf16),
    dmaps=((BLOCK, 2 * GROUPS * STATE), bf16),
    part=((NY, BLOCK, 2 * GROUPS * STATE), bf16),
    kept=((NY, BLOCK, 2 * GROUPS * STATE), f32),
    pair=((NY, BLOCK, 2 * GROUPS * STATE), bf16),
    inr=((4, BLOCK, 2 * GROUPS * STATE), bf16),
    inl=((4, BLOCK, 2 * GROUPS * STATE), bf16),
    outwr=((4, BLOCK, 2 * GROUPS * STATE), bf16),
    outwl=((4, BLOCK, 2 * GROUPS * STATE), bf16),
    quarter=((BLOCK, 2 * GROUPS * STATE), f32),
    piece=((NZ, 8, 256), f32),
    xin=((NX - 1, BLOCK // NX, 2 * GROUPS * STATE), f32),
    zin=((NZ - 1, 8, 256), f32),
    held=((NZ, 8, 256), f32),
)
PIECES = 16
SEMAPHORES = dict(
    own=(12,), x_s=(3,), x_r=(3,), y_s=(3,), y_r=(3,), t_s=(3,), t_r=(3,), m_s=(8,), m_r=(8,),
    h_s=(4,), h_r=(4,), wr_s=(4, 2), wr_r=(4, 2), wl_s=(4, 2), wl_r=(4, 2), wp_s=(8, 2), wp_r=(8, 2),
    b_s=(3,), b_r=(3,), up_s=(PIECES,), up_r=(PIECES,), dn_s=(PIECES,), dn_r=(PIECES,),
    ox_s=(3,), ox_r=(3,), ob_s=(3,), ob_r=(3,), ot_s=(3,), ot_r=(3,), e_s=(4,), e_r=(4, NX),
    sw_s=(8,), sw_r=(8,), rr_s=(4, 2), rr_r=(4, 2), rl_s=(4, 2), rl_r=(4, 2),
    qx_s=(3,), qx_r=(3,), qz_s=(7,), qz_r=(7,), gz_s=(7,), gz_r=(7,), gx_s=(3,), gx_r=(3,),
)


class Named:
    def __init__(self, names, refs):
        for name, ref in zip(names, refs, strict=True):
            setattr(self, name, ref)


INPUTS = ("w", "act", "x", "switch", "saved", "final", "gain", "dt", "msg", "taps")
OUTPUTS = ("dgate", "dxo", "dhid", "dts", "total")


def kernel(*refs):
    n_in, n_out, n_buf = len(INPUTS), len(OUTPUTS), len(BUFFERS)
    a = Named(INPUTS, refs[:n_in])
    o = Named(OUTPUTS, refs[n_in : n_in + n_out])
    s = Named(BUFFERS, refs[n_in + n_out : n_in + n_out + n_buf])
    m = Named(SEMAPHORES, refs[n_in + n_out + n_buf :])
    z, x, y, c = (lax.axis_index(name) for name in ("z", "x", "y", "c"))
    half = BLOCK // 2
    up, down = lax.rem(z + 1, NZ), lax.rem(z + NZ - 1, NZ)
    north, south = lax.rem(y + 1, NY), lax.rem(y + NY - 1, NY)
    other = 1 - c
    head = z * NX + x
    dest = z // 2
    slot = lax.rem(head, LH)
    mine = dest == x
    first, last = z == 0, z == NZ - 1
    x_first, x_last = x == 0, x == NX - 1

    def when(condition):
        return pl.when(condition)

    def unless(condition):
        return pl.when(jnp.logical_not(condition))

    def sender_of(i):
        return 2 * x + i // NX, i % NX

    def is_me(i):
        sz, sx = sender_of(i)
        return jnp.logical_and(sz == z, sx == x)

    @when(first)
    def _():
        s.cr[...] = jnp.zeros_like(s.cr)

    @when(last)
    def _():
        s.cl[...] = jnp.zeros_like(s.cl)

    @unless(x_first)
    def _():
        s.exp[...] = jnp.zeros_like(s.exp)
        s.ebp[...] = jnp.zeros_like(s.ebp)

    @unless(x_last)
    def _():
        s.exn[...] = jnp.zeros_like(s.exn)
        s.ebn[...] = jnp.zeros_like(s.ebn)

    barrier = pltpu.get_barrier_semaphore()
    for d in range(1, NX):
        greet(barrier, {"x": lax.rem(x + d, NX)})
    for d in range(1, NZ):
        greet(barrier, {"z": lax.rem(z + d, NZ)})
    greet(barrier, {"y": north})
    greet(barrier, {"y": south})
    greet(barrier, {"c": other})
    for i in range(LH):

        @unless(is_me(i))
        def _():
            sz, sx = sender_of(i)
            greet(barrier, {"z": sz, "x": sx})

    @when(x_first)
    def _():
        for n in range(NX):
            greet(barrier, {"z": down, "x": jnp.int32(n)})

    @when(x_last)
    def _():
        for n in range(NX):
            greet(barrier, {"z": up, "x": jnp.int32(n)})

    pl.semaphore_wait(barrier, NX - 1 + NZ - 1 + 3 + NZ - mine.astype(jnp.int32) + 2)

    def rows(h):
        return pl.ds(h * half, half)

    def w_ring(step, h, way):
        block = lax.rem(y - way * step + NY, NY) * NC + c
        src = a.w.at[rows(h)] if step == 0 else s.wf.at[block, rows(h)]
        send, recv, to = (m.wr_s, m.wr_r, north) if way > 0 else (m.wl_s, m.wl_r, south)
        return remote(src, s.wf.at[block, rows(h)], send.at[step, h], recv.at[step, h], {"y": to})

    def w_offset(n):
        return 0 if n == 0 else (-n if n < 5 else n - 4)

    def w_across(n, h):
        block = lax.rem(y + w_offset(n) + NY, NY) * NC + c
        src = a.w.at[rows(h)] if n == 0 else s.wf.at[block, rows(h)]
        return remote(src, s.wf.at[block, rows(h)], m.wp_s.at[n, h], m.wp_r.at[n, h], {"c": other})

    w_steps = [(step, h, way) for step in range(3) for h in range(2) for way in (1, -1)]
    w_steps += [(3, 0, 1), (3, 1, -1)]
    for step, h, way in w_steps[:4]:
        w_ring(step, h, way).start()
    own = [
        pltpu.make_async_copy(a.w, s.wf.at[y * NC + c], m.own.at[0]),
        pltpu.make_async_copy(a.x.at[:, columns(x, LW)], s.xh.at[x], m.own.at[1]),
        pltpu.make_async_copy(a.dt.at[columns(x, LH)], s.dth.at[x], m.own.at[2]),
    ]
    for copy in own:
        copy.start()
    for h in range(2):
        w_across(0, h).start()

    def x_to(d):
        peer = lax.rem(x + d, NX)
        return remote(
            a.x.at[:, columns(peer, LW)], s.xh.at[x], m.x_s.at[d - 1], m.x_r.at[d - 1], {"x": peer}
        )

    def dt_to(d):
        peer = lax.rem(x + d, NX)
        return remote(
            a.dt.at[columns(peer, LH)], s.dth.at[x], m.t_s.at[d - 1], m.t_r.at[d - 1], {"x": peer}
        )

    def dy_to(d):
        peer = lax.rem(x + d, NX)
        return remote(
            s.dy.at[:, columns(peer, LW)], s.dyh.at[x], m.y_s.at[d - 1], m.y_r.at[d - 1], {"x": peer}
        )

    def message(i):
        return remote(
            a.msg.at[i], s.prm.at[slot], m.m_s.at[i], m.m_r.at[slot], {"z": jnp.int32(i), "x": dest}
        )

    for d in range(1, NX):
        x_to(d).start()
        dt_to(d).start()
    keep = pltpu.make_async_copy(a.msg.at[z], s.prm.at[slot], m.own.at[3])
    for i in range(NZ):

        @unless(jnp.logical_and(mine, z == i))
        def _():
            message(i).start()

    @when(mine)
    def _():
        keep.start()

    for group in range(NORM_GROUPS):
        norm_group(group, a.saved, a.switch, a.final, a.gain, s.dy, o.dgate)
    for d in range(1, NX):
        dy_to(d).start()
    own_dy = pltpu.make_async_copy(s.dy.at[:, columns(x, LW)], s.dyh.at[x], m.own.at[4])
    own_dy.start()

    def projected(n, core):
        block = lax.rem(y + w_offset(n) + NY, NY) * NC + core
        return dot(a.act[:, columns(block, BLOCK)], s.wf[block])

    own[0].wait()
    maps = projected(0, c)
    for step in range(4):
        for h in range(2):
            for way in (1, -1):
                if step == 3 and (h == 0) != (way == 1):
                    continue
                w_ring(step, h, way).wait_recv()
                following = (step + 1, h, way)
                if following in w_steps:
                    w_ring(*following).start()
                w_across(1 + step if way == 1 or step == 3 else 5 + step, h).start()
        maps = maps + projected(1 + step, c)
        if step < 3:
            maps = maps + projected(5 + step, c)
        for n in ((0,), (1, 5), (2, 6), (3, 7))[step]:
            for h in range(2):
                w_across(n, h).wait_recv()
            maps = maps + projected(n, other)
    for h in range(2):
        w_across(4, h).wait_recv()
    maps = maps + projected(4, other)
    s.bc[...] = maps.astype(bf16)

    def bc_to(d):
        peer = lax.rem(x + d, NX)
        return remote(
            s.bc.at[:, columns(peer // 2, 2 * STATE)], s.bch.at[x], m.b_s.at[d - 1], m.b_r.at[d - 1], {"x": peer}
        )

    for d in range(1, NX):
        bc_to(d).start()
    own_bc = pltpu.make_async_copy(s.bc.at[:, columns(x // 2, 2 * STATE)], s.bch.at[x], m.own.at[5])
    own_bc.start()

    for d in range(1, NX):
        x_to(d).wait_recv()
    own[1].wait()
    tail_rows, head_rows = pl.ds(BLOCK - EDGE, EDGE), pl.ds(0, EDGE)
    edges_in = [
        remote(s.xh.at[NX - 1, tail_rows], s.xp, m.h_s.at[0], m.h_r.at[0], {"z": up}),
        remote(s.xh.at[0, head_rows], s.xn, m.h_s.at[1], m.h_r.at[1], {"z": down}),
        remote(s.bch.at[NX - 1, tail_rows], s.bp, m.h_s.at[2], m.h_r.at[2], {"z": up}),
        remote(s.bch.at[0, head_rows], s.bn, m.h_s.at[3], m.h_r.at[3], {"z": down}),
    ]
    edges_in[0].start()
    edges_in[1].start()

    r, cc = iota2((48, 3 * LW), 0), iota2((48, 3 * LW), 1)
    s.three[...] = jnp.logical_and(
        r // 16 == cc // LW, jnp.bitwise_and(r, 7) == jnp.bitwise_and(cc, LW - 1) // HEAD_DIM
    ).astype(bf16)
    r, cc = iota2((24, LH * BLOCK), 0), iota2((24, LH * BLOCK), 1)
    s.wide[...] = (jnp.bitwise_and(r, 7) == cc // BLOCK).astype(bf16)
    s.gather[...] = (iota2((LH, LW), 1) // HEAD_DIM == iota2((LH, LW), 0)).astype(bf16)
    for pad in (s.dxpad, s.dbcpad):
        pad[pl.ds(0, 2 * EDGE)] = jnp.zeros((2 * EDGE, pad.shape[1]), f32)
        pad[pl.ds(2 * EDGE + CHUNK, 2 * EDGE)] = jnp.zeros((2 * EDGE, pad.shape[1]), f32)

    for d in range(1, NX):
        dt_to(d).wait_recv()
        dy_to(d).wait_recv()
    own[2].wait()
    own_dy.wait()
    for i in range(LH):

        @unless(is_me(i))
        def _():
            sz, sx = sender_of(i)
            remote(a.msg.at[i], s.prm.at[i], m.m_s.at[i], m.m_r.at[i], {"z": sz, "x": sx}).wait_recv()

    @when(mine)
    def _():
        keep.wait()

    row, col = iota2((BLOCK, BLOCK), 0), iota2((BLOCK, BLOCK), 1)
    upper = (row <= col).astype(f32)
    lower = (row >= col).astype(f32)
    sign = (row > col).astype(f32) - (row < col).astype(f32)
    low_half = iota2((BLOCK, 128), 1) < HEAD_DIM
    head_row = iota2((8, BLOCK), 0)

    edges_in[0].wait()
    edges_in[1].wait()
    fill_padded(s.xpad, s.xh, s.xp, s.xn, z)
    for k in range(NX):
        at = pl.ds(k * BLOCK, BLOCK)
        dt = jax.nn.softplus(s.dth[k] + s.prm[:, 9, :])
        rate = dt * jnp.exp(s.prm[:, 10, :]) + s.prm[:, k, :]
        level = jnp.dot(rate, upper, precision=highest, preferred_element_type=f32)
        total = level[:, BLOCK - 1 : BLOCK]
        s.level[k] = level
        stack = jnp.concatenate(
            parts_of(dt, 2) + parts_of(jnp.exp(-level), 2) + parts_of(jnp.exp(level - total), 2), axis=0
        )
        spread = dot_tn(stack.astype(bf16), s.three[...])
        s.spread[at] = spread
        s.gamma[k] = jnp.broadcast_to(spread[BLOCK - 1 : BLOCK, LW : 2 * LW], (8, LW))
        for j in range(LH // 2):
            lanes = slice(128 * j, 128 * (j + 1))
            pre = jnp.zeros((BLOCK, 128), f32)
            for tap in range(CONV_K):
                pre = pre + pair_row(s.prm, 4 + tap, j) * s.xpad[pl.ds(k * BLOCK + EDGE - 2 + tap, BLOCK), lanes]
            u, slope = silu_parts(pre)
            s.u[at, lanes], s.slope[at, lanes] = u, slope
            pe = spread[:, LW + 128 * j : LW + 128 * (j + 1)]
            qe = spread[:, 2 * LW + 128 * j : 2 * LW + 128 * (j + 1)]
            v = u * spread[:, lanes]
            dy = s.dyh[k, :, lanes].astype(f32)
            s.v16[at, lanes] = v.astype(bf16)
            s.pv16[at, lanes], s.qv16[at, lanes] = (pe * v).astype(bf16), (qe * v).astype(bf16)
            s.pdy16[at, lanes], s.qdy16[at, lanes] = (pe * dy).astype(bf16), (qe * dy).astype(bf16)

    own_bc.wait()
    for d in range(1, NX):
        bc_to(d).wait_recv()
    edges_in[2].start()
    edges_in[3].start()
    edges_in[2].wait()
    edges_in[3].wait()
    fill_padded(s.bcpad, s.bch, s.bp, s.bn, z)
    s.decay[...] = jnp.ones_like(s.decay)
    for k in range(NX):
        at = pl.ds(k * BLOCK, BLOCK)
        for which, held, slopes in ((0, s.b16, s.bs), (1, s.c16, s.cs)):
            lanes = slice(which * STATE, (which + 1) * STATE)
            pre = jnp.zeros((BLOCK, STATE), f32)
            for tap in range(CONV_K):
                pre = pre + a.taps[tap : tap + 1, lanes] * s.bcpad[pl.ds(k * BLOCK + EDGE - 2 + tap, BLOCK), lanes]
            value, slopes[at] = silu_parts(pre)
            held[at] = value.astype(bf16)
        b, cc = s.b16[at], s.c16[at]
        kvr, cdr = dot_tn(b, s.qv16[at]), dot_tn(cc, s.qdy16[at])
        kvl, cdl = dot_tn(b, s.pv16[at]), dot_tn(cc, s.pdy16[at])
        s.right[k + 1, 0], s.right[k + 1, 1] = kvr, cdr
        if k > 0:
            s.left[k - 1, 0], s.left[k - 1, 1] = kvl, cdl
        if k == 0:
            s.sr[0], s.sr[1], s.sl[0], s.sl[1] = kvr, cdr, kvl, cdl
        else:
            g, before = s.gamma[k, 0:1], s.decay[0:1]
            s.sr[0] = s.sr[0] * g + kvr
            s.sr[1] = s.sr[1] * g + cdr
            s.sl[0] = s.sl[0] + before * kvl
            s.sl[1] = s.sl[1] + before * cdl
        s.decay[...] = s.decay[...] * s.gamma[k]

    def piece(n):
        return n // 8, pl.ds(pl.multiple_of(lax.rem(n // 4, 2) * 64, 64), 64), columns(lax.rem(n, 4), 128)

    def going_up(n):
        return remote(s.outr.at[piece(n)], s.cr.at[piece(n)], m.up_s.at[n], m.up_r.at[n], {"z": up})

    def going_down(n):
        return remote(s.outl.at[piece(n)], s.cl.at[piece(n)], m.dn_s.at[n], m.dn_r.at[n], {"z": down})

    def scan_step(t):
        n = t - z

        @when(jnp.logical_and(n >= 0, n < PIECES))
        def _():
            @unless(first)
            def _():
                going_up(n).wait_recv()

            @unless(last)
            def _():
                at = piece(n)
                s.outr[at] = (s.cr[at].astype(f32) * s.decay[0:1, at[2]] + s.sr[at]).astype(bf16)
                going_up(n).start()

        i = t - (NZ - 1 - z)

        @when(jnp.logical_and(i >= 0, i < PIECES))
        def _():
            @unless(last)
            def _():
                going_down(i).wait_recv()

            @unless(first)
            def _():
                at = piece(i)
                s.outl[at] = (s.cl[at].astype(f32) * s.decay[0:1, at[2]] + s.sl[at]).astype(bf16)
                going_down(i).start()

    def within(k, j):
        at = pl.ds(pl.multiple_of(k * BLOCK, BLOCK), BLOCK)
        lanes = columns(j, 128)
        parts = jnp.concatenate(parts_of(s.level[k], 3), axis=0).astype(bf16)
        level_cols = dot_tn(parts, s.wide[:, columns(j, 256)])
        vj, dyj = s.v16[at, lanes], s.dyh[k, :, lanes]
        signed, grid_t = s.signed[k], s.grid_t[k]
        halves = []
        weights = s.weights[k]
        dl = s.dl[k]
        for i in range(2):
            h = 2 * j + i
            near = jnp.exp(-jnp.abs(level_cols[:, 128 * i : 128 * (i + 1)] - s.level[k, pl.ds(h, 1), :]))
            keep_half = low_half if i == 0 else jnp.logical_not(low_half)
            shared = dot_nt(jnp.where(keep_half, dyj, jnp.zeros_like(dyj)), vj) * near
            weights = weights + shared
            crossing = (shared * signed).astype(bf16)
            pick = (head_row == h).astype(bf16)
            dl = dl + dot(pick, crossing) - dot_nt(pick, crossing)
            halves.append(dot((grid_t * near).astype(bf16), dyj))
        s.weights[k] = weights
        s.dl[k] = dl
        s.dv[at, lanes] = jnp.where(low_half, halves[0], halves[1])

    s.weights[...] = jnp.zeros_like(s.weights)
    s.dl[...] = jnp.zeros_like(s.dl)
    for t in range(2):
        scan_step(jnp.int32(t))
    for k in range(NX):
        at = pl.ds(k * BLOCK, BLOCK)
        b, cc = s.b16[at], s.c16[at]
        s.signed[k] = dot_nt(cc, b) * sign
        s.grid_t[k] = dot_nt(b, cc)

    def steps(t, carry):
        scan_step(t + 2)

        @when(t < NX * LH // 2)
        def _():
            within(t // (LH // 2), lax.rem(t, LH // 2))

        return carry

    lax.fori_loop(0, NZ - 1 + PIECES - 2, steps, 0)

    s.right[0, 0], s.right[0, 1] = s.cr[0].astype(f32), s.cr[1].astype(f32)
    s.left[NX - 1, 0], s.left[NX - 1, 1] = s.cl[0].astype(f32), s.cl[1].astype(f32)
    for k in range(NX):
        g = s.gamma[k, 0:1]
        s.right[k + 1, 0] = s.right[k + 1, 0] + s.right[k, 0] * g
        s.right[k + 1, 1] = s.right[k + 1, 1] + s.right[k, 1] * g
    for k in range(NX - 2, -1, -1):
        g = s.gamma[k + 1, 0:1]
        s.left[k, 0] = s.left[k, 0] + g * s.left[k + 1, 0]
        s.left[k, 1] = s.left[k, 1] + g * s.left[k + 1, 1]

    def through(k, carry):
        at = pl.ds(pl.multiple_of(k * BLOCK, BLOCK), BLOCK)
        padded = pl.ds(pl.multiple_of(2 * EDGE + k * BLOCK, EDGE), BLOCK)
        b, cc = s.b16[at], s.c16[at]
        weights = s.weights[k].astype(bf16)
        dc = dot(weights, b)
        db = dot_tn(weights, cc)
        dl = s.dl[k]
        dvu = jnp.zeros((8, BLOCK), f32)
        for j in range(LH // 2):
            lanes = slice(128 * j, 128 * (j + 1))
            kvr, cdr = s.right[k, 0, :, lanes].astype(bf16), s.right[k, 1, :, lanes].astype(bf16)
            kvl, cdl = s.left[k, 0, :, lanes].astype(bf16), s.left[k, 1, :, lanes].astype(bf16)
            pe = s.spread[at, LW + 128 * j : LW + 128 * (j + 1)]
            qe = s.spread[at, 2 * LW + 128 * j : 2 * LW + 128 * (j + 1)]
            from_later, from_earlier = dot(b, cdl), dot(b, cdr)
            pv, qv, pdy, qdy = s.pv16[at, lanes], s.qv16[at, lanes], s.pdy16[at, lanes], s.qdy16[at, lanes]
            dv = s.dv[at, lanes] + qe * from_later + pe * from_earlier
            cross = (
                qv.astype(f32) * from_later - pv.astype(f32) * from_earlier
                + qdy.astype(f32) * dot(cc, kvl) - pdy.astype(f32) * dot(cc, kvr)
            )
            dc = dc + dot_nt(pdy, kvr) + dot_nt(qdy, kvl)
            db = db + dot_nt(qv, cdl) + dot_nt(pv, cdr)
            picks = jnp.concatenate([s.gather[:, lanes]] * 2, axis=1)
            dl = dl + dot_nt(picks, jnp.concatenate(parts_of(cross, 2), axis=1).astype(bf16))
            dvu = dvu + dot_nt(picks, jnp.concatenate(parts_of(dv * s.u[at, lanes], 2), axis=1).astype(bf16))
            du = dv * s.spread[at, lanes] + pair_row(s.prm, 11, j) * s.dyh[k, :, lanes].astype(f32)
            s.dxpad[padded, lanes] = du * s.slope[at, lanes]
        s.dbcpad[padded, 0:STATE] = db * s.bs[at]
        s.dbcpad[padded, STATE : 2 * STATE] = dc * s.cs[at]
        s.dl[k], s.dvu[k] = dl, dvu
        return carry

    lax.fori_loop(0, NX, through, 0)

    def masked_edges(pad, width, tap_for, before_ref, behind_ref):
        for w in range(width // 128):
            lanes = slice(128 * w, 128 * (w + 1))
            before = unconvolved(pad, -EDGE, EDGE, lanes, tap_for(w))
            behind = unconvolved(pad, CHUNK, EDGE, lanes, tap_for(w))
            before_ref[:, lanes] = jnp.where(first, 0.0, before).astype(bf16)
            behind_ref[:, lanes] = jnp.where(last, 0.0, behind).astype(bf16)

    def map_tap(w):
        return lambda tap: a.taps[tap : tap + 1, 128 * w : 128 * (w + 1)]

    def input_tap(j):
        return lambda tap: pair_row(s.prm, 4 + tap, j)

    def bco_to(d):
        peer = lax.rem(x + d, NX)
        return remote(s.dbc.at[peer], s.bco.at[x], m.ob_s.at[d - 1], m.ob_r.at[d - 1], {"x": peer})

    def dto_to(d):
        peer = lax.rem(x + d, NX)
        return remote(s.ddt.at[peer], s.dto.at[x], m.ot_s.at[d - 1], m.ot_r.at[d - 1], {"x": peer})

    def dxo_to(d):
        peer = lax.rem(x + d, NX)
        return remote(
            s.dx.at[peer], o.dxo.at[:, columns(x, LW)], m.ox_s.at[d - 1], m.ox_r.at[d - 1], {"x": peer}
        )

    def edges_out(n):
        before, behind = {"z": down, "x": jnp.int32(NX - 1)}, {"z": up, "x": jnp.int32(0)}
        return (
            remote(s.dbp, s.ebn.at[n], m.e_s.at[0], m.e_r.at[0, n], before),
            remote(s.dbn, s.ebp.at[n], m.e_s.at[1], m.e_r.at[1, n], behind),
            remote(s.dxp, s.exn.at[:, columns(n, LW)], m.e_s.at[2], m.e_r.at[2, n], before),
            remote(s.dxn, s.exp.at[:, columns(n, LW)], m.e_s.at[3], m.e_r.at[3, n], behind),
        )

    masked_edges(s.dbcpad, 2 * STATE, map_tap, s.dbp, s.dbn)
    for copy in edges_out(x)[:2]:
        copy.start()
    for k in range(NX):
        for w in range(2):
            lanes = slice(STATE * w, STATE * (w + 1))
            s.dbc[k, :, lanes] = unconvolved(s.dbcpad, k * BLOCK, BLOCK, lanes, map_tap(w)).astype(bf16)
    for d in (2, 1, 3):
        bco_to(d).start()
    own_bco = pltpu.make_async_copy(s.dbc.at[x], s.bco.at[x], m.own.at[6])
    own_bco.start()

    masked_edges(s.dxpad, LW, input_tap, s.dxp, s.dxn)
    for copy in edges_out(x)[2:]:
        copy.start()
    for k in range(NX):
        for j in range(LH // 2):
            lanes = slice(128 * j, 128 * (j + 1))
            s.dx[k, :, lanes] = unconvolved(s.dxpad, k * BLOCK, BLOCK, lanes, input_tap(j)).astype(bf16)
    for d in (2, 1, 3):
        dxo_to(d).start()
    own_dx = pltpu.make_async_copy(s.dx.at[x], o.dxo.at[:, columns(x, LW)], m.own.at[7])
    own_dx.start()

    own_bco.wait()
    for d in range(1, NX):
        bco_to(d).wait_recv()

    @when(x_last)
    def _():
        for n in range(NX):
            edges_out(n)[0].wait_recv()

    @when(x_first)
    def _():
        for n in range(NX):
            edges_out(n)[1].wait_recv()

    for g in range(GROUPS):
        lanes = slice(2 * STATE * g, 2 * STATE * (g + 1))
        both = s.bco[2 * g].astype(f32) + s.bco[2 * g + 1].astype(f32)
        edge = s.ebp[2 * g].astype(f32) + s.ebp[2 * g + 1].astype(f32)
        s.dmaps[0:EDGE, lanes] = (both[0:EDGE] + edge).astype(bf16)
        s.dmaps[EDGE : BLOCK - EDGE, lanes] = both[EDGE : BLOCK - EDGE].astype(bf16)
        edge = s.ebn[2 * g].astype(f32) + s.ebn[2 * g + 1].astype(f32)
        s.dmaps[BLOCK - EDGE :, lanes] = (both[BLOCK - EDGE :] + edge).astype(bf16)

    order = [4, 3, 5, 2, 6, 1, 7, 0]

    def weight_part(n, core):
        block = lax.rem(y + order[n], NY) * NC + core
        return dot_tn(a.act[:, columns(block, BLOCK)], s.dmaps[...])

    def swap(n):
        return remote(s.part.at[n], s.pair.at[n], m.sw_s.at[n], m.sw_r.at[n], {"c": other})

    for n in range(NY):
        s.part[n] = weight_part(n, other).astype(bf16)
        swap(n).start()
    for n in range(NY):
        s.kept[n] = weight_part(n, c)

    def reduced(step, h, way):
        send, recv, to = (m.rr_s, m.rr_r, north) if way > 0 else (m.rl_s, m.rl_r, south)
        out, into = (s.outwr, s.inr) if way > 0 else (s.outwl, s.inl)
        return remote(out.at[step, rows(h)], into.at[step, rows(h)], send.at[step, h], recv.at[step, h], {"y": to})

    def both_cores(n, h):
        return s.kept[n, rows(h)] + s.pair[n, rows(h)].astype(f32)

    def hidden_part(n):
        s_block = n
        o.dhid[:, 128 * n : 128 * (n + 1)] = dot_nt(s.dmaps[...], s.wf[s_block]).astype(bf16)

    for step in range(4):
        for n in ((0,), (1, 2), (3, 4), (5, 6))[step]:
            swap(n).wait_recv()
        for h in range(2):
            for way in (1, -1):
                if step == 0 and (h == 0) != (way == 1):
                    continue
                n = order.index((way * (4 - step)) % NY)
                value = both_cores(n, h)
                if step > 1 or (step == 1 and (h == 0) == (way == 1)):
                    reduced(step - 1, h, way).wait_recv()
                    value = value + (s.inr if way > 0 else s.inl)[step - 1, rows(h)].astype(f32)
                (s.outwr if way > 0 else s.outwl)[step, rows(h)] = value.astype(bf16)
                reduced(step, h, way).start()
        for n in range(4 * step, 4 * step + 4):
            hidden_part(n)
    swap(7).wait_recv()
    for h in range(2):
        value = both_cores(7, h)
        reduced(3, h, 1).wait_recv()
        value = value + s.inr[3, rows(h)].astype(f32)
        reduced(3, h, -1).wait_recv()
        s.quarter[rows(h)] = value + s.inl[3, rows(h)].astype(f32)

    strip = BLOCK // NX

    def strip_to(d):
        peer = lax.rem(x + d, NX)
        return remote(
            s.quarter.at[columns(peer, strip)], s.xin.at[d - 1], m.qx_s.at[d - 1], m.qx_r.at[d - 1], {"x": peer}
        )

    for d in (2, 1, 3):
        strip_to(d).start()

    own_dx.wait()
    for d in range(1, NX):
        dxo_to(d).wait_recv()

    @when(x_last)
    def _():
        for n in range(NX):
            edges_out(n)[2].wait_recv()
        at = slice(BLOCK - EDGE, BLOCK)
        o.dxo[at, :] = (o.dxo[at, :].astype(f32) + s.exn[...].astype(f32)).astype(bf16)

    @when(x_first)
    def _():
        for n in range(NX):
            edges_out(n)[3].wait_recv()
        o.dxo[0:EDGE, :] = (o.dxo[0:EDGE, :].astype(f32) + s.exp[...].astype(f32)).astype(bf16)

    strips = s.quarter[columns(x, strip)]
    for d in range(1, NX):
        strip_to(d).wait_recv()
        strips = strips + s.xin[d - 1]
    for i in range(NZ):
        s.piece[i] = strips[8 * (i // 2) : 8 * (i // 2) + 8, 256 * (i % 2) : 256 * (i % 2) + 256]

    def piece_to(d):
        peer = lax.rem(z + d, NZ)
        return remote(s.piece.at[peer], s.zin.at[d - 1], m.qz_s.at[d - 1], m.qz_r.at[d - 1], {"z": peer})

    for d in (4, 3, 5, 2, 6, 1, 7):
        piece_to(d).start()

    met = s.right[NX, 0] * s.left[NX - 1, 1] + s.right[NX, 1] * s.left[NX - 1, 0]
    picks = jnp.concatenate([s.gather[...]] * 2, axis=1)
    crossing_end = dot_nt(picks, jnp.concatenate(parts_of(met, 2), axis=1).astype(bf16))
    after = -jnp.sum(crossing_end, axis=1, keepdims=True)
    for k in range(NX - 1, -1, -1):
        d_rate = jnp.dot(s.dl[k], lower, precision=highest, preferred_element_type=f32) + after
        after = d_rate[:, 0:1]
        d_dt = d_rate * jnp.exp(s.prm[:, 10, :]) + s.dvu[k]
        s.ddt[k] = d_dt / (1.0 + jnp.exp(-(s.dth[k] + s.prm[:, 9, :])))
    for d in range(1, NX):
        dto_to(d).start()
    own_ddt = pltpu.make_async_copy(s.ddt.at[x], s.dto.at[x], m.own.at[8])
    own_ddt.start()

    value = s.piece[z]
    for d in range(1, NZ):
        piece_to(d).wait_recv()
        value = value + s.zin[d - 1]
    s.held[z] = value

    def piece_back(d):
        return remote(s.held.at[z], s.held.at[z], m.gz_s.at[d - 1], m.gz_r.at[d - 1], {"z": lax.rem(z + d, NZ)})

    def piece_from(d):
        source = lax.rem(z - d + NZ, NZ)
        return remote(s.held.at[z], s.held.at[source], m.gz_s.at[d - 1], m.gz_r.at[d - 1], {"z": source})

    for d in (4, 3, 5, 2, 6, 1, 7):
        piece_back(d).start()
    own_ddt.wait()
    for d in range(1, NX):
        dto_to(d).wait_recv()
    for n in range(NX):
        o.dts[8 * n : 8 * n + 8] = s.dto[n]
    for d in range(1, NZ):
        piece_from(d).wait_recv()
    own_strip = columns(x, strip)
    o.total[own_strip] = jnp.concatenate(
        [jnp.concatenate([s.held[2 * i], s.held[2 * i + 1]], axis=1) for i in range(NZ // 2)], axis=0
    )

    def strip_back(d):
        at = o.total.at[own_strip]
        return remote(at, at, m.gx_s.at[d - 1], m.gx_r.at[d - 1], {"x": lax.rem(x + d, NX)})

    def strip_from(d):
        source = lax.rem(x - d + NX, NX)
        at = o.total.at[columns(source, strip)]
        return remote(at, at, m.gx_s.at[d - 1], m.gx_r.at[d - 1], {"x": source})

    for d in (2, 1, 3):
        strip_back(d).start()

    for step, h, way in w_steps:
        w_ring(step, h, way).wait_send()
    for h in range(2):
        for n in range(8):
            w_across(n, h).wait_send()
    for d in range(1, NX):
        for copy in (x_to(d), dt_to(d), dy_to(d), bc_to(d), bco_to(d), dto_to(d), dxo_to(d), strip_to(d)):
            copy.wait_send()
    for i in range(NZ):

        @unless(jnp.logical_and(mine, z == i))
        def _():
            message(i).wait_send()

    for copy in edges_out(x):
        copy.wait_send()

    def sent(n, carry):
        @unless(last)
        def _():
            going_up(n).wait_send()

        @unless(first)
        def _():
            going_down(n).wait_send()

        return carry

    lax.fori_loop(0, PIECES, sent, 0)
    for n in range(NY):
        swap(n).wait_send()
    for step in range(4):
        for h in range(2):
            for way in (1, -1):
                if step > 0 or (h == 0) == (way == 1):
                    reduced(step, h, way).wait_send()
    for d in range(1, NZ):
        piece_to(d).wait_send()
        piece_back(d).wait_send()
    for d in range(1, NX):
        strip_from(d).wait_recv()
    for d in range(1, NX):
        strip_back(d).wait_send()


def whole(w, act, x, switch, saved, final, gain, dt, msg, taps):
    shapes = (
        jax.ShapeDtypeStruct((BLOCK, INNER), bf16),
        jax.ShapeDtypeStruct((BLOCK, INNER), bf16),
        jax.ShapeDtypeStruct((BLOCK, INNER), bf16),
        jax.ShapeDtypeStruct((HEADS, BLOCK), f32),
        jax.ShapeDtypeStruct((BLOCK, 2 * GROUPS * STATE), f32),
    )
    scratch = [pltpu.VMEM(shape, dtype) for shape, dtype in BUFFERS.values()]
    scratch += [DMA(shape) for shape in SEMAPHORES.values()]
    return pl.pallas_call(
        kernel,
        out_shape=shapes,
        in_specs=[vmem()] * len(INPUTS),
        out_specs=tuple(vmem() for _ in shapes),
        scratch_shapes=scratch,
        compiler_params=pltpu.CompilerParams(
            collective_id=0, has_side_effects=True, vmem_limit_bytes=VMEM_LIMIT
        ),
        name="mixer_backward",
    )(w, act, x, switch, saved, final, gain, dt, msg, taps)


def interleaved(first, second):
    return jnp.concatenate(
        [first[..., :STATE], second[..., :STATE], first[..., STATE:], second[..., STATE:]], axis=-1
    )


def local(
    layer_activity, writer_matrix, reader_matrix, source_unfiltered, switch_raw_signal, saved_result,
    final_adjoint, delta_raw, extra_logdrop, source_filter_coefs, writer_filter_coefs, reader_filter_coefs,
    delta_offset, fading_exponents, direct_factor, rescale_factor,
):
    tokens = layer_activity.shape[1]
    shard = interleaved(writer_matrix, reader_matrix)
    taps = jnp.concatenate([source_filter_coefs, source_filter_coefs], axis=1)
    scalars = jnp.broadcast_to(
        jnp.concatenate([delta_offset, fading_exponents, direct_factor])[:, None], (3, BLOCK)
    )
    params = jnp.concatenate([taps, scalars, jnp.zeros((4, BLOCK), f32)], axis=0)
    drops = extra_logdrop.reshape(NZ, NX, BLOCK)
    message = jnp.concatenate([drops, jnp.broadcast_to(params[None], (NZ, 12, BLOCK))], axis=1)
    delta = delta_raw.reshape(tokens, HEADS).T.astype(f32)
    group = lax.axis_index("x") // 2
    all_taps = interleaved(writer_filter_coefs, reader_filter_coefs)
    map_taps = jnp.where(group == 0, all_taps[:, : 2 * STATE], all_taps[:, 2 * STATE :])
    d_gate, d_x, d_hidden, d_dt, total = whole(
        shard,
        layer_activity.reshape(tokens, -1),
        source_unfiltered.reshape(tokens, INNER),
        switch_raw_signal.reshape(tokens, INNER),
        saved_result.reshape(tokens, INNER),
        final_adjoint.reshape(tokens, INNER),
        rescale_factor.reshape(1, INNER),
        delta,
        message,
        map_taps,
    )
    return (
        d_hidden.reshape(1, tokens, -1),
        d_x.reshape(1, tokens, INNER),
        d_gate.reshape(1, tokens, INNER),
        d_dt.T.astype(bf16).reshape(1, tokens, HEADS),
        jnp.concatenate([total[:, :STATE], total[:, 2 * STATE : 3 * STATE]], axis=1),
        jnp.concatenate([total[:, STATE : 2 * STATE], total[:, 3 * STATE :]], axis=1),
    )


def solution(mesh):
    split = Mesh(mesh.devices.reshape(NZ, NX, NY, NC), ("z", "x", "y", "c"))
    sp, dp = ("z", "x"), ("y", "c")
    in_specs = (
        P(dp, sp, None),
        P(dp, None),
        P(dp, None),
        P(dp, sp, None),
        P(dp, sp, None),
        P(dp, sp, None),
        P(dp, sp, None),
        P(dp, sp, None),
        P(dp, None, sp),
        P(None, sp),
        P(),
        P(),
        P(sp),
        P(sp),
        P(sp),
        P(),
    )
    out_specs = (
        P(dp, sp, None),
        P(dp, sp, None),
        P(dp, sp, None),
        P(dp, sp, None),
        P(dp, None),
        P(dp, None),
    )
    return jax.shard_map(local, mesh=split, in_specs=in_specs, out_specs=out_specs, check_vma=False)
```

time: 539 us -> 170 us (0.32); the launches traced: 533 us -> 169 us
  Pallas kernels: 0 us -> 155 us
  waiting for transfers between devices: 123 us -> 0 us
  other arithmetic: 116 us -> 5.32 us
  local copies, waits for them, and re-layouts: 101 us -> 6.06 us
  matrix products: 73.2 us -> 0 us
  starting transfers between devices: 64.7 us -> 0 us
  blocking collectives: 36.7 us -> 0 us
  between operations: 17.5 us -> 2.62 us
    pallas_call x0 -> x1, Pallas kernels: none -> 155 us  [whole(): pl.pallas_call(kernel, out_shape=shapes, in_specs=[vmem()] * len(INPUTS),...]
    all_to_all x8 -> x0, waiting for transfers between devices: 111 us -> none  [the longest x2 61.2 us: in_one_piece(): lax.all_to_all(both, axis, split_axis=split_dim, concat_axis=concat_dim,...]
    dot_general x24 -> x0, matrix products: 72.9 us -> none  [the longest x3 17.6 us: one_channel_scan(): jnp.einsum('ktn,ksn->kts', reading, keyed, precision=highest) * within]
    all_to_all x8 -> x0, starting transfers between devices: 64.4 us -> none  [the longest x2 16.1 us: in_one_piece(): lax.all_to_all(both, axis, split_axis=split_dim, concat_axis=concat_dim,...]
    unnamed x4 -> x0, other arithmetic: 49.7 us -> none
    psum x1 -> x0, blocking collectives: 36.7 us -> none  [over_axes(): return functools.reduce(lax.psum, axes, value)]
    concatenate x2 -> x1, local copies, waits for them, and re-layouts: 36.2 us -> 0.08 us  [local(): jnp.concatenate([taps, scalars, jnp.zeros((4, BLOCK), f32)], axis=0)]
    all_to_all x1 -> x0, other arithmetic: 32.1 us -> none  [local(): lax.all_to_all(delta_derivative.T.reshape(1, window, local_channels), SP,...]
  transfers between devices with their start and end apart: 10 -> 0, of which waited for: 6 -> 0; matrix products, arithmetic and copies ran while one was open for 36% -> 0% of each run, Pallas kernels for 0% -> 0%
where the time goes in v2:
time: 170 us; the launch traced here: 169 us
  Pallas kernels  155 us (91%)
  local copies, waits for them, and re-layouts  6.06 us (4%)
  other arithmetic  5.32 us (3%)
  between operations  2.62 us (2%)
    pallas_call x1, Pallas kernels, whole(): pl.pallas_call(kernel, out_shape=shapes, in_specs=[vmem()] * len(INPUTS),...  155 us
    unnamed x23, local copies, waits for them, and re-layouts  4.94 us

profile of v2, /device:TPU:8, one launch (start us, length us, event | category | flops | bytes accessed | tf_op | source)
XLA Modules:
  0.0 169.2 jit_solution(6061403388857312868)
XLA Ops:
  2.6 0.1 pad_maximum_fusion.4
  2.7 0.0 copy-start.9
  2.7 0.0 copy-start.6
  2.7 0.1 pad.13.clone
  2.7 0.6 copy-done.9
  3.3 0.1 maximum_maximum_fusion
  3.4 0.0 copy-done.6
  3.4 0.0 copy-start.7
  3.4 0.0 copy-start.8
  3.4 0.6 convert_bitcast_fusion.refs_7_
  4.0 0.1 copy-done.7
  4.1 0.0 copy-done.8
  4.2 0.6 maximum_select_fusion.refs_9_
  4.8 0.0 copy-start.5
  4.8 0.7 copy-done.5
  5.5 0.0 copy-start.3
  5.5 0.0 copy-start.4
  5.5 0.6 pad_maximum_fusion.3.refs_8_
  6.1 0.2 copy-done.3
  6.3 0.1 copy-done.4
  6.4 0.7 pad_maximum_fusion.refs_0_
  7.1 155.2 %mixer_backward.1 = (bf16[128,2048]{1,0:T(8,128)(2,1)}, bf16[128,2048]{1,0:T(8,128)(2,1)}, bf16[128,2048]{1,0:T(8,128)(2,1)}, f32[32,128]{1,0:T(8,128)}, f32[128,512]{1,0:T(8,128)}) custom-call(bf16[128,512]{1,0:T(8,128)(2,1)} %pad_maximum_fusion.refs_0_, bf16[128,2048]{1,0:T(8,128)(2,1)} %bitcast.22, bf16[128,2048]{1,0:T(8,128)(2,1)} %bitcast.23, ...), custom_call_target="tpu_custom_call" | custom-call | tf_op jit(solution)/shard_map/mixer_backward/pallas_call | solution.py:933
  162.3 1.3 convert_bitcast_fusion.1
  163.6 0.0 copy-start.2
  163.6 1.0 fusion
  164.7 0.7 pad_maximum_fusion.2
  165.3 0.7 pad_maximum_fusion.1
  166.0 0.0 copy-done.2
  166.0 0.0 copy-start.1
  166.0 0.8 copy.28
  166.8 0.4 copy-done.1
  167.2 0.0 copy-start
  167.2 0.8 copy.29
  168.0 0.4 copy-done
  168.4 0.8 copy.30
  (4 shorter events, 0.0 us)
Async XLA Ops:
  2.7 0.7 copy-start.9
  2.7 0.8 copy-start.6
  3.4 0.7 copy-start.7
  3.4 0.7 copy-start.8
  4.8 0.7 copy-start.5
  5.5 0.8 copy-start.3
  5.5 0.9 copy-start.4
  163.6 2.4 %copy-start.2 = (bf16[128,2048]{1,0:T(8,128)(2,1)S(1)}, bf16[128,2048]{1,0:T(8,128)(2,1)}, u32[]{:S(2)}) copy-start(bf16[128,2048]{1,0:T(8,128)(2,1)} %get-tuple-element.11) | copy-start | bytes 1572868
  166.0 1.2 copy-start.1
  167.2 1.2 copy-start

commit v3 on v2

--- a/solution.py
+++ b/solution.py
@@ -117,6 +117,10 @@
 
 
 BUFFERS = dict(
+    w=((BLOCK, 2 * GROUPS * STATE), bf16),
+    dt=((HEADS, BLOCK), f32),
+    msg=((NZ, 16, BLOCK), f32),
+    taps=((8, 2 * STATE), f32),
     dy=((BLOCK, INNER), bf16),
     xh=((NX, BLOCK, LW), bf16),
     dyh=((NX, BLOCK, LW), bf16),
@@ -193,13 +197,17 @@
     held=((NZ, 8, 256), f32),
 )
 PIECES = 16
+LAG = 5
+CUTS = 4
+UNITS = NX * LH // 2
 SEMAPHORES = dict(
     own=(12,), x_s=(3,), x_r=(3,), y_s=(3,), y_r=(3,), t_s=(3,), t_r=(3,), m_s=(8,), m_r=(8,),
-    h_s=(4,), h_r=(4,), wr_s=(4, 2), wr_r=(4, 2), wl_s=(4, 2), wl_r=(4, 2), wp_s=(8, 2), wp_r=(8, 2),
+    h_s=(4, NX), h_r=(4,), wr_s=(4, CUTS), wr_r=(4, CUTS), wl_s=(4, CUTS), wl_r=(4, CUTS),
+    wp_s=(8, CUTS), wp_r=(8, CUTS),
     b_s=(3,), b_r=(3,), up_s=(PIECES,), up_r=(PIECES,), dn_s=(PIECES,), dn_r=(PIECES,),
     ox_s=(3,), ox_r=(3,), ob_s=(3,), ob_r=(3,), ot_s=(3,), ot_r=(3,), e_s=(4,), e_r=(4, NX),
-    sw_s=(8,), sw_r=(8,), rr_s=(4, 2), rr_r=(4, 2), rl_s=(4, 2), rl_r=(4, 2),
-    qx_s=(3,), qx_r=(3,), qz_s=(7,), qz_r=(7,), gz_s=(7,), gz_r=(7,), gx_s=(3,), gx_r=(3,),
+    sw_s=(8,), sw_r=(8,), rr_s=(4, CUTS), rr_r=(4, CUTS), rl_s=(4, CUTS), rl_r=(4, CUTS),
+    qx_s=(3,), qx_r=(3,), qz_s=(7,), qz_r=(7,), gz_s=(7,), gz_r=(7,), gx_s=(2, 3), gx_r=(2, 3),
 )
 
 
@@ -209,8 +217,11 @@
             setattr(self, name, ref)
 
 
-INPUTS = ("w", "act", "x", "switch", "saved", "final", "gain", "dt", "msg", "taps")
-OUTPUTS = ("dgate", "dxo", "dhid", "dts", "total")
+INPUTS = (
+    "wb", "wc", "act", "x", "switch", "saved", "final", "gain", "delta", "drops",
+    "source_taps", "writer_taps", "reader_taps", "offset", "fading", "skip",
+)
+OUTPUTS = ("dgate", "dxo", "dhid", "dts", "dwb", "dwc")
 
 
 def kernel(*refs):
@@ -220,7 +231,7 @@
     s = Named(BUFFERS, refs[n_in + n_out : n_in + n_out + n_buf])
     m = Named(SEMAPHORES, refs[n_in + n_out + n_buf :])
     z, x, y, c = (lax.axis_index(name) for name in ("z", "x", "y", "c"))
-    half = BLOCK // 2
+    cut = BLOCK // CUTS
     up, down = lax.rem(z + 1, NZ), lax.rem(z + NZ - 1, NZ)
     north, south = lax.rem(y + 1, NY), lax.rem(y + NY - 1, NY)
     other = 1 - c
@@ -262,6 +273,27 @@
         s.exn[...] = jnp.zeros_like(s.exn)
         s.ebn[...] = jnp.zeros_like(s.ebn)
 
+    gather_w = []
+    for g in range(GROUPS):
+        lanes = slice(STATE * g, STATE * (g + 1))
+        for n, ref in enumerate((a.wb, a.wc)):
+            to = slice(STATE * (2 * g + n), STATE * (2 * g + n + 1))
+            gather_w.append(pltpu.make_async_copy(ref.at[:, lanes], s.w.at[:, to], m.own.at[2 * g + n]))
+    for copy in gather_w:
+        copy.start()
+    s.dt[...] = a.delta[...].astype(f32)
+    row_taps = jnp.concatenate([a.source_taps[...]] * 2, axis=1)
+    for i in range(NZ):
+        s.msg[i, 0:4] = a.drops[i]
+        s.msg[i, 4:9] = row_taps
+        for n, ref in enumerate((a.offset, a.fading, a.skip)):
+            s.msg[i, 9 + n : 10 + n] = jnp.full((1, BLOCK), ref[0], f32)
+    low_group = x < NX // 2
+    for n, ref in enumerate((a.writer_taps, a.reader_taps)):
+        s.taps[0:CONV_K, STATE * n : STATE * (n + 1)] = jnp.where(low_group, ref[:, :STATE], ref[:, STATE:])
+    for copy in gather_w:
+        copy.wait()
+
     barrier = pltpu.get_barrier_semaphore()
     for d in range(1, NX):
         greet(barrier, {"x": lax.rem(x + d, NX)})
@@ -277,6 +309,9 @@
             sz, sx = sender_of(i)
             greet(barrier, {"z": sz, "x": sx})
 
+    greet(barrier, {"z": down, "x": jnp.int32(NX - 1)})
+    greet(barrier, {"z": up, "x": jnp.int32(0)})
+
     @when(x_first)
     def _():
         for n in range(NX):
@@ -287,14 +322,18 @@
         for n in range(NX):
             greet(barrier, {"z": up, "x": jnp.int32(n)})
 
-    pl.semaphore_wait(barrier, NX - 1 + NZ - 1 + 3 + NZ - mine.astype(jnp.int32) + 2)
+    pl.semaphore_wait(
+        barrier,
+        NX - 1 + NZ - 1 + 3 + NZ + 2
+        - mine.astype(jnp.int32) + NX * x_first.astype(jnp.int32) + NX * x_last.astype(jnp.int32),
+    )
 
     def rows(h):
-        return pl.ds(h * half, half)
+        return pl.ds(h * cut, cut)
 
     def w_ring(step, h, way):
         block = lax.rem(y - way * step + NY, NY) * NC + c
-        src = a.w.at[rows(h)] if step == 0 else s.wf.at[block, rows(h)]
+        src = s.w.at[rows(h)] if step == 0 else s.wf.at[block, rows(h)]
         send, recv, to = (m.wr_s, m.wr_r, north) if way > 0 else (m.wl_s, m.wl_r, south)
         return remote(src, s.wf.at[block, rows(h)], send.at[step, h], recv.at[step, h], {"y": to})
 
@@ -303,22 +342,50 @@
 
     def w_across(n, h):
         block = lax.rem(y + w_offset(n) + NY, NY) * NC + c
-        src = a.w.at[rows(h)] if n == 0 else s.wf.at[block, rows(h)]
+        src = s.w.at[rows(h)] if n == 0 else s.wf.at[block, rows(h)]
         return remote(src, s.wf.at[block, rows(h)], m.wp_s.at[n, h], m.wp_r.at[n, h], {"c": other})
 
-    w_steps = [(step, h, way) for step in range(3) for h in range(2) for way in (1, -1)]
-    w_steps += [(3, 0, 1), (3, 1, -1)]
-    for step, h, way in w_steps[:4]:
+    def near_side(h, way):
+        return (h < CUTS // 2) == (way == 1)
+
+    w_steps = [
+        (step, h, way) for step in range(4) for h in range(CUTS) for way in (1, -1) if step < 3 or near_side(h, way)
+    ]
+    for step, h, way in w_steps[: 2 * CUTS]:
         w_ring(step, h, way).start()
     own = [
-        pltpu.make_async_copy(a.w, s.wf.at[y * NC + c], m.own.at[0]),
+        pltpu.make_async_copy(s.w, s.wf.at[y * NC + c], m.own.at[0]),
         pltpu.make_async_copy(a.x.at[:, columns(x, LW)], s.xh.at[x], m.own.at[1]),
-        pltpu.make_async_copy(a.dt.at[columns(x, LH)], s.dth.at[x], m.own.at[2]),
+        pltpu.make_async_copy(s.dt.at[columns(x, LH)], s.dth.at[x], m.own.at[2]),
     ]
     for copy in own:
         copy.start()
-    for h in range(2):
+    for h in range(CUTS):
         w_across(0, h).start()
+
+    def edge_in(which, n):
+        tail, lead = pl.ds(BLOCK - EDGE, EDGE), pl.ds(0, EDGE)
+        lanes, pair_lanes = columns(n, LW), columns(n // 2, 2 * STATE)
+        src, dst, to = (
+            (a.x.at[tail, lanes], s.xp, up),
+            (a.x.at[lead, lanes], s.xn, down),
+            (s.bc.at[tail, pair_lanes], s.bp, up),
+            (s.bc.at[lead, pair_lanes], s.bn, down),
+        )[which]
+        return remote(src, dst, m.h_s.at[which, n], m.h_r.at[which], {"z": to, "x": jnp.int32(n)})
+
+    def edges_start(pair):
+        for n in range(NX):
+
+            @when(x_last)
+            def _():
+                edge_in(2 * pair, n).start()
+
+            @when(x_first)
+            def _():
+                edge_in(2 * pair + 1, n).start()
+
+    edges_start(0)
 
     def x_to(d):
         peer = lax.rem(x + d, NX)
@@ -329,7 +396,7 @@
     def dt_to(d):
         peer = lax.rem(x + d, NX)
         return remote(
-            a.dt.at[columns(peer, LH)], s.dth.at[x], m.t_s.at[d - 1], m.t_r.at[d - 1], {"x": peer}
+            s.dt.at[columns(peer, LH)], s.dth.at[x], m.t_s.at[d - 1], m.t_r.at[d - 1], {"x": peer}
         )
 
     def dy_to(d):
@@ -340,13 +407,13 @@
 
     def message(i):
         return remote(
-            a.msg.at[i], s.prm.at[slot], m.m_s.at[i], m.m_r.at[slot], {"z": jnp.int32(i), "x": dest}
+            s.msg.at[i], s.prm.at[slot], m.m_s.at[i], m.m_r.at[slot], {"z": jnp.int32(i), "x": dest}
         )
 
     for d in range(1, NX):
         x_to(d).start()
         dt_to(d).start()
-    keep = pltpu.make_async_copy(a.msg.at[z], s.prm.at[slot], m.own.at[3])
+    keep = pltpu.make_async_copy(s.msg.at[z], s.prm.at[slot], m.own.at[3])
     for i in range(NZ):
 
         @unless(jnp.logical_and(mine, z == i))
@@ -368,26 +435,55 @@
         block = lax.rem(y + w_offset(n) + NY, NY) * NC + core
         return dot(a.act[:, columns(block, BLOCK)], s.wf[block])
 
+    def inputs_of(k):
+        for j in range(LH // 2):
+            lanes = slice(128 * j, 128 * (j + 1))
+            pre = jnp.zeros((BLOCK, 128), f32)
+            for tap in range(CONV_K):
+                pre = pre + pair_row(s.prm, 4 + tap, j) * s.xpad[pl.ds(k * BLOCK + EDGE - 2 + tap, BLOCK), lanes]
+            at = pl.ds(k * BLOCK, BLOCK)
+            s.u[at, lanes], s.slope[at, lanes] = silu_parts(pre)
+
     own[0].wait()
     maps = projected(0, c)
     for step in range(4):
-        for h in range(2):
+        for h in range(CUTS):
             for way in (1, -1):
-                if step == 3 and (h == 0) != (way == 1):
+                if step == 3 and not near_side(h, way):
                     continue
                 w_ring(step, h, way).wait_recv()
                 following = (step + 1, h, way)
                 if following in w_steps:
                     w_ring(*following).start()
                 w_across(1 + step if way == 1 or step == 3 else 5 + step, h).start()
-        maps = maps + projected(1 + step, c)
         if step < 3:
-            maps = maps + projected(5 + step, c)
+            maps = maps + projected(1 + step, c) + projected(5 + step, c)
         for n in ((0,), (1, 5), (2, 6), (3, 7))[step]:
-            for h in range(2):
+            for h in range(CUTS):
                 w_across(n, h).wait_recv()
             maps = maps + projected(n, other)
-    for h in range(2):
+        if step == 2:
+            for d in range(1, NX):
+                x_to(d).wait_recv()
+            own[1].wait()
+            edge_in(0, x).wait_recv()
+            edge_in(1, x).wait_recv()
+            for i in range(LH):
+
+                @unless(is_me(i))
+                def _():
+                    sz, sx = sender_of(i)
+                    remote(s.msg.at[i], s.prm.at[i], m.m_s.at[i], m.m_r.at[i], {"z": sz, "x": sx}).wait_recv()
+
+            @when(mine)
+            def _():
+                keep.wait()
+
+            fill_padded(s.xpad, s.xh, s.xp, s.xn, z)
+            for k in range(NX):
+                inputs_of(k)
+    maps = maps + projected(4, c)
+    for h in range(CUTS):
         w_across(4, h).wait_recv()
     maps = maps + projected(4, other)
     s.bc[...] = maps.astype(bf16)
@@ -402,19 +498,7 @@
         bc_to(d).start()
     own_bc = pltpu.make_async_copy(s.bc.at[:, columns(x // 2, 2 * STATE)], s.bch.at[x], m.own.at[5])
     own_bc.start()
-
-    for d in range(1, NX):
-        x_to(d).wait_recv()
-    own[1].wait()
-    tail_rows, head_rows = pl.ds(BLOCK - EDGE, EDGE), pl.ds(0, EDGE)
-    edges_in = [
-        remote(s.xh.at[NX - 1, tail_rows], s.xp, m.h_s.at[0], m.h_r.at[0], {"z": up}),
-        remote(s.xh.at[0, head_rows], s.xn, m.h_s.at[1], m.h_r.at[1], {"z": down}),
-        remote(s.bch.at[NX - 1, tail_rows], s.bp, m.h_s.at[2], m.h_r.at[2], {"z": up}),
-        remote(s.bch.at[0, head_rows], s.bn, m.h_s.at[3], m.h_r.at[3], {"z": down}),
-    ]
-    edges_in[0].start()
-    edges_in[1].start()
+    edges_start(1)
 
     r, cc = iota2((48, 3 * LW), 0), iota2((48, 3 * LW), 1)
     s.three[...] = jnp.logical_and(
@@ -432,17 +516,6 @@
         dy_to(d).wait_recv()
     own[2].wait()
     own_dy.wait()
-    for i in range(LH):
-
-        @unless(is_me(i))
-        def _():
-            sz, sx = sender_of(i)
-            remote(a.msg.at[i], s.prm.at[i], m.m_s.at[i], m.m_r.at[i], {"z": sz, "x": sx}).wait_recv()
-
-    @when(mine)
-    def _():
-        keep.wait()
-
     row, col = iota2((BLOCK, BLOCK), 0), iota2((BLOCK, BLOCK), 1)
     upper = (row <= col).astype(f32)
     lower = (row >= col).astype(f32)
@@ -450,9 +523,6 @@
     low_half = iota2((BLOCK, 128), 1) < HEAD_DIM
     head_row = iota2((8, BLOCK), 0)
 
-    edges_in[0].wait()
-    edges_in[1].wait()
-    fill_padded(s.xpad, s.xh, s.xp, s.xn, z)
     for k in range(NX):
         at = pl.ds(k * BLOCK, BLOCK)
         dt = jax.nn.softplus(s.dth[k] + s.prm[:, 9, :])
@@ -468,14 +538,9 @@
         s.gamma[k] = jnp.broadcast_to(spread[BLOCK - 1 : BLOCK, LW : 2 * LW], (8, LW))
         for j in range(LH // 2):
             lanes = slice(128 * j, 128 * (j + 1))
-            pre = jnp.zeros((BLOCK, 128), f32)
-            for tap in range(CONV_K):
-                pre = pre + pair_row(s.prm, 4 + tap, j) * s.xpad[pl.ds(k * BLOCK + EDGE - 2 + tap, BLOCK), lanes]
-            u, slope = silu_parts(pre)
-            s.u[at, lanes], s.slope[at, lanes] = u, slope
             pe = spread[:, LW + 128 * j : LW + 128 * (j + 1)]
             qe = spread[:, 2 * LW + 128 * j : 2 * LW + 128 * (j + 1)]
-            v = u * spread[:, lanes]
+            v = s.u[at, lanes] * spread[:, lanes]
             dy = s.dyh[k, :, lanes].astype(f32)
             s.v16[at, lanes] = v.astype(bf16)
             s.pv16[at, lanes], s.qv16[at, lanes] = (pe * v).astype(bf16), (qe * v).astype(bf16)
@@ -484,10 +549,8 @@
     own_bc.wait()
     for d in range(1, NX):
         bc_to(d).wait_recv()
-    edges_in[2].start()
-    edges_in[3].start()
-    edges_in[2].wait()
-    edges_in[3].wait()
+    edge_in(2, x).wait_recv()
+    edge_in(3, x).wait_recv()
     fill_padded(s.bcpad, s.bch, s.bp, s.bn, z)
     s.decay[...] = jnp.ones_like(s.decay)
     for k in range(NX):
@@ -496,7 +559,7 @@
             lanes = slice(which * STATE, (which + 1) * STATE)
             pre = jnp.zeros((BLOCK, STATE), f32)
             for tap in range(CONV_K):
-                pre = pre + a.taps[tap : tap + 1, lanes] * s.bcpad[pl.ds(k * BLOCK + EDGE - 2 + tap, BLOCK), lanes]
+                pre = pre + s.taps[tap : tap + 1, lanes] * s.bcpad[pl.ds(k * BLOCK + EDGE - 2 + tap, BLOCK), lanes]
             value, slopes[at] = silu_parts(pre)
             held[at] = value.astype(bf16)
         b, cc = s.b16[at], s.c16[at]
@@ -525,7 +588,7 @@
         return remote(s.outl.at[piece(n)], s.cl.at[piece(n)], m.dn_s.at[n], m.dn_r.at[n], {"z": down})
 
     def scan_step(t):
-        n = t - z
+        n = t - LAG * z
 
         @when(jnp.logical_and(n >= 0, n < PIECES))
         def _():
@@ -539,7 +602,7 @@
                 s.outr[at] = (s.cr[at].astype(f32) * s.decay[0:1, at[2]] + s.sr[at]).astype(bf16)
                 going_up(n).start()
 
-        i = t - (NZ - 1 - z)
+        i = t - LAG * (NZ - 1 - z)
 
         @when(jnp.logical_and(i >= 0, i < PIECES))
         def _():
@@ -579,24 +642,55 @@
 
     s.weights[...] = jnp.zeros_like(s.weights)
     s.dl[...] = jnp.zeros_like(s.dl)
-    for t in range(2):
-        scan_step(jnp.int32(t))
     for k in range(NX):
         at = pl.ds(k * BLOCK, BLOCK)
         b, cc = s.b16[at], s.c16[at]
         s.signed[k] = dot_nt(cc, b) * sign
         s.grid_t[k] = dot_nt(b, cc)
 
+    far = z // (NZ // 2)
+    near_end = z * (1 - far) + (NZ - 1 - z) * far
+    before = LAG * near_end
+    between = before + PIECES
+    until = LAG * (NZ - 1 - near_end)
+
+    def unit(n):
+        within(n // (LH // 2), lax.rem(n, LH // 2))
+
     def steps(t, carry):
-        scan_step(t + 2)
-
-        @when(t < NX * LH // 2)
+        scan_step(t)
+
+        @when(t < before)
         def _():
-            within(t // (LH // 2), lax.rem(t, LH // 2))
+            unit(t)
+
+        @when(jnp.logical_and(t >= between, t < until))
+        def _():
+            def two(i, inner):
+                n = before + 2 * (t - between) + i
+
+                @when(n < UNITS)
+                def _():
+                    unit(n)
+
+                return inner
+
+            lax.fori_loop(0, 2, two, 0)
 
         return carry
 
-    lax.fori_loop(0, NZ - 1 + PIECES - 2, steps, 0)
+    lax.fori_loop(0, PIECES + LAG * (NZ - 1), steps, 0)
+
+    def rest(n, carry):
+        done = jnp.where(until > between, before + 2 * (until - between), before)
+
+        @when(n >= done)
+        def _():
+            unit(n)
+
+        return carry
+
+    lax.fori_loop(0, UNITS, rest, 0)
 
     s.right[0, 0], s.right[0, 1] = s.cr[0].astype(f32), s.cr[1].astype(f32)
     s.left[NX - 1, 0], s.left[NX - 1, 1] = s.cl[0].astype(f32), s.cl[1].astype(f32)
@@ -609,13 +703,24 @@
         s.left[k, 0] = s.left[k, 0] + g * s.left[k + 1, 0]
         s.left[k, 1] = s.left[k, 1] + g * s.left[k + 1, 1]
 
-    def through(k, carry):
+    def map_gradients(k, carry):
+        at = pl.ds(pl.multiple_of(k * BLOCK, BLOCK), BLOCK)
+        padded = pl.ds(pl.multiple_of(2 * EDGE + k * BLOCK, EDGE), BLOCK)
+        weights = s.weights[k].astype(bf16)
+        dc = dot(weights, s.b16[at])
+        db = dot_tn(weights, s.c16[at])
+        dc = dc + dot_nt(s.pdy16[at], s.right[k, 0].astype(bf16)) + dot_nt(s.qdy16[at], s.left[k, 0].astype(bf16))
+        db = db + dot_nt(s.qv16[at], s.left[k, 1].astype(bf16)) + dot_nt(s.pv16[at], s.right[k, 1].astype(bf16))
+        s.dbcpad[padded, 0:STATE] = db * s.bs[at]
+        s.dbcpad[padded, STATE : 2 * STATE] = dc * s.cs[at]
+        return carry
+
+    lax.fori_loop(0, NX, map_gradients, 0)
+
+    def input_gradients(k, carry):
         at = pl.ds(pl.multiple_of(k * BLOCK, BLOCK), BLOCK)
         padded = pl.ds(pl.multiple_of(2 * EDGE + k * BLOCK, EDGE), BLOCK)
         b, cc = s.b16[at], s.c16[at]
-        weights = s.weights[k].astype(bf16)
-        dc = dot(weights, b)
-        db = dot_tn(weights, cc)
         dl = s.dl[k]
         dvu = jnp.zeros((8, BLOCK), f32)
         for j in range(LH // 2):
@@ -631,19 +736,13 @@
                 qv.astype(f32) * from_later - pv.astype(f32) * from_earlier
                 + qdy.astype(f32) * dot(cc, kvl) - pdy.astype(f32) * dot(cc, kvr)
             )
-            dc = dc + dot_nt(pdy, kvr) + dot_nt(qdy, kvl)
-            db = db + dot_nt(qv, cdl) + dot_nt(pv, cdr)
             picks = jnp.concatenate([s.gather[:, lanes]] * 2, axis=1)
             dl = dl + dot_nt(picks, jnp.concatenate(parts_of(cross, 2), axis=1).astype(bf16))
             dvu = dvu + dot_nt(picks, jnp.concatenate(parts_of(dv * s.u[at, lanes], 2), axis=1).astype(bf16))
             du = dv * s.spread[at, lanes] + pair_row(s.prm, 11, j) * s.dyh[k, :, lanes].astype(f32)
             s.dxpad[padded, lanes] = du * s.slope[at, lanes]
-        s.dbcpad[padded, 0:STATE] = db * s.bs[at]
-        s.dbcpad[padded, STATE : 2 * STATE] = dc * s.cs[at]
         s.dl[k], s.dvu[k] = dl, dvu
         return carry
-
-    lax.fori_loop(0, NX, through, 0)
 
     def masked_edges(pad, width, tap_for, before_ref, behind_ref):
         for w in range(width // 128):
@@ -654,7 +753,7 @@
             behind_ref[:, lanes] = jnp.where(last, 0.0, behind).astype(bf16)
 
     def map_tap(w):
-        return lambda tap: a.taps[tap : tap + 1, 128 * w : 128 * (w + 1)]
+        return lambda tap: s.taps[tap : tap + 1, 128 * w : 128 * (w + 1)]
 
     def input_tap(j):
         return lambda tap: pair_row(s.prm, 4 + tap, j)
@@ -694,6 +793,7 @@
     own_bco = pltpu.make_async_copy(s.dbc.at[x], s.bco.at[x], m.own.at[6])
     own_bco.start()
 
+    lax.fori_loop(0, NX, input_gradients, 0)
     masked_edges(s.dxpad, LW, input_tap, s.dxp, s.dxn)
     for copy in edges_out(x)[2:]:
         copy.start()
@@ -741,8 +841,7 @@
     for n in range(NY):
         s.part[n] = weight_part(n, other).astype(bf16)
         swap(n).start()
-    for n in range(NY):
-        s.kept[n] = weight_part(n, c)
+    s.kept[0] = weight_part(0, c)
 
     def reduced(step, h, way):
         send, recv, to = (m.rr_s, m.rr_r, north) if way > 0 else (m.rl_s, m.rl_r, south)
@@ -759,26 +858,28 @@
     for step in range(4):
         for n in ((0,), (1, 2), (3, 4), (5, 6))[step]:
             swap(n).wait_recv()
-        for h in range(2):
+        for h in range(CUTS):
             for way in (1, -1):
-                if step == 0 and (h == 0) != (way == 1):
+                if step == 0 and not near_side(h, way):
                     continue
                 n = order.index((way * (4 - step)) % NY)
                 value = both_cores(n, h)
-                if step > 1 or (step == 1 and (h == 0) == (way == 1)):
+                if step > 1 or (step == 1 and near_side(h, way)):
                     reduced(step - 1, h, way).wait_recv()
                     value = value + (s.inr if way > 0 else s.inl)[step - 1, rows(h)].astype(f32)
                 (s.outwr if way > 0 else s.outwl)[step, rows(h)] = value.astype(bf16)
                 reduced(step, h, way).start()
+        for n in ((1, 2), (3, 4), (5, 6), (7,))[step]:
+            s.kept[n] = weight_part(n, c)
         for n in range(4 * step, 4 * step + 4):
             hidden_part(n)
     swap(7).wait_recv()
-    for h in range(2):
+    for h in range(CUTS):
         value = both_cores(7, h)
-        reduced(3, h, 1).wait_recv()
-        value = value + s.inr[3, rows(h)].astype(f32)
-        reduced(3, h, -1).wait_recv()
-        s.quarter[rows(h)] = value + s.inl[3, rows(h)].astype(f32)
+        for way in (1, -1):
+            reduced(3, h, way).wait_recv()
+            value = value + (s.inr if way > 0 else s.inl)[3, rows(h)].astype(f32)
+        s.quarter[rows(h)] = value
 
     strip = BLOCK // NX
 
@@ -854,32 +955,44 @@
     own_ddt.wait()
     for d in range(1, NX):
         dto_to(d).wait_recv()
-    for n in range(NX):
-        o.dts[8 * n : 8 * n + 8] = s.dto[n]
+    for n in range(NX // 2):
+        o.dts[16 * n : 16 * n + 16] = jnp.concatenate([s.dto[2 * n], s.dto[2 * n + 1]], axis=0).astype(bf16)
     for d in range(1, NZ):
         piece_from(d).wait_recv()
     own_strip = columns(x, strip)
-    o.total[own_strip] = jnp.concatenate(
+    strip_total = jnp.concatenate(
         [jnp.concatenate([s.held[2 * i], s.held[2 * i + 1]], axis=1) for i in range(NZ // 2)], axis=0
     )
-
-    def strip_back(d):
-        at = o.total.at[own_strip]
-        return remote(at, at, m.gx_s.at[d - 1], m.gx_r.at[d - 1], {"x": lax.rem(x + d, NX)})
-
-    def strip_from(d):
+    for n, out in enumerate((o.dwb, o.dwc)):
+        for g in range(GROUPS):
+            lane = STATE * (2 * g + n)
+            out[own_strip, STATE * g : STATE * (g + 1)] = strip_total[:, lane : lane + STATE]
+
+    def strip_back(n, d):
+        at = (o.dwb, o.dwc)[n].at[own_strip]
+        return remote(at, at, m.gx_s.at[n, d - 1], m.gx_r.at[n, d - 1], {"x": lax.rem(x + d, NX)})
+
+    def strip_from(n, d):
         source = lax.rem(x - d + NX, NX)
-        at = o.total.at[columns(source, strip)]
-        return remote(at, at, m.gx_s.at[d - 1], m.gx_r.at[d - 1], {"x": source})
+        at = (o.dwb, o.dwc)[n].at[columns(source, strip)]
+        return remote(at, at, m.gx_s.at[n, d - 1], m.gx_r.at[n, d - 1], {"x": source})
 
     for d in (2, 1, 3):
-        strip_back(d).start()
+        for n in range(2):
+            strip_back(n, d).start()
 
     for step, h, way in w_steps:
         w_ring(step, h, way).wait_send()
-    for h in range(2):
+    for h in range(CUTS):
         for n in range(8):
             w_across(n, h).wait_send()
+    for which in range(4):
+        for n in range(NX):
+
+            @when((x_last, x_first)[which % 2])
+            def _():
+                edge_in(which, n).wait_send()
+
     for d in range(1, NX):
         for copy in (x_to(d), dt_to(d), dy_to(d), bc_to(d), bco_to(d), dto_to(d), dxo_to(d), strip_to(d)):
             copy.wait_send()
@@ -907,46 +1020,44 @@
     for n in range(NY):
         swap(n).wait_send()
     for step in range(4):
-        for h in range(2):
+        for h in range(CUTS):
             for way in (1, -1):
-                if step > 0 or (h == 0) == (way == 1):
+                if step > 0 or near_side(h, way):
                     reduced(step, h, way).wait_send()
     for d in range(1, NZ):
         piece_to(d).wait_send()
         piece_back(d).wait_send()
     for d in range(1, NX):
-        strip_from(d).wait_recv()
-    for d in range(1, NX):
-        strip_back(d).wait_send()
-
-
-def whole(w, act, x, switch, saved, final, gain, dt, msg, taps):
+        for n in range(2):
+            strip_from(n, d).wait_recv()
+    for d in range(1, NX):
+        for n in range(2):
+            strip_back(n, d).wait_send()
+
+
+def whole(*args):
     shapes = (
         jax.ShapeDtypeStruct((BLOCK, INNER), bf16),
         jax.ShapeDtypeStruct((BLOCK, INNER), bf16),
         jax.ShapeDtypeStruct((BLOCK, INNER), bf16),
-        jax.ShapeDtypeStruct((HEADS, BLOCK), f32),
-        jax.ShapeDtypeStruct((BLOCK, 2 * GROUPS * STATE), f32),
+        jax.ShapeDtypeStruct((HEADS, BLOCK), bf16),
+        jax.ShapeDtypeStruct((BLOCK, GROUPS * STATE), f32),
+        jax.ShapeDtypeStruct((BLOCK, GROUPS * STATE), f32),
     )
     scratch = [pltpu.VMEM(shape, dtype) for shape, dtype in BUFFERS.values()]
     scratch += [DMA(shape) for shape in SEMAPHORES.values()]
+    scalar = pl.BlockSpec(memory_space=pltpu.SMEM)
     return pl.pallas_call(
         kernel,
         out_shape=shapes,
-        in_specs=[vmem()] * len(INPUTS),
+        in_specs=[vmem()] * (len(INPUTS) - 3) + [scalar] * 3,
         out_specs=tuple(vmem() for _ in shapes),
         scratch_shapes=scratch,
         compiler_params=pltpu.CompilerParams(
             collective_id=0, has_side_effects=True, vmem_limit_bytes=VMEM_LIMIT
         ),
         name="mixer_backward",
-    )(w, act, x, switch, saved, final, gain, dt, msg, taps)
-
-
-def interleaved(first, second):
-    return jnp.concatenate(
-        [first[..., :STATE], second[..., :STATE], first[..., STATE:], second[..., STATE:]], axis=-1
-    )
+    )(*args)
 
 
 def local(
@@ -955,37 +1066,31 @@
     delta_offset, fading_exponents, direct_factor, rescale_factor,
 ):
     tokens = layer_activity.shape[1]
-    shard = interleaved(writer_matrix, reader_matrix)
-    taps = jnp.concatenate([source_filter_coefs, source_filter_coefs], axis=1)
-    scalars = jnp.broadcast_to(
-        jnp.concatenate([delta_offset, fading_exponents, direct_factor])[:, None], (3, BLOCK)
-    )
-    params = jnp.concatenate([taps, scalars, jnp.zeros((4, BLOCK), f32)], axis=0)
-    drops = extra_logdrop.reshape(NZ, NX, BLOCK)
-    message = jnp.concatenate([drops, jnp.broadcast_to(params[None], (NZ, 12, BLOCK))], axis=1)
-    delta = delta_raw.reshape(tokens, HEADS).T.astype(f32)
-    group = lax.axis_index("x") // 2
-    all_taps = interleaved(writer_filter_coefs, reader_filter_coefs)
-    map_taps = jnp.where(group == 0, all_taps[:, : 2 * STATE], all_taps[:, 2 * STATE :])
-    d_gate, d_x, d_hidden, d_dt, total = whole(
-        shard,
+    d_gate, d_x, d_hidden, d_dt, d_w_b, d_w_c = whole(
+        writer_matrix,
+        reader_matrix,
         layer_activity.reshape(tokens, -1),
         source_unfiltered.reshape(tokens, INNER),
         switch_raw_signal.reshape(tokens, INNER),
         saved_result.reshape(tokens, INNER),
         final_adjoint.reshape(tokens, INNER),
         rescale_factor.reshape(1, INNER),
-        delta,
-        message,
-        map_taps,
+        delta_raw.reshape(tokens, HEADS).T,
+        extra_logdrop.reshape(NZ, NX, BLOCK),
+        source_filter_coefs,
+        writer_filter_coefs,
+        reader_filter_coefs,
+        delta_offset,
+        fading_exponents,
+        direct_factor,
     )
     return (
         d_hidden.reshape(1, tokens, -1),
         d_x.reshape(1, tokens, INNER),
         d_gate.reshape(1, tokens, INNER),
-        d_dt.T.astype(bf16).reshape(1, tokens, HEADS),
-        jnp.concatenate([total[:, :STATE], total[:, 2 * STATE : 3 * STATE]], axis=1),
-        jnp.concatenate([total[:, STATE : 2 * STATE], total[:, 3 * STATE :]], axis=1),
+        d_dt.T.reshape(1, tokens, HEADS),
+        d_w_b,
+        d_w_c,
     )
 
 

time: 170 us -> 128 us (0.75)
  the two profiles are of different devices: /device:TPU:8 before, /device:TPU:16 now
where the time goes in v3:
time: 128 us; the launch traced here: 127 us
  Pallas kernels  119 us (93%)
  local copies, waits for them, and re-layouts  6.18 us (5%)
  between operations  2.6 us (2%)
    pallas_call x1, Pallas kernels, whole(): pl.pallas_call(kernel, out_shape=shapes, in_specs=[vmem()] * (len(INPUTS)...  119 us
    unnamed x16, local copies, waits for them, and re-layouts  6.18 us

profile of v3, /device:TPU:16, one launch (start us, length us, event | category | flops | bytes accessed | tf_op | source)
XLA Modules:
  0.0 127.3 jit_solution(1981531907882027213)
XLA Ops:
  2.6 118.5 %mixer_backward.1 = (bf16[128,2048]{1,0:T(8,128)(2,1)}, bf16[128,2048]{1,0:T(8,128)(2,1)}, bf16[128,2048]{1,0:T(8,128)(2,1)}, bf16[32,128]{1,0:T(8,128)(2,1)}, f32[128,256]{1,0:T(8,128)}, /*index=5*/f32[128,256]{1,0:T(8,128)}) custom-call(bf16[128,256]{1,0:T(8,128)(2,1)} %refs_0_.1, bf16[128,256]{1,0:T(8,128)(2,1)} %refs_1_.1, bf16[128,2048]{1,0:T(8,128)(2,1)} %bitcast.19, ...), custom_call_target="tpu_custom_call" | custom-call | tf_op jit(solution)/shard_map/mixer_backward/pallas_call | solution.py:1050
  121.1 0.0 copy-start.1
  121.1 1.9 %copy.31 = bf16[1,128,2048]{2,1,0:T(8,128)(2,1)} copy(bf16[1,128,2048]{2,1,0:T(8,128)(2,1)} %bitcast.18) | data formatting | bytes 1048576
  123.1 0.0 copy-done.1
  123.1 0.0 copy-start
  123.1 0.8 copy.32
  123.9 0.4 copy-done
  124.3 0.0 copy-start.4
  124.3 0.0 copy-start.3
  124.3 0.8 copy.33
  125.1 0.0 copy-done.4
  125.1 0.6 copy.34
  125.7 0.0 copy-done.3
  125.7 0.0 copy-start.2
  125.7 0.7 copy.35
  126.4 0.3 copy-done.2
  126.7 0.7 copy.36
Async XLA Ops:
  121.1 2.0 %copy-start.1 = (bf16[128,2048]{1,0:T(8,128)(2,1)S(1)}, bf16[128,2048]{1,0:T(8,128)(2,1)}, u32[]{:S(2)}) copy-start(bf16[128,2048]{1,0:T(8,128)(2,1)} %get-tuple-element.13) | copy-start | bytes 1572868
  123.1 1.2 copy-start
  124.3 0.8 copy-start.4
  124.3 1.4 %copy-start.3 = (f32[128,256]{1,0:T(8,128)S(1)}, f32[128,256]{1,0:T(8,128)}, u32[]{:S(2)}) copy-start(f32[128,256]{1,0:T(8,128)} %get-tuple-element.28) | copy-start | bytes 393220
  125.7 1.0 copy-start.2

commit v4 on v3

--- a/solution.py
+++ b/solution.py
@@ -191,13 +191,17 @@
     outwr=((4, BLOCK, 2 * GROUPS * STATE), bf16),
     outwl=((4, BLOCK, 2 * GROUPS * STATE), bf16),
     quarter=((BLOCK, 2 * GROUPS * STATE), f32),
-    piece=((NZ, 8, 256), f32),
-    xin=((NX - 1, BLOCK // NX, 2 * GROUPS * STATE), f32),
-    zin=((NZ - 1, 8, 256), f32),
-    held=((NZ, 8, 256), f32),
+    quarter16=((BLOCK, 2 * GROUPS * STATE), bf16),
+    piece=((NZ, 16, 128), f32),
+    piece16=((NZ, 16, 128), bf16),
+    xin=((NX - 1, BLOCK // NX, 2 * GROUPS * STATE), bf16),
+    zin=((NZ - 1, 16, 128), bf16),
+    held=((NZ, 16, 128), bf16),
+    summed=((BLOCK, 2 * GROUPS * STATE), bf16),
 )
 PIECES = 16
-LAG = 5
+EARLY = 6
+LAG = 8
 CUTS = 4
 UNITS = NX * LH // 2
 SEMAPHORES = dict(
@@ -207,7 +211,7 @@
     b_s=(3,), b_r=(3,), up_s=(PIECES,), up_r=(PIECES,), dn_s=(PIECES,), dn_r=(PIECES,),
     ox_s=(3,), ox_r=(3,), ob_s=(3,), ob_r=(3,), ot_s=(3,), ot_r=(3,), e_s=(4,), e_r=(4, NX),
     sw_s=(8,), sw_r=(8,), rr_s=(4, CUTS), rr_r=(4, CUTS), rl_s=(4, CUTS), rl_r=(4, CUTS),
-    qx_s=(3,), qx_r=(3,), qz_s=(7,), qz_r=(7,), gz_s=(7,), gz_r=(7,), gx_s=(2, 3), gx_r=(2, 3),
+    qx_s=(3,), qx_r=(3,), qz_s=(7,), qz_r=(7,), gz_s=(7,), gz_r=(7,), gx_s=(3,), gx_r=(3,),
 )
 
 
@@ -650,8 +654,8 @@
 
     far = z // (NZ // 2)
     near_end = z * (1 - far) + (NZ - 1 - z) * far
-    before = LAG * near_end
-    between = before + PIECES
+    early = EARLY * near_end
+    between = LAG * near_end + PIECES
     until = LAG * (NZ - 1 - near_end)
 
     def unit(n):
@@ -660,14 +664,14 @@
     def steps(t, carry):
         scan_step(t)
 
-        @when(t < before)
+        @when(jnp.logical_and(t < early, t < UNITS))
         def _():
             unit(t)
 
         @when(jnp.logical_and(t >= between, t < until))
         def _():
             def two(i, inner):
-                n = before + 2 * (t - between) + i
+                n = early + 2 * (t - between) + i
 
                 @when(n < UNITS)
                 def _():
@@ -682,7 +686,7 @@
     lax.fori_loop(0, PIECES + LAG * (NZ - 1), steps, 0)
 
     def rest(n, carry):
-        done = jnp.where(until > between, before + 2 * (until - between), before)
+        done = jnp.where(until > between, early + 2 * (until - between), early)
 
         @when(n >= done)
         def _():
@@ -880,13 +884,14 @@
             reduced(3, h, way).wait_recv()
             value = value + (s.inr if way > 0 else s.inl)[3, rows(h)].astype(f32)
         s.quarter[rows(h)] = value
+        s.quarter16[rows(h)] = value.astype(bf16)
 
     strip = BLOCK // NX
 
     def strip_to(d):
         peer = lax.rem(x + d, NX)
         return remote(
-            s.quarter.at[columns(peer, strip)], s.xin.at[d - 1], m.qx_s.at[d - 1], m.qx_r.at[d - 1], {"x": peer}
+            s.quarter16.at[columns(peer, strip)], s.xin.at[d - 1], m.qx_s.at[d - 1], m.qx_r.at[d - 1], {"x": peer}
         )
 
     for d in (2, 1, 3):
@@ -912,13 +917,14 @@
     strips = s.quarter[columns(x, strip)]
     for d in range(1, NX):
         strip_to(d).wait_recv()
-        strips = strips + s.xin[d - 1]
+        strips = strips + s.xin[d - 1].astype(f32)
     for i in range(NZ):
-        s.piece[i] = strips[8 * (i // 2) : 8 * (i // 2) + 8, 256 * (i % 2) : 256 * (i % 2) + 256]
+        part = strips[16 * (i // 4) : 16 * (i // 4) + 16, 128 * (i % 4) : 128 * (i % 4) + 128]
+        s.piece[i], s.piece16[i] = part, part.astype(bf16)
 
     def piece_to(d):
         peer = lax.rem(z + d, NZ)
-        return remote(s.piece.at[peer], s.zin.at[d - 1], m.qz_s.at[d - 1], m.qz_r.at[d - 1], {"z": peer})
+        return remote(s.piece16.at[peer], s.zin.at[d - 1], m.qz_s.at[d - 1], m.qz_r.at[d - 1], {"z": peer})
 
     for d in (4, 3, 5, 2, 6, 1, 7):
         piece_to(d).start()
@@ -940,8 +946,8 @@
     value = s.piece[z]
     for d in range(1, NZ):
         piece_to(d).wait_recv()
-        value = value + s.zin[d - 1]
-    s.held[z] = value
+        value = value + s.zin[d - 1].astype(f32)
+    s.held[z] = value.astype(bf16)
 
     def piece_back(d):
         return remote(s.held.at[z], s.held.at[z], m.gz_s.at[d - 1], m.gz_r.at[d - 1], {"z": lax.rem(z + d, NZ)})
@@ -960,26 +966,21 @@
     for d in range(1, NZ):
         piece_from(d).wait_recv()
     own_strip = columns(x, strip)
-    strip_total = jnp.concatenate(
-        [jnp.concatenate([s.held[2 * i], s.held[2 * i + 1]], axis=1) for i in range(NZ // 2)], axis=0
-    )
-    for n, out in enumerate((o.dwb, o.dwc)):
-        for g in range(GROUPS):
-            lane = STATE * (2 * g + n)
-            out[own_strip, STATE * g : STATE * (g + 1)] = strip_total[:, lane : lane + STATE]
-
-    def strip_back(n, d):
-        at = (o.dwb, o.dwc)[n].at[own_strip]
-        return remote(at, at, m.gx_s.at[n, d - 1], m.gx_r.at[n, d - 1], {"x": lax.rem(x + d, NX)})
-
-    def strip_from(n, d):
+    for i in range(NZ):
+        at = pl.ds(pl.multiple_of(x * strip + 16 * (i // 4), 16), 16)
+        s.summed[at, 128 * (i % 4) : 128 * (i % 4) + 128] = s.held[i]
+
+    def strip_back(d):
+        at = s.summed.at[own_strip]
+        return remote(at, at, m.gx_s.at[d - 1], m.gx_r.at[d - 1], {"x": lax.rem(x + d, NX)})
+
+    def strip_from(d):
         source = lax.rem(x - d + NX, NX)
-        at = (o.dwb, o.dwc)[n].at[columns(source, strip)]
-        return remote(at, at, m.gx_s.at[n, d - 1], m.gx_r.at[n, d - 1], {"x": source})
+        at = s.summed.at[columns(source, strip)]
+        return remote(at, at, m.gx_s.at[d - 1], m.gx_r.at[d - 1], {"x": source})
 
     for d in (2, 1, 3):
-        for n in range(2):
-            strip_back(n, d).start()
+        strip_back(d).start()
 
     for step, h, way in w_steps:
         w_ring(step, h, way).wait_send()
@@ -1028,11 +1029,13 @@
         piece_to(d).wait_send()
         piece_back(d).wait_send()
     for d in range(1, NX):
-        for n in range(2):
-            strip_from(n, d).wait_recv()
-    for d in range(1, NX):
-        for n in range(2):
-            strip_back(n, d).wait_send()
+        strip_from(d).wait_recv()
+    for n, out in enumerate((o.dwb, o.dwc)):
+        for g in range(GROUPS):
+            lane = STATE * (2 * g + n)
+            out[:, STATE * g : STATE * (g + 1)] = s.summed[:, lane : lane + STATE].astype(f32)
+    for d in range(1, NX):
+        strip_back(d).wait_send()
 
 
 def whole(*args):
@@ -1060,13 +1063,29 @@
     )(*args)
 
 
+def deliver_kernel(*refs):
+    half = len(refs) // 2
+    for given, out in zip(refs[:half], refs[half:], strict=True):
+        out[...] = given[...]
+
+
+def delivered(arrays):
+    return pl.pallas_call(
+        deliver_kernel,
+        out_shape=tuple(jax.ShapeDtypeStruct(v.shape, v.dtype) for v in arrays),
+        in_specs=[vmem()] * len(arrays),
+        out_specs=tuple(vmem() for _ in arrays),
+        name="deliver",
+    )(*arrays)
+
+
 def local(
     layer_activity, writer_matrix, reader_matrix, source_unfiltered, switch_raw_signal, saved_result,
     final_adjoint, delta_raw, extra_logdrop, source_filter_coefs, writer_filter_coefs, reader_filter_coefs,
     delta_offset, fading_exponents, direct_factor, rescale_factor,
 ):
     tokens = layer_activity.shape[1]
-    d_gate, d_x, d_hidden, d_dt, d_w_b, d_w_c = whole(
+    outputs = whole(
         writer_matrix,
         reader_matrix,
         layer_activity.reshape(tokens, -1),
@@ -1084,6 +1103,7 @@
         fading_exponents,
         direct_factor,
     )
+    d_gate, d_x, d_hidden, d_dt, d_w_b, d_w_c = delivered(outputs)
     return (
         d_hidden.reshape(1, tokens, -1),
         d_x.reshape(1, tokens, INNER),

time: 128 us -> 120 us (0.938)
  local copies, waits for them, and re-layouts: 6.18 us -> 0 us
  Pallas kernels: 119 us -> 117 us
    unnamed x16 -> x0, local copies, waits for them, and re-layouts: 6.18 us -> none
    pallas_call x1, Pallas kernels: 119 us -> 114 us  [whole(): pl.pallas_call(kernel, out_shape=shapes, in_specs=[vmem()] * (len(INPUTS)...]
    pallas_call x0 -> x1, Pallas kernels: none -> 2.69 us  [delivered(): pl.pallas_call(deliver_kernel, out_shape=tuple((jax.ShapeDtypeStruct(v.sh...]
where the time goes in v4:
time: 120 us; the launch traced here: 119 us
  Pallas kernels  117 us (98%)
  between operations  2.58 us (2%)
    pallas_call x1, Pallas kernels, whole(): pl.pallas_call(kernel, out_shape=shapes, in_specs=[vmem()] * (len(INPUTS)...  114 us
    pallas_call x1, Pallas kernels, delivered(): pl.pallas_call(deliver_kernel, out_shape=tuple((jax.ShapeDtypeStruct(v.sh...  2.69 us

profile of v4, /device:TPU:16, one launch (start us, length us, event | category | flops | bytes accessed | tf_op | source)
XLA Modules:
  0.0 119.4 jit_solution(14774499086505712303)
XLA Ops:
  2.6 114.1 %mixer_backward.1 = (bf16[128,2048]{1,0:T(8,128)(2,1)}, bf16[128,2048]{1,0:T(8,128)(2,1)}, bf16[128,2048]{1,0:T(8,128)(2,1)}, bf16[32,128]{1,0:T(8,128)(2,1)}, f32[128,256]{1,0:T(8,128)}, /*index=5*/f32[128,256]{1,0:T(8,128)}) custom-call(bf16[128,256]{1,0:T(8,128)(2,1)} %refs_0_.1, bf16[128,256]{1,0:T(8,128)(2,1)} %refs_1_.1, bf16[128,2048]{1,0:T(8,128)(2,1)} %bitcast.16, ...), custom_call_target="tpu_custom_call" | custom-call | tf_op jit(solution)/shard_map/mixer_backward/pallas_call | solution.py:1053
  116.7 2.7 %deliver.1 = (bf16[128,2048]{1,0:T(8,128)(2,1)}, bf16[128,2048]{1,0:T(8,128)(2,1)}, bf16[128,2048]{1,0:T(8,128)(2,1)}, bf16[32,128]{1,0:T(8,128)(2,1)}, f32[128,256]{1,0:T(8,128)}, /*index=5*/f32[128,256]{1,0:T(8,128)}) custom-call(bf16[128,2048]{1,0:T(8,128)(2,1)} %get-tuple-element.18.refs_0_, bf16[128,2048]{1,0:T(8,128)(2,1)} %get-tuple-element.19.refs_1_, ...), custom_call_target="tpu_custom_call" | custom-call | tf_op jit(solution)/shard_map/deliver/pallas_call | solution.py:1073

commit v5 on v4

--- a/solution.py
+++ b/solution.py
@@ -116,7 +116,12 @@
     return total
 
 
+STREAMED = ("x", "saved", "switch", "final", "act")
 BUFFERS = dict(
+    **{f"{name}_in": ((BLOCK, INNER), bf16) for name in STREAMED},
+    dgate_out=((BLOCK, INNER), bf16),
+    dxo_out=((BLOCK, INNER), bf16),
+    dhid_out=((BLOCK, INNER), bf16),
     w=((BLOCK, 2 * GROUPS * STATE), bf16),
     dt=((HEADS, BLOCK), f32),
     msg=((NZ, 16, BLOCK), f32),
@@ -205,7 +210,7 @@
 CUTS = 4
 UNITS = NX * LH // 2
 SEMAPHORES = dict(
-    own=(12,), x_s=(3,), x_r=(3,), y_s=(3,), y_r=(3,), t_s=(3,), t_r=(3,), m_s=(8,), m_r=(8,),
+    own=(12,), big=(8,), x_s=(3,), x_r=(3,), y_s=(3,), y_r=(3,), t_s=(3,), t_r=(3,), m_s=(8,), m_r=(8,),
     h_s=(4, NX), h_r=(4,), wr_s=(4, CUTS), wr_r=(4, CUTS), wl_s=(4, CUTS), wl_r=(4, CUTS),
     wp_s=(8, CUTS), wp_r=(8, CUTS),
     b_s=(3,), b_r=(3,), up_s=(PIECES,), up_r=(PIECES,), dn_s=(PIECES,), dn_r=(PIECES,),
@@ -276,6 +281,18 @@
     def _():
         s.exn[...] = jnp.zeros_like(s.exn)
         s.ebn[...] = jnp.zeros_like(s.ebn)
+
+    loads = {}
+    for n, name in enumerate(STREAMED):
+        held_here = getattr(s, f"{name}_in")
+        loads[name] = pltpu.make_async_copy(getattr(a, name), held_here, m.big.at[n])
+        loads[name].start()
+        setattr(a, name, held_here)
+    stores = [
+        pltpu.make_async_copy(s.dgate_out, o.dgate, m.big.at[5]),
+        pltpu.make_async_copy(s.dhid_out, o.dhid, m.big.at[6]),
+        pltpu.make_async_copy(s.dxo_out, o.dxo, m.big.at[7]),
+    ]
 
     gather_w = []
     for g in range(GROUPS):
@@ -357,6 +374,7 @@
     ]
     for step, h, way in w_steps[: 2 * CUTS]:
         w_ring(step, h, way).start()
+    loads["x"].wait()
     own = [
         pltpu.make_async_copy(s.w, s.wf.at[y * NC + c], m.own.at[0]),
         pltpu.make_async_copy(a.x.at[:, columns(x, LW)], s.xh.at[x], m.own.at[1]),
@@ -428,12 +446,15 @@
     def _():
         keep.start()
 
+    for name in STREAMED[1:]:
+        loads[name].wait()
     for group in range(NORM_GROUPS):
-        norm_group(group, a.saved, a.switch, a.final, a.gain, s.dy, o.dgate)
+        norm_group(group, a.saved, a.switch, a.final, a.gain, s.dy, s.dgate_out)
     for d in range(1, NX):
         dy_to(d).start()
     own_dy = pltpu.make_async_copy(s.dy.at[:, columns(x, LW)], s.dyh.at[x], m.own.at[4])
     own_dy.start()
+    stores[0].start()
 
     def projected(n, core):
         block = lax.rem(y + w_offset(n) + NY, NY) * NC + core
@@ -498,7 +519,7 @@
             s.bc.at[:, columns(peer // 2, 2 * STATE)], s.bch.at[x], m.b_s.at[d - 1], m.b_r.at[d - 1], {"x": peer}
         )
 
-    for d in range(1, NX):
+    for d in (2, 1, 3):
         bc_to(d).start()
     own_bc = pltpu.make_async_copy(s.bc.at[:, columns(x // 2, 2 * STATE)], s.bch.at[x], m.own.at[5])
     own_bc.start()
@@ -773,7 +794,7 @@
     def dxo_to(d):
         peer = lax.rem(x + d, NX)
         return remote(
-            s.dx.at[peer], o.dxo.at[:, columns(x, LW)], m.ox_s.at[d - 1], m.ox_r.at[d - 1], {"x": peer}
+            s.dx.at[peer], s.dxo_out.at[:, columns(x, LW)], m.ox_s.at[d - 1], m.ox_r.at[d - 1], {"x": peer}
         )
 
     def edges_out(n):
@@ -807,7 +828,7 @@
             s.dx[k, :, lanes] = unconvolved(s.dxpad, k * BLOCK, BLOCK, lanes, input_tap(j)).astype(bf16)
     for d in (2, 1, 3):
         dxo_to(d).start()
-    own_dx = pltpu.make_async_copy(s.dx.at[x], o.dxo.at[:, columns(x, LW)], m.own.at[7])
+    own_dx = pltpu.make_async_copy(s.dx.at[x], s.dxo_out.at[:, columns(x, LW)], m.own.at[7])
     own_dx.start()
 
     own_bco.wait()
@@ -857,7 +878,7 @@
 
     def hidden_part(n):
         s_block = n
-        o.dhid[:, 128 * n : 128 * (n + 1)] = dot_nt(s.dmaps[...], s.wf[s_block]).astype(bf16)
+        s.dhid_out[:, 128 * n : 128 * (n + 1)] = dot_nt(s.dmaps[...], s.wf[s_block]).astype(bf16)
 
     for step in range(4):
         for n in ((0,), (1, 2), (3, 4), (5, 6))[step]:
@@ -897,6 +918,8 @@
     for d in (2, 1, 3):
         strip_to(d).start()
 
+    stores[1].start()
+
     own_dx.wait()
     for d in range(1, NX):
         dxo_to(d).wait_recv()
@@ -906,14 +929,15 @@
         for n in range(NX):
             edges_out(n)[2].wait_recv()
         at = slice(BLOCK - EDGE, BLOCK)
-        o.dxo[at, :] = (o.dxo[at, :].astype(f32) + s.exn[...].astype(f32)).astype(bf16)
+        s.dxo_out[at, :] = (s.dxo_out[at, :].astype(f32) + s.exn[...].astype(f32)).astype(bf16)
 
     @when(x_first)
     def _():
         for n in range(NX):
             edges_out(n)[3].wait_recv()
-        o.dxo[0:EDGE, :] = (o.dxo[0:EDGE, :].astype(f32) + s.exp[...].astype(f32)).astype(bf16)
-
+        s.dxo_out[0:EDGE, :] = (s.dxo_out[0:EDGE, :].astype(f32) + s.exp[...].astype(f32)).astype(bf16)
+
+    stores[2].start()
     strips = s.quarter[columns(x, strip)]
     for d in range(1, NX):
         strip_to(d).wait_recv()
@@ -1028,6 +1052,8 @@
     for d in range(1, NZ):
         piece_to(d).wait_send()
         piece_back(d).wait_send()
+    for copy in stores:
+        copy.wait()
     for d in range(1, NX):
         strip_from(d).wait_recv()
     for n, out in enumerate((o.dwb, o.dwc)):
@@ -1050,11 +1076,12 @@
     scratch = [pltpu.VMEM(shape, dtype) for shape, dtype in BUFFERS.values()]
     scratch += [DMA(shape) for shape in SEMAPHORES.values()]
     scalar = pl.BlockSpec(memory_space=pltpu.SMEM)
+    anywhere = pl.BlockSpec(memory_space=pl.ANY)
     return pl.pallas_call(
         kernel,
         out_shape=shapes,
-        in_specs=[vmem()] * (len(INPUTS) - 3) + [scalar] * 3,
-        out_specs=tuple(vmem() for _ in shapes),
+        in_specs=[anywhere if name in STREAMED else vmem() for name in INPUTS[:-3]] + [scalar] * 3,
+        out_specs=(anywhere,) * 3 + (vmem(),) * 3,
         scratch_shapes=scratch,
         compiler_params=pltpu.CompilerParams(
             collective_id=0, has_side_effects=True, vmem_limit_bytes=VMEM_LIMIT

time: 120 us -> 119 us (level)
  no operation moved by 1% of the time
where the time goes in v5:
time: 119 us; the launch traced here: 118 us
  Pallas kernels  116 us (97%)
  between operations  2.58 us (2%)
    pallas_call x1, Pallas kernels, whole(): pl.pallas_call(kernel, out_shape=shapes, in_specs=[anywhere if name in ST...  113 us
    pallas_call x1, Pallas kernels, delivered(): pl.pallas_call(deliver_kernel, out_shape=tuple((jax.ShapeDtypeStruct(v.sh...  2.69 us

profile of v5, /device:TPU:16, one launch (start us, length us, event | category | flops | bytes accessed | tf_op | source)
XLA Modules:
  0.0 118.4 jit_solution(14099590381368020208)
XLA Ops:
  2.6 113.1 %mixer_backward.1 = (bf16[128,2048]{1,0:T(8,128)(2,1)}, bf16[128,2048]{1,0:T(8,128)(2,1)}, bf16[128,2048]{1,0:T(8,128)(2,1)}, bf16[32,128]{1,0:T(8,128)(2,1)}, f32[128,256]{1,0:T(8,128)}, /*index=5*/f32[128,256]{1,0:T(8,128)}) custom-call(bf16[128,256]{1,0:T(8,128)(2,1)} %refs_0_.1, bf16[128,256]{1,0:T(8,128)(2,1)} %refs_1_.1, bf16[128,2048]{1,0:T(8,128)(2,1)} %bitcast.16, ...), custom_call_target="tpu_custom_call" | custom-call | tf_op jit(solution)/shard_map/mixer_backward/pallas_call | solution.py:1080
  115.7 2.7 %deliver.1 = (bf16[128,2048]{1,0:T(8,128)(2,1)}, bf16[128,2048]{1,0:T(8,128)(2,1)}, bf16[128,2048]{1,0:T(8,128)(2,1)}, bf16[32,128]{1,0:T(8,128)(2,1)}, f32[128,256]{1,0:T(8,128)}, /*index=5*/f32[128,256]{1,0:T(8,128)}) custom-call(bf16[128,2048]{1,0:T(8,128)(2,1)} %get-tuple-element.18.refs_0_, bf16[128,2048]{1,0:T(8,128)(2,1)} %get-tuple-element.19.refs_1_, ...), custom_call_target="tpu_custom_call" | custom-call | tf_op jit(solution)/shard_map/deliver/pallas_call | solution.py:1100
